TPU v7x, 512 devices: a whole 4x4x16 slice. The times are simulated.
512 devices in a mesh: sp: 128 (over z, x, core), tp: 4 (over y).
Axes of the slice: x: 4, y: 4, z: 16, core: 2. Of those that a mesh axis runs over, the one named last changes fastest.
Arguments:
- query_main: bfloat16 [16384, 2048], P('sp', 'tp'), may hold values from -6 to 6
- query_rotary: bfloat16 [16384, 1024], P('sp', 'tp'), may hold values from -7 to 7
- latent: bfloat16 [16384, 512], P('sp'), may hold values from -24 to 24
- key_rotary: bfloat16 [16384, 64], P('sp'), may hold values from -8 to 8
- key_weight: bfloat16 [512, 2048], P(None, 'tp'), may hold values from -0.25 to 0.25
- value_weight: bfloat16 [512, 2048], P(None, 'tp'), may hold values from -0.25 to 0.25
- head_output: bfloat16 [16384, 2048], P('sp', 'tp'), may hold values from -2 to 2
- output_grad: bfloat16 [16384, 2048], P('sp', 'tp'), may hold values from -128 to 128
- row_logsum: float32 [16, 16384], P('tp', 'sp'), may hold values from 3 to 16, as said below
Outputs:
- grad_query_main: float32 [16384, 2048], P('sp', 'tp')
- grad_query_rotary: float32 [16384, 1024], P('sp', 'tp')
- grad_latent: float32 [16384, 512], P('sp')
- grad_key_rotary: float32 [16384, 64], P('sp')
- grad_key_weight: float32 [512, 2048], P('sp', 'tp')
Inputs may be any that keep to these rules, and one draw needn't show every extreme that they name: With p the place of token i in its sequence and q = i % 128, row_logsum[h, i] minus the logarithm of (p + 1 + 54 (q + 1)) lies between -0.3 and 1.5.
All inputs are finite; a program needn't handle non-finite values.
Results may differ from a plain program's by a relative error of at most 0.003.
The roundings to bfloat16 on the way count: a program that leaves them out, or rounds other values in their place, can miss the bound.
Values may be sent and summed in bfloat16 or wider, within the bound.
No kernel may reach another device: no remote copies, remote signals or barrier semaphores. Data moves between devices by JAX's collectives and lax.ppermute only.
A program may use at most 64 MiB of HBM per device.

v0:
```python
import jax
import jax.numpy as jnp
from jax import lax
from jax.sharding import Mesh
from jax.sharding import PartitionSpec as P

SEQ_DEVICES = 32
SP = ("sp_0", "sp_1", "sp_2")


def shifted(shard, axis, by):
    peers = lax.axis_size(axis)
    pairs = [(i, i + by) for i in range(peers) if 0 <= i + by < peers]
    return lax.ppermute(shard, axis, pairs)


def from_behind(block, axis, distance):
    devices = range(lax.axis_size(axis))
    route = [((i - distance) % len(devices), i) for i in devices]
    return lax.ppermute(block, axis, route)


def from_everyone(shard, axis):
    peers = lax.axis_size(axis)
    return lax.all_to_all(
        jnp.broadcast_to(shard[None], (peers, *shard.shape)), axis, 0, 0, tiled=True
    )


def of_everyone(shard, axis):
    return from_everyone(shard, axis).sum(axis=0)


def in_one(arrays, axis):
    ends = [0]
    for a in arrays:
        ends.append(ends[-1] + a.size)
    so_far = of_everyone(jnp.concatenate([a.ravel() for a in arrays]), axis)
    return tuple((so_far[b:e].reshape(a.shape) for a, b, e in zip(arrays, ends, ends[1:])))


def sum_in_order(tiles, axes, turns):
    inside = tiles.shape[1:]
    tiles = tiles.reshape(*(lax.axis_size(a) for a in axes), *inside)
    tiles = jnp.moveaxis(tiles, turns, range(len(axes))).reshape(-1, *inside)
    for k in turns:
        tiles = lax.psum_scatter(tiles, axes[k], scatter_dimension=0, tiled=True)
    return tiles[0]


def split_up(shard, dim, peers):
    shape = shard.shape
    tiles = shard.reshape(*shape[:dim], peers, shape[dim] // peers, *shape[dim + 1 :])
    return jnp.moveaxis(tiles, dim, 0)


def summed_rows(shard, axes, turns, dim):
    peers = lax.axis_size(axes)
    return sum_in_order(split_up(shard, dim, peers), axes, turns)


def per_device(
    query_main,
    query_rotary,
    latent,
    key_rotary,
    key_weight,
    value_weight,
    head_output,
    output_grad,
    row_logsum,
):
    devices = lax.axis_size(SP)
    my_index = lax.axis_index(SP)
    group_span = min(SEQ_DEVICES, devices)
    lead_span = group_span // 4
    own_sequence = (my_index + lead_span) // group_span
    heads_here, tok_rows = row_logsum.shape
    lat_width = latent.shape[1]
    rot_width = key_rotary.shape[1]
    main_width = key_weight.shape[1] // heads_here
    value_width = value_weight.shape[1] // heads_here
    factor = (main_width + rot_width) ** (-0.5)
    main_query = query_main.reshape(tok_rows, heads_here, main_width)
    rot_query = query_rotary.reshape(tok_rows, heads_here, rot_width)
    key_proj = key_weight.reshape(lat_width, heads_here, main_width)
    value_proj = value_weight.reshape(lat_width, heads_here, value_width)
    grad_heads = output_grad.reshape(tok_rows, heads_here, value_width)
    query_latent = jnp.einsum(
        "thd,lhd->thl", main_query, key_proj, preferred_element_type=jnp.float32
    ).astype(jnp.bfloat16)
    grad_rows = jnp.einsum(
        "thd,lhd->thl", grad_heads, value_proj, preferred_element_type=jnp.float32
    ).astype(jnp.bfloat16)
    row_terms = jnp.sum(
        head_output.reshape(tok_rows, heads_here, value_width).astype(jnp.float32)
        * grad_heads.astype(jnp.float32),
        axis=2,
    )
    row_logs = row_logsum.T
    query_place = my_index * tok_rows + jnp.arange(tok_rows)

    def attend_block(state, key_block, grad_block, block_index, first_row):
        mixed_sum, rot_sum = state
        lat_block, rot_block = key_block
        acc_lat, acc_rot = grad_block
        key_place = block_index * tok_rows + first_row + jnp.arange(lat_block.shape[0])
        seen = key_place[None, :] <= query_place[:, None]
        scores = jnp.einsum(
            "thl,kl->thk", query_latent, lat_block, preferred_element_type=jnp.float32
        )
        scores = scores + jnp.einsum(
            "thr,kr->thk", rot_query, rot_block, preferred_element_type=jnp.float32
        )
        weights = jnp.where(seen[:, None, :], jnp.exp(factor * scores - row_logs[:, :, None]), 0.0)
        slopes = jnp.einsum("thl,kl->thk", grad_rows, lat_block, preferred_element_type=jnp.float32)
        dscores = weights * (slopes - row_terms[:, :, None])
        weights_low = weights.astype(jnp.bfloat16)
        dscores_low = dscores.astype(jnp.bfloat16)
        mixed_sum = mixed_sum + jnp.einsum(
            "thk,kl->thl", dscores_low, lat_block, preferred_element_type=jnp.float32
        )
        rot_sum = rot_sum + jnp.einsum(
            "thk,kr->thr", dscores_low, rot_block, preferred_element_type=jnp.float32
        )
        part_lat = factor * jnp.einsum(
            "thk,thl->kl", dscores_low, query_latent, preferred_element_type=jnp.float32
        )
        part_lat = part_lat + jnp.einsum(
            "thk,thl->kl", weights_low, grad_rows, preferred_element_type=jnp.float32
        )
        part_rot = factor * jnp.einsum(
            "thk,thr->kr", dscores_low, rot_query, preferred_element_type=jnp.float32
        )
        return ((mixed_sum, rot_sum), (acc_lat + part_lat, acc_rot + part_rot))

    def visit_block(state, key_block, grad_block, block_index, first_row):
        useful = ((block_index + lead_span) // group_span == own_sequence) & (
            block_index <= my_index
        )

        def work(operand):
            return attend_block(operand[0], key_block, operand[1], block_index, first_row)

        def skip(operand):
            return operand

        return lax.cond(useful, work, skip, (state, grad_block))

    zero_state = (
        jnp.zeros((tok_rows, heads_here, lat_width), jnp.float32),
        jnp.zeros((tok_rows, heads_here, rot_width), jnp.float32),
    )
    zero_grads = (
        jnp.zeros((tok_rows, lat_width), jnp.float32),
        jnp.zeros((tok_rows, rot_width), jnp.float32),
    )

    def forward_step(step, carry):
        state, key_block, grad_block = carry
        state, grad_block = visit_block(
            state, key_block, grad_block, (my_index - step) % devices, 0
        )
        key_block = shifted((key_block[0], key_block[1]), SP, 1)
        grad_block = from_behind((grad_block[0], grad_block[1]), SP, 1)
        return (state, key_block, grad_block)

    state, key_block, grad_block = lax.fori_loop(
        0, group_span - 1, forward_step, (zero_state, (latent, key_rotary), zero_grads)
    )
    state, grad_block = visit_block(
        state, key_block, grad_block, (my_index + 1 - group_span) % devices, 0
    )
    lat_grad, rot_grad = from_behind((grad_block[0], grad_block[1]), SP, 1 - group_span)
    lat_grad, rot_grad = in_one((lat_grad, rot_grad), "tp")
    mixed_sum, rot_sum = state
    mixed_low = mixed_sum.astype(jnp.bfloat16)
    grad_main = factor * jnp.einsum(
        "thl,lhd->thd", mixed_low, key_proj, preferred_element_type=jnp.float32
    )
    term = jnp.einsum("thl,thd->lhd", mixed_low, main_query, preferred_element_type=jnp.float32)
    grad_weight = summed_rows(
        factor * term.reshape(lat_width // devices * lax.axis_size(SP), heads_here * main_width),
        SP,
        (2, 0, 1),
        0,
    )
    return (
        grad_main.reshape(tok_rows, heads_here * main_width),
        (factor * rot_sum).reshape(tok_rows, heads_here * rot_width),
        lat_grad,
        rot_grad,
        grad_weight,
    )


def solution(mesh):
    finer = Mesh(mesh.devices.reshape(16, 4, 2, mesh.shape["tp"]), ("sp_0", "sp_1", "sp_2", "tp"))
    return jax.shard_map(
        per_device,
        mesh=finer,
        in_specs=(
            P(SP, "tp"),
            P(SP, "tp"),
            P(SP, None),
            P(SP, None),
            P(None, "tp"),
            P(None, "tp"),
            P(SP, "tp"),
            P(SP, "tp"),
            P("tp", SP),
        ),
        out_specs=(P(SP, "tp"), P(SP, "tp"), P(SP, None), P(SP, None), P(SP, "tp")),
        check_vma=False,
    )
```

profile of v0, /device:TPU:8, one launch (start us, length us, event | category | flops | bytes accessed | tf_op | source)
XLA Modules:
  0.0 737.1 jit_solution(15190983055127998566)
XLA Ops:
  12.4 477.9 %while.26 = (s32[]{:T(128)}, f32[128,4,512]{2,0,1:T(8,128)S(1)}, f32[128,4,64]{0,2,1:T(8,128)}, bf16[128,512]{1,0:T(8,128)(2,1)S(1)}, bf16[128,64]{0,1:T(8,128)(...) while((s32[]{:T(128)}, f32[128,4,512]{2,0,1:T(8,128)S(1)}, ...), condition=%wide.region_4.5_spmd.clone, body=%wide.region_1.4_spmd.clone.sunk | while | flops 361759008 | bytes 10788718 | solution.py:168
  12.5 3.7 conditional.5
  18.1 3.5 collective-permute-start
  23.6 3.5 collective-permute-start.1
  27.1 7.1 collective-permute-done.3
  43.0 4.0 collective-permute-done.3
  49.9 3.9 collective-permute-start
  55.8 5.3 collective-permute-start.1
  68.4 5.6 collective-permute-start.3
  74.0 3.9 collective-permute-start.1
  81.1 4.0 collective-permute-start
  87.1 7.6 %collective-permute-start.1 = (bf16[128,64]{0,1:T(8,128)(2,1)S(1)}, bf16[128,64]{0,1:T(8,128)(2,1)S(1)}, u32[]{:S(2)}, u32[]{:S(2)}) collective-permute-start(bf16[128,64]{0,1:T(8,128)(2,1)S(1)} %copy.198), channel_id=1, source_target_pairs={{0,4},{4,8},{8,12},{12,16},{16,20},{20,24},{24,28},{28,32},{32,36}... | collective-permute-start | bytes 49160 | tf_op jit(solution)/shard_map/while/body/eval_jaxpr/ppermute | solution.py:14
  97.9 4.0 collective-permute-start
  103.8 3.9 collective-permute-start.1
  111.5 3.2 collective-permute-start.2
  114.7 4.2 collective-permute-start
  120.8 3.9 collective-permute-start.1
  130.4 4.9 collective-permute-start
  137.5 3.9 collective-permute-start.1
  148.7 3.4 collective-permute-start.3
  152.0 6.0 collective-permute-start.1
  161.2 4.2 collective-permute-start
  167.3 7.4 %collective-permute-start.1 = (bf16[128,64]{0,1:T(8,128)(2,1)S(1)}, bf16[128,64]{0,1:T(8,128)(2,1)S(1)}, u32[]{:S(2)}, u32[]{:S(2)}) collective-permute-start(bf16[128,64]{0,1:T(8,128)(2,1)S(1)} %copy.198), channel_id=1, source_target_pairs={{0,4},{4,8},{8,12},{12,16},{16,20},{20,24},{24,28},{28,32},{32,36}... | collective-permute-start | bytes 49160 | tf_op jit(solution)/shard_map/while/body/eval_jaxpr/ppermute | solution.py:14
  178.0 4.2 collective-permute-start
  184.1 4.0 collective-permute-start.1
  199.0 6.0 collective-permute-start.1
  208.3 5.2 collective-permute-start
  215.7 6.0 collective-permute-start.1
  225.1 4.1 collective-permute-start
  229.1 3.2 collective-permute-start.3
  232.3 6.3 collective-permute-start.1
  241.8 4.2 collective-permute-start
  247.9 6.0 collective-permute-start.1
  257.5 3.7 collective-permute-start
  263.5 6.0 collective-permute-start.1
  273.8 4.2 collective-permute-start
  280.2 6.0 collective-permute-start.1
  289.5 5.0 collective-permute-start
  296.8 6.3 collective-permute-start.1
  306.3 4.2 collective-permute-start
  312.4 5.3 collective-permute-start.1
  327.0 7.1 collective-permute-start.1
  337.4 4.2 collective-permute-start
  343.8 6.0 collective-permute-start.1
  353.1 4.1 collective-permute-start
  359.1 3.9 collective-permute-start.1
  372.1 3.9 collective-permute-start.1
  385.2 4.9 collective-permute-start.1
  399.4 3.9 collective-permute-start.1
  412.5 3.9 collective-permute-start.1
  425.6 3.9 collective-permute-start.1
  438.6 4.4 collective-permute-start.1
  452.6 6.0 collective-permute-start.1
  462.0 4.1 collective-permute-start
  468.0 5.5 collective-permute-start.1
  477.6 3.2 collective-permute-start
  482.7 4.4 collective-permute-start.1
  490.3 29.5 %collective-permute-start.4 = (f32[128,512]{1,0:T(8,128)S(1)}, f32[128,512]{1,0:T(8,128)S(1)}, u32[]{:S(2)}, u32[]{:S(2)}) collective-permute-start(f32[128,512]{1,0:T(8,128)S(1)} %get-tuple-element.740), channel_id=1, source_target_pairs={{124,0},{128,4},{132,8},{136,12},{140,16},{144,20},{148,24},{152,2... | collective-permute-start | bytes 786440 | tf_op jit(solution)/shard_map/ppermute | solution.py:20
  519.9 7.0 collective-permute-start.5
  532.8 9.7 %collective-permute-done.5 = f32[128,64]{0,1:T(8,128)S(1)} collective-permute-done((f32[128,64]{0,1:T(8,128)S(1)}, f32[128,64]{0,1:T(8,128)S(1)}, u32[]{:S(2)}, u32[]{:S(2)}) %collective-permute-start.5) | collective-permute-done | bytes 32800 | tf_op jit(solution)/shard_map/ppermute | solution.py:20
  544.4 4.9 all-to-all-start
  551.3 18.9 %all-reduce.6.cloned.1.call-done = f32[128,4,512]{2,1,0:T(4,128)} async-done(((f32[128,4,512]{2,1,0:T(4,128)}), f32[128,4,512]{2,1,0:T(4,128)}) %all-reduce.6.cloned.1.call-update) | async-done | bytes 1048592
  580.8 130.5 %all-reduce.8.cloned.1.call-done = f32[64,4,512]{2,1,0:T(4,128)} async-done(((f32[64,4,512]{2,1,0:T(4,128)}), f32[64,4,512]{2,1,0:T(4,128)}) %all-reduce.8.cloned.1.call-update) | async-done | bytes 524304
  712.1 17.0 %all-reduce.2 = f32[4,4,512]{2,1,0:T(4,128)S(1)} all-reduce(f32[4,4,512]{2,1,0:T(4,128)S(1)} %constant_dynamic-slice_fusion), channel_id=4, replica_groups=mesh['sp_0'=16,'sp_1'=4,'sp_2'=2,'tp'=4] {'sp_1'}, use_global_device_ids=true, to_apply=%region_10.11.clone | all-reduce | flops 8192 | bytes 65536
  (461 shorter events, 238.2 us)
Async XLA Ops:
  7.2 563.0 %all-reduce.6.cloned.1.call-start = ((), (), s32[]{:S(2)}) async-start(), calls=%async_computation.1 | async-start | bytes 2097152
  16.2 18.7 %collective-permute-start.2 = (f32[128,512]{1,0:T(8,128)S(1)}, f32[128,512]{1,0:T(8,128)S(1)}, u32[]{:S(2)}, u32[]{:S(2)}) collective-permute-start(f32[128,512]{1,0:T(8,128)S(1)} %get-tuple-element.872), channel_id=1, source_target_pairs={{508,0},{0,4},{4,8},{8,12},{12,16},{16,20},{20,24},{24,28},{28,32}... | collective-permute-start | bytes 786440 | tf_op jit(solution)/shard_map/while/body/eval_jaxpr/ppermute | solution.py:20
  18.1 16.9 %collective-permute-start = (bf16[128,512]{1,0:T(8,128)(2,1)S(1)}, bf16[128,512]{1,0:T(8,128)(2,1)S(1)}, u32[]{:S(2)}, u32[]{:S(2)}) collective-permute-start(bf16[128,512]{1,0:T(8,128)(2,1)S(1)} %copy.197), channel_id=1, source_target_pairs={{0,4},{4,8},{8,12},{12,16},{16,20},{20,24},{24,28},{28,32},{32,36}... | collective-permute-start | bytes 393224 | tf_op jit(solution)/shard_map/while/body/eval_jaxpr/ppermute | solution.py:14
  21.6 12.5 %collective-permute-start.3 = (f32[128,64]{0,1:T(8,128)S(1)}, f32[128,64]{0,1:T(8,128)}, u32[]{:S(2)}, u32[]{:S(2)}) collective-permute-start(f32[128,64]{0,1:T(8,128)S(1)} %get-tuple-element.873), channel_id=1, source_target_pairs={{508,0},{0,4},{4,8},{8,12},{12,16},{16,20},{20,24},{24,28},{28,32}... | collective-permute-start | bytes 98312 | tf_op jit(solution)/shard_map/while/body/eval_jaxpr/ppermute | solution.py:20
  23.6 11.4 %collective-permute-start.1 = (bf16[128,64]{0,1:T(8,128)(2,1)S(1)}, bf16[128,64]{0,1:T(8,128)(2,1)S(1)}, u32[]{:S(2)}, u32[]{:S(2)}) collective-permute-start(bf16[128,64]{0,1:T(8,128)(2,1)S(1)} %copy.198), channel_id=1, source_target_pairs={{0,4},{4,8},{8,12},{12,16},{16,20},{20,24},{24,28},{28,32},{32,36}... | collective-permute-start | bytes 49160 | tf_op jit(solution)/shard_map/while/body/eval_jaxpr/ppermute | solution.py:14
  35.1 12.7 %collective-permute-start.2 = (f32[128,512]{1,0:T(8,128)S(1)}, f32[128,512]{1,0:T(8,128)S(1)}, u32[]{:S(2)}, u32[]{:S(2)}) collective-permute-start(f32[128,512]{1,0:T(8,128)S(1)} %get-tuple-element.872), channel_id=1, source_target_pairs={{508,0},{0,4},{4,8},{8,12},{12,16},{16,20},{20,24},{24,28},{28,32}... | collective-permute-start | bytes 786440 | tf_op jit(solution)/shard_map/while/body/eval_jaxpr/ppermute | solution.py:20
  48.0 15.3 %collective-permute-start.2 = (f32[128,512]{1,0:T(8,128)S(1)}, f32[128,512]{1,0:T(8,128)S(1)}, u32[]{:S(2)}, u32[]{:S(2)}) collective-permute-start(f32[128,512]{1,0:T(8,128)S(1)} %get-tuple-element.872), channel_id=1, source_target_pairs={{508,0},{0,4},{4,8},{8,12},{12,16},{16,20},{20,24},{24,28},{28,32}... | collective-permute-start | bytes 786440 | tf_op jit(solution)/shard_map/while/body/eval_jaxpr/ppermute | solution.py:20
  49.9 13.4 %collective-permute-start = (bf16[128,512]{1,0:T(8,128)(2,1)S(1)}, bf16[128,512]{1,0:T(8,128)(2,1)S(1)}, u32[]{:S(2)}, u32[]{:S(2)}) collective-permute-start(bf16[128,512]{1,0:T(8,128)(2,1)S(1)} %copy.197), channel_id=1, source_target_pairs={{0,4},{4,8},{8,12},{12,16},{16,20},{20,24},{24,28},{28,32},{32,36}... | collective-permute-start | bytes 393224 | tf_op jit(solution)/shard_map/while/body/eval_jaxpr/ppermute | solution.py:14
  63.4 15.3 %collective-permute-start.2 = (f32[128,512]{1,0:T(8,128)S(1)}, f32[128,512]{1,0:T(8,128)S(1)}, u32[]{:S(2)}, u32[]{:S(2)}) collective-permute-start(f32[128,512]{1,0:T(8,128)S(1)} %get-tuple-element.872), channel_id=1, source_target_pairs={{508,0},{0,4},{4,8},{8,12},{12,16},{16,20},{20,24},{24,28},{28,32}... | collective-permute-start | bytes 786440 | tf_op jit(solution)/shard_map/while/body/eval_jaxpr/ppermute | solution.py:20
  65.4 13.4 %collective-permute-start = (bf16[128,512]{1,0:T(8,128)(2,1)S(1)}, bf16[128,512]{1,0:T(8,128)(2,1)S(1)}, u32[]{:S(2)}, u32[]{:S(2)}) collective-permute-start(bf16[128,512]{1,0:T(8,128)(2,1)S(1)} %copy.197), channel_id=1, source_target_pairs={{0,4},{4,8},{8,12},{12,16},{16,20},{20,24},{24,28},{28,32},{32,36}... | collective-permute-start | bytes 393224 | tf_op jit(solution)/shard_map/while/body/eval_jaxpr/ppermute | solution.py:14
  78.9 16.6 %collective-permute-start.2 = (f32[128,512]{1,0:T(8,128)S(1)}, f32[128,512]{1,0:T(8,128)S(1)}, u32[]{:S(2)}, u32[]{:S(2)}) collective-permute-start(f32[128,512]{1,0:T(8,128)S(1)} %get-tuple-element.872), channel_id=1, source_target_pairs={{508,0},{0,4},{4,8},{8,12},{12,16},{16,20},{20,24},{24,28},{28,32}... | collective-permute-start | bytes 786440 | tf_op jit(solution)/shard_map/while/body/eval_jaxpr/ppermute | solution.py:20
  81.1 14.4 %collective-permute-start = (bf16[128,512]{1,0:T(8,128)(2,1)S(1)}, bf16[128,512]{1,0:T(8,128)(2,1)S(1)}, u32[]{:S(2)}, u32[]{:S(2)}) collective-permute-start(bf16[128,512]{1,0:T(8,128)(2,1)S(1)} %copy.197), channel_id=1, source_target_pairs={{0,4},{4,8},{8,12},{12,16},{16,20},{20,24},{24,28},{28,32},{32,36}... | collective-permute-start | bytes 393224 | tf_op jit(solution)/shard_map/while/body/eval_jaxpr/ppermute | solution.py:14
  95.6 15.7 %collective-permute-start.2 = (f32[128,512]{1,0:T(8,128)S(1)}, f32[128,512]{1,0:T(8,128)S(1)}, u32[]{:S(2)}, u32[]{:S(2)}) collective-permute-start(f32[128,512]{1,0:T(8,128)S(1)} %get-tuple-element.872), channel_id=1, source_target_pairs={{508,0},{0,4},{4,8},{8,12},{12,16},{16,20},{20,24},{24,28},{28,32}... | collective-permute-start | bytes 786440 | tf_op jit(solution)/shard_map/while/body/eval_jaxpr/ppermute | solution.py:20
  97.9 13.5 %collective-permute-start = (bf16[128,512]{1,0:T(8,128)(2,1)S(1)}, bf16[128,512]{1,0:T(8,128)(2,1)S(1)}, u32[]{:S(2)}, u32[]{:S(2)}) collective-permute-start(bf16[128,512]{1,0:T(8,128)(2,1)S(1)} %copy.197), channel_id=1, source_target_pairs={{0,4},{4,8},{8,12},{12,16},{16,20},{20,24},{24,28},{28,32},{32,36}... | collective-permute-start | bytes 393224 | tf_op jit(solution)/shard_map/while/body/eval_jaxpr/ppermute | solution.py:14
  111.5 16.8 %collective-permute-start.2 = (f32[128,512]{1,0:T(8,128)S(1)}, f32[128,512]{1,0:T(8,128)S(1)}, u32[]{:S(2)}, u32[]{:S(2)}) collective-permute-start(f32[128,512]{1,0:T(8,128)S(1)} %get-tuple-element.872), channel_id=1, source_target_pairs={{508,0},{0,4},{4,8},{8,12},{12,16},{16,20},{20,24},{24,28},{28,32}... | collective-permute-start | bytes 786440 | tf_op jit(solution)/shard_map/while/body/eval_jaxpr/ppermute | solution.py:20
  114.7 13.7 %collective-permute-start = (bf16[128,512]{1,0:T(8,128)(2,1)S(1)}, bf16[128,512]{1,0:T(8,128)(2,1)S(1)}, u32[]{:S(2)}, u32[]{:S(2)}) collective-permute-start(bf16[128,512]{1,0:T(8,128)(2,1)S(1)} %copy.197), channel_id=1, source_target_pairs={{0,4},{4,8},{8,12},{12,16},{16,20},{20,24},{24,28},{28,32},{32,36}... | collective-permute-start | bytes 393224 | tf_op jit(solution)/shard_map/while/body/eval_jaxpr/ppermute | solution.py:14
  128.5 16.3 %collective-permute-start.2 = (f32[128,512]{1,0:T(8,128)S(1)}, f32[128,512]{1,0:T(8,128)S(1)}, u32[]{:S(2)}, u32[]{:S(2)}) collective-permute-start(f32[128,512]{1,0:T(8,128)S(1)} %get-tuple-element.872), channel_id=1, source_target_pairs={{508,0},{0,4},{4,8},{8,12},{12,16},{16,20},{20,24},{24,28},{28,32}... | collective-permute-start | bytes 786440 | tf_op jit(solution)/shard_map/while/body/eval_jaxpr/ppermute | solution.py:20
  130.4 14.4 %collective-permute-start = (bf16[128,512]{1,0:T(8,128)(2,1)S(1)}, bf16[128,512]{1,0:T(8,128)(2,1)S(1)}, u32[]{:S(2)}, u32[]{:S(2)}) collective-permute-start(bf16[128,512]{1,0:T(8,128)(2,1)S(1)} %copy.197), channel_id=1, source_target_pairs={{0,4},{4,8},{8,12},{12,16},{16,20},{20,24},{24,28},{28,32},{32,36}... | collective-permute-start | bytes 393224 | tf_op jit(solution)/shard_map/while/body/eval_jaxpr/ppermute | solution.py:14
  144.9 13.9 %collective-permute-start.2 = (f32[128,512]{1,0:T(8,128)S(1)}, f32[128,512]{1,0:T(8,128)S(1)}, u32[]{:S(2)}, u32[]{:S(2)}) collective-permute-start(f32[128,512]{1,0:T(8,128)S(1)} %get-tuple-element.872), channel_id=1, source_target_pairs={{508,0},{0,4},{4,8},{8,12},{12,16},{16,20},{20,24},{24,28},{28,32}... | collective-permute-start | bytes 786440 | tf_op jit(solution)/shard_map/while/body/eval_jaxpr/ppermute | solution.py:20
  146.9 12.0 %collective-permute-start = (bf16[128,512]{1,0:T(8,128)(2,1)S(1)}, bf16[128,512]{1,0:T(8,128)(2,1)S(1)}, u32[]{:S(2)}, u32[]{:S(2)}) collective-permute-start(bf16[128,512]{1,0:T(8,128)(2,1)S(1)} %copy.197), channel_id=1, source_target_pairs={{0,4},{4,8},{8,12},{12,16},{16,20},{20,24},{24,28},{28,32},{32,36}... | collective-permute-start | bytes 393224 | tf_op jit(solution)/shard_map/while/body/eval_jaxpr/ppermute | solution.py:14
  159.0 16.6 %collective-permute-start.2 = (f32[128,512]{1,0:T(8,128)S(1)}, f32[128,512]{1,0:T(8,128)S(1)}, u32[]{:S(2)}, u32[]{:S(2)}) collective-permute-start(f32[128,512]{1,0:T(8,128)S(1)} %get-tuple-element.872), channel_id=1, source_target_pairs={{508,0},{0,4},{4,8},{8,12},{12,16},{16,20},{20,24},{24,28},{28,32}... | collective-permute-start | bytes 786440 | tf_op jit(solution)/shard_map/while/body/eval_jaxpr/ppermute | solution.py:20
  161.2 14.4 %collective-permute-start = (bf16[128,512]{1,0:T(8,128)(2,1)S(1)}, bf16[128,512]{1,0:T(8,128)(2,1)S(1)}, u32[]{:S(2)}, u32[]{:S(2)}) collective-permute-start(bf16[128,512]{1,0:T(8,128)(2,1)S(1)} %copy.197), channel_id=1, source_target_pairs={{0,4},{4,8},{8,12},{12,16},{16,20},{20,24},{24,28},{28,32},{32,36}... | collective-permute-start | bytes 393224 | tf_op jit(solution)/shard_map/while/body/eval_jaxpr/ppermute | solution.py:14
  175.7 15.8 %collective-permute-start.2 = (f32[128,512]{1,0:T(8,128)S(1)}, f32[128,512]{1,0:T(8,128)S(1)}, u32[]{:S(2)}, u32[]{:S(2)}) collective-permute-start(f32[128,512]{1,0:T(8,128)S(1)} %get-tuple-element.872), channel_id=1, source_target_pairs={{508,0},{0,4},{4,8},{8,12},{12,16},{16,20},{20,24},{24,28},{28,32}... | collective-permute-start | bytes 786440 | tf_op jit(solution)/shard_map/while/body/eval_jaxpr/ppermute | solution.py:20
  178.0 13.7 %collective-permute-start = (bf16[128,512]{1,0:T(8,128)(2,1)S(1)}, bf16[128,512]{1,0:T(8,128)(2,1)S(1)}, u32[]{:S(2)}, u32[]{:S(2)}) collective-permute-start(bf16[128,512]{1,0:T(8,128)(2,1)S(1)} %copy.197), channel_id=1, source_target_pairs={{0,4},{4,8},{8,12},{12,16},{16,20},{20,24},{24,28},{28,32},{32,36}... | collective-permute-start | bytes 393224 | tf_op jit(solution)/shard_map/while/body/eval_jaxpr/ppermute | solution.py:14
  191.8 14.4 %collective-permute-start.2 = (f32[128,512]{1,0:T(8,128)S(1)}, f32[128,512]{1,0:T(8,128)S(1)}, u32[]{:S(2)}, u32[]{:S(2)}) collective-permute-start(f32[128,512]{1,0:T(8,128)S(1)} %get-tuple-element.872), channel_id=1, source_target_pairs={{508,0},{0,4},{4,8},{8,12},{12,16},{16,20},{20,24},{24,28},{28,32}... | collective-permute-start | bytes 786440 | tf_op jit(solution)/shard_map/while/body/eval_jaxpr/ppermute | solution.py:20
  193.7 12.5 %collective-permute-start = (bf16[128,512]{1,0:T(8,128)(2,1)S(1)}, bf16[128,512]{1,0:T(8,128)(2,1)S(1)}, u32[]{:S(2)}, u32[]{:S(2)}) collective-permute-start(bf16[128,512]{1,0:T(8,128)(2,1)S(1)} %copy.197), channel_id=1, source_target_pairs={{0,4},{4,8},{8,12},{12,16},{16,20},{20,24},{24,28},{28,32},{32,36}... | collective-permute-start | bytes 393224 | tf_op jit(solution)/shard_map/while/body/eval_jaxpr/ppermute | solution.py:14
  206.4 16.6 %collective-permute-start.2 = (f32[128,512]{1,0:T(8,128)S(1)}, f32[128,512]{1,0:T(8,128)S(1)}, u32[]{:S(2)}, u32[]{:S(2)}) collective-permute-start(f32[128,512]{1,0:T(8,128)S(1)} %get-tuple-element.872), channel_id=1, source_target_pairs={{508,0},{0,4},{4,8},{8,12},{12,16},{16,20},{20,24},{24,28},{28,32}... | collective-permute-start | bytes 786440 | tf_op jit(solution)/shard_map/while/body/eval_jaxpr/ppermute | solution.py:20
  208.3 14.7 %collective-permute-start = (bf16[128,512]{1,0:T(8,128)(2,1)S(1)}, bf16[128,512]{1,0:T(8,128)(2,1)S(1)}, u32[]{:S(2)}, u32[]{:S(2)}) collective-permute-start(bf16[128,512]{1,0:T(8,128)(2,1)S(1)} %copy.197), channel_id=1, source_target_pairs={{0,4},{4,8},{8,12},{12,16},{16,20},{20,24},{24,28},{28,32},{32,36}... | collective-permute-start | bytes 393224 | tf_op jit(solution)/shard_map/while/body/eval_jaxpr/ppermute | solution.py:14
  223.1 16.2 %collective-permute-start.2 = (f32[128,512]{1,0:T(8,128)S(1)}, f32[128,512]{1,0:T(8,128)S(1)}, u32[]{:S(2)}, u32[]{:S(2)}) collective-permute-start(f32[128,512]{1,0:T(8,128)S(1)} %get-tuple-element.872), channel_id=1, source_target_pairs={{508,0},{0,4},{4,8},{8,12},{12,16},{16,20},{20,24},{24,28},{28,32}... | collective-permute-start | bytes 786440 | tf_op jit(solution)/shard_map/while/body/eval_jaxpr/ppermute | solution.py:20
  225.1 14.4 %collective-permute-start = (bf16[128,512]{1,0:T(8,128)(2,1)S(1)}, bf16[128,512]{1,0:T(8,128)(2,1)S(1)}, u32[]{:S(2)}, u32[]{:S(2)}) collective-permute-start(bf16[128,512]{1,0:T(8,128)(2,1)S(1)} %copy.197), channel_id=1, source_target_pairs={{0,4},{4,8},{8,12},{12,16},{16,20},{20,24},{24,28},{28,32},{32,36}... | collective-permute-start | bytes 393224 | tf_op jit(solution)/shard_map/while/body/eval_jaxpr/ppermute | solution.py:14
  239.6 15.8 %collective-permute-start.2 = (f32[128,512]{1,0:T(8,128)S(1)}, f32[128,512]{1,0:T(8,128)S(1)}, u32[]{:S(2)}, u32[]{:S(2)}) collective-permute-start(f32[128,512]{1,0:T(8,128)S(1)} %get-tuple-element.872), channel_id=1, source_target_pairs={{508,0},{0,4},{4,8},{8,12},{12,16},{16,20},{20,24},{24,28},{28,32}... | collective-permute-start | bytes 786440 | tf_op jit(solution)/shard_map/while/body/eval_jaxpr/ppermute | solution.py:20
  241.8 13.7 %collective-permute-start = (bf16[128,512]{1,0:T(8,128)(2,1)S(1)}, bf16[128,512]{1,0:T(8,128)(2,1)S(1)}, u32[]{:S(2)}, u32[]{:S(2)}) collective-permute-start(bf16[128,512]{1,0:T(8,128)(2,1)S(1)} %copy.197), channel_id=1, source_target_pairs={{0,4},{4,8},{8,12},{12,16},{16,20},{20,24},{24,28},{28,32},{32,36}... | collective-permute-start | bytes 393224 | tf_op jit(solution)/shard_map/while/body/eval_jaxpr/ppermute | solution.py:14
  255.6 15.1 %collective-permute-start.2 = (f32[128,512]{1,0:T(8,128)S(1)}, f32[128,512]{1,0:T(8,128)S(1)}, u32[]{:S(2)}, u32[]{:S(2)}) collective-permute-start(f32[128,512]{1,0:T(8,128)S(1)} %get-tuple-element.872), channel_id=1, source_target_pairs={{508,0},{0,4},{4,8},{8,12},{12,16},{16,20},{20,24},{24,28},{28,32}... | collective-permute-start | bytes 786440 | tf_op jit(solution)/shard_map/while/body/eval_jaxpr/ppermute | solution.py:20
  257.5 13.2 %collective-permute-start = (bf16[128,512]{1,0:T(8,128)(2,1)S(1)}, bf16[128,512]{1,0:T(8,128)(2,1)S(1)}, u32[]{:S(2)}, u32[]{:S(2)}) collective-permute-start(bf16[128,512]{1,0:T(8,128)(2,1)S(1)} %copy.197), channel_id=1, source_target_pairs={{0,4},{4,8},{8,12},{12,16},{16,20},{20,24},{24,28},{28,32},{32,36}... | collective-permute-start | bytes 393224 | tf_op jit(solution)/shard_map/while/body/eval_jaxpr/ppermute | solution.py:14
  270.9 16.6 %collective-permute-start.2 = (f32[128,512]{1,0:T(8,128)S(1)}, f32[128,512]{1,0:T(8,128)S(1)}, u32[]{:S(2)}, u32[]{:S(2)}) collective-permute-start(f32[128,512]{1,0:T(8,128)S(1)} %get-tuple-element.872), channel_id=1, source_target_pairs={{508,0},{0,4},{4,8},{8,12},{12,16},{16,20},{20,24},{24,28},{28,32}... | collective-permute-start | bytes 786440 | tf_op jit(solution)/shard_map/while/body/eval_jaxpr/ppermute | solution.py:20
  273.8 13.7 %collective-permute-start = (bf16[128,512]{1,0:T(8,128)(2,1)S(1)}, bf16[128,512]{1,0:T(8,128)(2,1)S(1)}, u32[]{:S(2)}, u32[]{:S(2)}) collective-permute-start(bf16[128,512]{1,0:T(8,128)(2,1)S(1)} %copy.197), channel_id=1, source_target_pairs={{0,4},{4,8},{8,12},{12,16},{16,20},{20,24},{24,28},{28,32},{32,36}... | collective-permute-start | bytes 393224 | tf_op jit(solution)/shard_map/while/body/eval_jaxpr/ppermute | solution.py:14
  287.6 16.4 %collective-permute-start.2 = (f32[128,512]{1,0:T(8,128)S(1)}, f32[128,512]{1,0:T(8,128)S(1)}, u32[]{:S(2)}, u32[]{:S(2)}) collective-permute-start(f32[128,512]{1,0:T(8,128)S(1)} %get-tuple-element.872), channel_id=1, source_target_pairs={{508,0},{0,4},{4,8},{8,12},{12,16},{16,20},{20,24},{24,28},{28,32}... | collective-permute-start | bytes 786440 | tf_op jit(solution)/shard_map/while/body/eval_jaxpr/ppermute | solution.py:20
  289.5 14.5 %collective-permute-start = (bf16[128,512]{1,0:T(8,128)(2,1)S(1)}, bf16[128,512]{1,0:T(8,128)(2,1)S(1)}, u32[]{:S(2)}, u32[]{:S(2)}) collective-permute-start(bf16[128,512]{1,0:T(8,128)(2,1)S(1)} %copy.197), channel_id=1, source_target_pairs={{0,4},{4,8},{8,12},{12,16},{16,20},{20,24},{24,28},{28,32},{32,36}... | collective-permute-start | bytes 393224 | tf_op jit(solution)/shard_map/while/body/eval_jaxpr/ppermute | solution.py:14
  304.2 15.7 %collective-permute-start.2 = (f32[128,512]{1,0:T(8,128)S(1)}, f32[128,512]{1,0:T(8,128)S(1)}, u32[]{:S(2)}, u32[]{:S(2)}) collective-permute-start(f32[128,512]{1,0:T(8,128)S(1)} %get-tuple-element.872), channel_id=1, source_target_pairs={{508,0},{0,4},{4,8},{8,12},{12,16},{16,20},{20,24},{24,28},{28,32}... | collective-permute-start | bytes 786440 | tf_op jit(solution)/shard_map/while/body/eval_jaxpr/ppermute | solution.py:20
  306.3 13.7 %collective-permute-start = (bf16[128,512]{1,0:T(8,128)(2,1)S(1)}, bf16[128,512]{1,0:T(8,128)(2,1)S(1)}, u32[]{:S(2)}, u32[]{:S(2)}) collective-permute-start(bf16[128,512]{1,0:T(8,128)(2,1)S(1)} %copy.197), channel_id=1, source_target_pairs={{0,4},{4,8},{8,12},{12,16},{16,20},{20,24},{24,28},{28,32},{32,36}... | collective-permute-start | bytes 393224 | tf_op jit(solution)/shard_map/while/body/eval_jaxpr/ppermute | solution.py:14
  320.1 14.9 %collective-permute-start.2 = (f32[128,512]{1,0:T(8,128)S(1)}, f32[128,512]{1,0:T(8,128)S(1)}, u32[]{:S(2)}, u32[]{:S(2)}) collective-permute-start(f32[128,512]{1,0:T(8,128)S(1)} %get-tuple-element.872), channel_id=1, source_target_pairs={{508,0},{0,4},{4,8},{8,12},{12,16},{16,20},{20,24},{24,28},{28,32}... | collective-permute-start | bytes 786440 | tf_op jit(solution)/shard_map/while/body/eval_jaxpr/ppermute | solution.py:20
  322.0 13.0 %collective-permute-start = (bf16[128,512]{1,0:T(8,128)(2,1)S(1)}, bf16[128,512]{1,0:T(8,128)(2,1)S(1)}, u32[]{:S(2)}, u32[]{:S(2)}) collective-permute-start(bf16[128,512]{1,0:T(8,128)(2,1)S(1)} %copy.197), channel_id=1, source_target_pairs={{0,4},{4,8},{8,12},{12,16},{16,20},{20,24},{24,28},{28,32},{32,36}... | collective-permute-start | bytes 393224 | tf_op jit(solution)/shard_map/while/body/eval_jaxpr/ppermute | solution.py:14
  335.1 15.8 %collective-permute-start.2 = (f32[128,512]{1,0:T(8,128)S(1)}, f32[128,512]{1,0:T(8,128)S(1)}, u32[]{:S(2)}, u32[]{:S(2)}) collective-permute-start(f32[128,512]{1,0:T(8,128)S(1)} %get-tuple-element.872), channel_id=1, source_target_pairs={{508,0},{0,4},{4,8},{8,12},{12,16},{16,20},{20,24},{24,28},{28,32}... | collective-permute-start | bytes 786440 | tf_op jit(solution)/shard_map/while/body/eval_jaxpr/ppermute | solution.py:20
  337.4 13.7 %collective-permute-start = (bf16[128,512]{1,0:T(8,128)(2,1)S(1)}, bf16[128,512]{1,0:T(8,128)(2,1)S(1)}, u32[]{:S(2)}, u32[]{:S(2)}) collective-permute-start(bf16[128,512]{1,0:T(8,128)(2,1)S(1)} %copy.197), channel_id=1, source_target_pairs={{0,4},{4,8},{8,12},{12,16},{16,20},{20,24},{24,28},{28,32},{32,36}... | collective-permute-start | bytes 393224 | tf_op jit(solution)/shard_map/while/body/eval_jaxpr/ppermute | solution.py:14
  351.2 15.4 %collective-permute-start.2 = (f32[128,512]{1,0:T(8,128)S(1)}, f32[128,512]{1,0:T(8,128)S(1)}, u32[]{:S(2)}, u32[]{:S(2)}) collective-permute-start(f32[128,512]{1,0:T(8,128)S(1)} %get-tuple-element.872), channel_id=1, source_target_pairs={{508,0},{0,4},{4,8},{8,12},{12,16},{16,20},{20,24},{24,28},{28,32}... | collective-permute-start | bytes 786440 | tf_op jit(solution)/shard_map/while/body/eval_jaxpr/ppermute | solution.py:20
  353.1 13.5 %collective-permute-start = (bf16[128,512]{1,0:T(8,128)(2,1)S(1)}, bf16[128,512]{1,0:T(8,128)(2,1)S(1)}, u32[]{:S(2)}, u32[]{:S(2)}) collective-permute-start(bf16[128,512]{1,0:T(8,128)(2,1)S(1)} %copy.197), channel_id=1, source_target_pairs={{0,4},{4,8},{8,12},{12,16},{16,20},{20,24},{24,28},{28,32},{32,36}... | collective-permute-start | bytes 393224 | tf_op jit(solution)/shard_map/while/body/eval_jaxpr/ppermute | solution.py:14
  366.8 12.9 %collective-permute-start.2 = (f32[128,512]{1,0:T(8,128)S(1)}, f32[128,512]{1,0:T(8,128)S(1)}, u32[]{:S(2)}, u32[]{:S(2)}) collective-permute-start(f32[128,512]{1,0:T(8,128)S(1)} %get-tuple-element.872), channel_id=1, source_target_pairs={{508,0},{0,4},{4,8},{8,12},{12,16},{16,20},{20,24},{24,28},{28,32}... | collective-permute-start | bytes 786440 | tf_op jit(solution)/shard_map/while/body/eval_jaxpr/ppermute | solution.py:20
  379.8 12.9 %collective-permute-start.2 = (f32[128,512]{1,0:T(8,128)S(1)}, f32[128,512]{1,0:T(8,128)S(1)}, u32[]{:S(2)}, u32[]{:S(2)}) collective-permute-start(f32[128,512]{1,0:T(8,128)S(1)} %get-tuple-element.872), channel_id=1, source_target_pairs={{508,0},{0,4},{4,8},{8,12},{12,16},{16,20},{20,24},{24,28},{28,32}... | collective-permute-start | bytes 786440 | tf_op jit(solution)/shard_map/while/body/eval_jaxpr/ppermute | solution.py:20
  392.9 14.1 %collective-permute-start.2 = (f32[128,512]{1,0:T(8,128)S(1)}, f32[128,512]{1,0:T(8,128)S(1)}, u32[]{:S(2)}, u32[]{:S(2)}) collective-permute-start(f32[128,512]{1,0:T(8,128)S(1)} %get-tuple-element.872), channel_id=1, source_target_pairs={{508,0},{0,4},{4,8},{8,12},{12,16},{16,20},{20,24},{24,28},{28,32}... | collective-permute-start | bytes 786440 | tf_op jit(solution)/shard_map/while/body/eval_jaxpr/ppermute | solution.py:20
  394.8 12.2 %collective-permute-start = (bf16[128,512]{1,0:T(8,128)(2,1)S(1)}, bf16[128,512]{1,0:T(8,128)(2,1)S(1)}, u32[]{:S(2)}, u32[]{:S(2)}) collective-permute-start(bf16[128,512]{1,0:T(8,128)(2,1)S(1)} %copy.197), channel_id=1, source_target_pairs={{0,4},{4,8},{8,12},{12,16},{16,20},{20,24},{24,28},{28,32},{32,36}... | collective-permute-start | bytes 393224 | tf_op jit(solution)/shard_map/while/body/eval_jaxpr/ppermute | solution.py:14
  407.1 12.9 %collective-permute-start.2 = (f32[128,512]{1,0:T(8,128)S(1)}, f32[128,512]{1,0:T(8,128)S(1)}, u32[]{:S(2)}, u32[]{:S(2)}) collective-permute-start(f32[128,512]{1,0:T(8,128)S(1)} %get-tuple-element.872), channel_id=1, source_target_pairs={{508,0},{0,4},{4,8},{8,12},{12,16},{16,20},{20,24},{24,28},{28,32}... | collective-permute-start | bytes 786440 | tf_op jit(solution)/shard_map/while/body/eval_jaxpr/ppermute | solution.py:20
  420.2 12.9 %collective-permute-start.2 = (f32[128,512]{1,0:T(8,128)S(1)}, f32[128,512]{1,0:T(8,128)S(1)}, u32[]{:S(2)}, u32[]{:S(2)}) collective-permute-start(f32[128,512]{1,0:T(8,128)S(1)} %get-tuple-element.872), channel_id=1, source_target_pairs={{508,0},{0,4},{4,8},{8,12},{12,16},{16,20},{20,24},{24,28},{28,32}... | collective-permute-start | bytes 786440 | tf_op jit(solution)/shard_map/while/body/eval_jaxpr/ppermute | solution.py:20
  422.1 11.0 %collective-permute-start = (bf16[128,512]{1,0:T(8,128)(2,1)S(1)}, bf16[128,512]{1,0:T(8,128)(2,1)S(1)}, u32[]{:S(2)}, u32[]{:S(2)}) collective-permute-start(bf16[128,512]{1,0:T(8,128)(2,1)S(1)} %copy.197), channel_id=1, source_target_pairs={{0,4},{4,8},{8,12},{12,16},{16,20},{20,24},{24,28},{28,32},{32,36}... | collective-permute-start | bytes 393224 | tf_op jit(solution)/shard_map/while/body/eval_jaxpr/ppermute | solution.py:14
  433.2 12.9 %collective-permute-start.2 = (f32[128,512]{1,0:T(8,128)S(1)}, f32[128,512]{1,0:T(8,128)S(1)}, u32[]{:S(2)}, u32[]{:S(2)}) collective-permute-start(f32[128,512]{1,0:T(8,128)S(1)} %get-tuple-element.872), channel_id=1, source_target_pairs={{508,0},{0,4},{4,8},{8,12},{12,16},{16,20},{20,24},{24,28},{28,32}... | collective-permute-start | bytes 786440 | tf_op jit(solution)/shard_map/while/body/eval_jaxpr/ppermute | solution.py:20
  446.3 13.6 %collective-permute-start.2 = (f32[128,512]{1,0:T(8,128)S(1)}, f32[128,512]{1,0:T(8,128)S(1)}, u32[]{:S(2)}, u32[]{:S(2)}) collective-permute-start(f32[128,512]{1,0:T(8,128)S(1)} %get-tuple-element.872), channel_id=1, source_target_pairs={{508,0},{0,4},{4,8},{8,12},{12,16},{16,20},{20,24},{24,28},{28,32}... | collective-permute-start | bytes 786440 | tf_op jit(solution)/shard_map/while/body/eval_jaxpr/ppermute | solution.py:20
  448.2 11.7 %collective-permute-start = (bf16[128,512]{1,0:T(8,128)(2,1)S(1)}, bf16[128,512]{1,0:T(8,128)(2,1)S(1)}, u32[]{:S(2)}, u32[]{:S(2)}) collective-permute-start(bf16[128,512]{1,0:T(8,128)(2,1)S(1)} %copy.197), channel_id=1, source_target_pairs={{0,4},{4,8},{8,12},{12,16},{16,20},{20,24},{24,28},{28,32},{32,36}... | collective-permute-start | bytes 393224 | tf_op jit(solution)/shard_map/while/body/eval_jaxpr/ppermute | solution.py:14
  460.0 15.4 %collective-permute-start.2 = (f32[128,512]{1,0:T(8,128)S(1)}, f32[128,512]{1,0:T(8,128)S(1)}, u32[]{:S(2)}, u32[]{:S(2)}) collective-permute-start(f32[128,512]{1,0:T(8,128)S(1)} %get-tuple-element.872), channel_id=1, source_target_pairs={{508,0},{0,4},{4,8},{8,12},{12,16},{16,20},{20,24},{24,28},{28,32}... | collective-permute-start | bytes 786440 | tf_op jit(solution)/shard_map/while/body/eval_jaxpr/ppermute | solution.py:20
  462.0 13.5 %collective-permute-start = (bf16[128,512]{1,0:T(8,128)(2,1)S(1)}, bf16[128,512]{1,0:T(8,128)(2,1)S(1)}, u32[]{:S(2)}, u32[]{:S(2)}) collective-permute-start(bf16[128,512]{1,0:T(8,128)(2,1)S(1)} %copy.197), channel_id=1, source_target_pairs={{0,4},{4,8},{8,12},{12,16},{16,20},{20,24},{24,28},{28,32},{32,36}... | collective-permute-start | bytes 393224 | tf_op jit(solution)/shard_map/while/body/eval_jaxpr/ppermute | solution.py:14
  475.6 14.6 %collective-permute-start.2 = (f32[128,512]{1,0:T(8,128)S(1)}, f32[128,512]{1,0:T(8,128)S(1)}, u32[]{:S(2)}, u32[]{:S(2)}) collective-permute-start(f32[128,512]{1,0:T(8,128)S(1)} %get-tuple-element.872), channel_id=1, source_target_pairs={{508,0},{0,4},{4,8},{8,12},{12,16},{16,20},{20,24},{24,28},{28,32}... | collective-permute-start | bytes 786440 | tf_op jit(solution)/shard_map/while/body/eval_jaxpr/ppermute | solution.py:20
  477.6 12.7 %collective-permute-start = (bf16[128,512]{1,0:T(8,128)(2,1)S(1)}, bf16[128,512]{1,0:T(8,128)(2,1)S(1)}, u32[]{:S(2)}, u32[]{:S(2)}) collective-permute-start(bf16[128,512]{1,0:T(8,128)(2,1)S(1)} %copy.197), channel_id=1, source_target_pairs={{0,4},{4,8},{8,12},{12,16},{16,20},{20,24},{24,28},{28,32},{32,36}... | collective-permute-start | bytes 393224 | tf_op jit(solution)/shard_map/while/body/eval_jaxpr/ppermute | solution.py:14
  490.3 52.4 %collective-permute-start.4 = (f32[128,512]{1,0:T(8,128)S(1)}, f32[128,512]{1,0:T(8,128)S(1)}, u32[]{:S(2)}, u32[]{:S(2)}) collective-permute-start(f32[128,512]{1,0:T(8,128)S(1)} %get-tuple-element.740), channel_id=1, source_target_pairs={{124,0},{128,4},{132,8},{136,12},{140,16},{144,20},{148,24},{152,2... | collective-permute-start | bytes 786440 | tf_op jit(solution)/shard_map/ppermute | solution.py:20
  519.9 22.6 %collective-permute-start.5 = (f32[128,64]{0,1:T(8,128)S(1)}, f32[128,64]{0,1:T(8,128)S(1)}, u32[]{:S(2)}, u32[]{:S(2)}) collective-permute-start(f32[128,64]{0,1:T(8,128)S(1)} %get-tuple-element.741), channel_id=1, source_target_pairs={{124,0},{128,4},{132,8},{136,12},{140,16},{144,20},{148,24},{152,2... | collective-permute-start | bytes 98312 | tf_op jit(solution)/shard_map/ppermute | solution.py:20
  544.4 33.7 %all-to-all-start = ((f32[4,1,73728]{2,1,0:T(1,128)}), f32[4,1,73728]{2,1,0:T(1,128)S(1)}, u32[]{:S(2)}, u32[]{:S(2)}) async-start(f32[4,1,73728]{2,1,0:T(1,128)} %broadcast_in_dim.52), calls=%async_computation | async-start | bytes 2359296 | tf_op jit(solution)/shard_map/all_to_all | solution.py:25
  549.3 162.0 %all-reduce.8.cloned.1.call-start = ((), (), s32[]{:S(2)}) async-start(), calls=%async_computation.2 | async-start | bytes 1048576
  (78 other events, 581.2 us)
Sparse Core Ops, SparseCore 0:
  532.9 37.1 all-reduce.5
  572.5 138.7 all-reduce.7
where the time goes:
time: 744 us; the launch traced here: 737 us
  starting transfers between devices  435 us (58%)
  waiting for transfers between devices  210 us (28%)
  local copies, waits for them, and re-layouts  46 us (6%)
  blocking collectives  17 us (2%)
  between operations  15.7 us (2%)
    ppermute x62, starting transfers between devices, shifted(): return lax.ppermute(shard, axis, pairs)  262 us
    ppermute x64, starting transfers between devices, from_behind(): return lax.ppermute(block, axis, route)  168 us
    unnamed x4, waiting for transfers between devices  149 us
    ppermute x64, waiting for transfers between devices, from_behind(): return lax.ppermute(block, axis, route)  59.9 us
    while x124, local copies, waits for them, and re-layouts  24.5 us
    unnamed x1, blocking collectives  17 us
  transfers between devices with their start and end apart: 129, of which 28 were waited for; matrix products, arithmetic and copies ran while one was open for 6% of the time, Pallas kernels for 0%

commit v1 on v0

v1 whole, which is shorter than its diff:
```python
import jax
import jax.numpy as jnp
from jax import lax
from jax.experimental import pallas as pl
from jax.experimental.pallas import tpu as pltpu
from jax.sharding import Mesh
from jax.sharding import PartitionSpec as P

Z, X, C, Y = "sp_0", "sp_1", "sp_2", "tp"
SP = (Z, X, C)
GROUP = 4
bf16 = jnp.bfloat16
f32 = jnp.float32


def shift(block, axis, by):
    peers = lax.axis_size(axis)
    return lax.ppermute(block, axis, [(i, (i + by) % peers) for i in range(peers)])


def exchange(tiles, axis, groups=None):
    return lax.all_to_all(tiles, axis, 0, 0, tiled=True, axis_index_groups=groups)


def dot(a, b, dims):
    return lax.dot_general(a, b, (dims, ((), ())), preferred_element_type=f32)


def pack_kernel(qm, qr, og, ho, logs, lat, rot, qpack, kpack):
    heads, toks = logs.shape
    width = qm.shape[1] // heads
    qpack[:, 0:512] = qm[...]
    qpack[:, 512:768] = qr[...]
    qpack[:, 768:1280] = og[...]
    lane = lax.broadcasted_iota(jnp.int32, (toks, 128), 1)
    extra = jnp.zeros((toks, 128), f32)
    logs_t = logs[...].T
    for h in range(heads):
        cols = slice(h * width, (h + 1) * width)
        term = jnp.sum(ho[:, cols].astype(f32) * og[:, cols].astype(f32), axis=1, keepdims=True)
        for k, value in enumerate((logs_t[:, h : h + 1], term)):
            for part in range(3):
                piece = value.astype(bf16).astype(f32)
                value = value - piece
                extra = jnp.where(lane == (h * 2 + k) * 3 + part, piece, extra)
    qpack[:, 1280:1408] = extra.astype(bf16)
    kpack[:, 0:512] = lat[...]
    kpack[:, 512:576] = rot[...]
    kpack[:, 576:640] = jnp.zeros((toks, 64), bf16)


def pack(qm, qr, og, ho, logs, lat, rot):
    toks = qm.shape[0]
    return pl.pallas_call(
        pack_kernel,
        out_shape=(
            jax.ShapeDtypeStruct((toks, 1408), bf16),
            jax.ShapeDtypeStruct((toks, 640), bf16),
        ),
        name="pack",
    )(qm, qr, og, ho, logs, lat, rot)


def attend_kernel(
    info, q0, q1, q2, q3, k0, k1, k2, k3, kother, wk, wv,
    d0, d1, d2, d3, own, other, wout,
    qcur, kcur, q_s, qt_s, g_s, gt_s, log_s, term_s, acc, ds_acc, w_acc, wt_acc,
):
    heads, toks, width = 4, 128, 128
    factor = 192.0**-0.5
    my_x = info[3]
    my_c = info[4]
    ds_acc[...] = jnp.zeros_like(ds_acc)
    w_acc[...] = jnp.zeros_like(w_acc)
    wt_acc[...] = jnp.zeros_like(wt_acc)
    q_s[:, 576:640] = jnp.zeros((heads * toks, 64), bf16)

    def chunk(g, _):
        for i, ref in enumerate((q0, q1, q2, q3)):

            @pl.when(g == i)
            def _(ref=ref):
                qcur[...] = ref[...]

        extra = qcur[:, 1280:1408].astype(f32)
        for h in range(heads):
            rows = slice(h * toks, (h + 1) * toks)
            cols = slice(h * width, (h + 1) * width)
            qm_h = qcur[:, cols]
            og_h = qcur[:, 768 + h * width : 768 + (h + 1) * width]
            qr_h = qcur[:, 512 + h * 64 : 512 + (h + 1) * 64]
            q_s[rows, 0:512] = dot(qm_h, wk[:, cols], ((1,), (1,))).astype(bf16)
            qt_s[0:512, rows] = dot(wk[:, cols], qm_h, ((1,), (1,))).astype(bf16)
            g_s[rows, :] = dot(og_h, wv[:, cols], ((1,), (1,))).astype(bf16)
            gt_s[:, rows] = dot(wv[:, cols], og_h, ((1,), (1,))).astype(bf16)
            q_s[rows, 512:576] = qr_h
            qt_s[512:576, rows] = qr_h.T
            for k, ref in enumerate((log_s, term_s)):
                at = (h * 2 + k) * 3
                value = extra[:, at : at + 1] + extra[:, at + 1 : at + 2] + extra[:, at + 2 : at + 3]
                ref[rows, :] = jnp.broadcast_to(value, (toks, 128))
        acc[...] = jnp.zeros_like(acc)
        from_x = (my_x - g + GROUP) % GROUP

        def plane(p, _):
            useful = jnp.where(p == 0, from_x >= my_x, info[jnp.maximum(p - 1, 0)] == 1)

            @pl.when(useful)
            def _():
                for i, ref in enumerate((k0, k1, k2, k3)):

                    @pl.when(p == i)
                    def _(ref=ref):
                        kcur[0:toks, :] = ref[...]

                kcur[toks : 2 * toks, :] = kother[p]
                scores = dot(q_s[...], kcur[...], ((1,), (1,)))
                slopes = dot(g_s[...], kcur[:, 0:512], ((1,), (1,)))
                logs = jnp.concatenate([log_s[...]] * 2, axis=1)
                terms = jnp.concatenate([term_s[...]] * 2, axis=1)
                shape = scores.shape
                row = lax.broadcasted_iota(jnp.int32, shape, 0) % toks
                col = lax.broadcasted_iota(jnp.int32, shape, 1)
                key_c = jnp.where(col < toks, my_c, 1 - my_c)
                key_place = (my_x * 2 + key_c) * toks + col % toks
                query_place = (from_x * 2 + my_c) * toks + row
                query_place = query_place + jnp.where(p == 0, 0, 1 << 20)
                weights = jnp.where(key_place <= query_place, jnp.exp(factor * scores - logs), 0.0)
                dscores = (weights * (slopes - terms)).astype(bf16)
                acc[...] += dot(dscores, kcur[...], ((1,), (0,)))
                ds_acc[p] += dot(qt_s[...], dscores, ((1,), (0,)))
                w_acc[p] += dot(gt_s[...], weights.astype(bf16), ((1,), (0,)))

            return 0

        lax.fori_loop(0, GROUP, plane, 0)
        mains, rots = [], []
        for h in range(heads):
            rows = slice(h * toks, (h + 1) * toks)
            cols = slice(h * width, (h + 1) * width)
            mixed = acc[rows, 0:512]
            high = mixed.astype(bf16)
            low = (mixed - high.astype(f32)).astype(bf16)
            w_h = wk[:, cols]
            mains.append(factor * (dot(high, w_h, ((1,), (0,))) + dot(low, w_h, ((1,), (0,)))))
            rots.append(factor * acc[rows, 512:576])
            qm_h = qcur[:, cols]
            wt_acc[cols, :] += dot(qm_h, high, ((0,), (0,))) + dot(qm_h, low, ((0,), (0,)))
        for i, ref in enumerate((d0, d1, d2, d3)):

            @pl.when(g == i)
            def _(ref=ref):
                ref[:, 0:512] = jnp.concatenate(mains, axis=1)
                ref[:, 512:768] = jnp.concatenate(rots, axis=1)

        return 0

    lax.fori_loop(0, GROUP, chunk, 0)
    for p in range(GROUP):
        lat_t = factor * ds_acc[p, 0:512, :] + w_acc[p]
        rot_t = factor * ds_acc[p, 512:576, :]
        both = jnp.concatenate([lat_t, rot_t], axis=0)
        for y in range(4):
            own[y, p] = both[y * 144 : (y + 1) * 144, 0:toks]
            other[y, p] = both[y * 144 : (y + 1) * 144, toks : 2 * toks]
    wout[...] = factor * wt_acc[...].T


def attend(info, qs, ks, kother, wk, wv):
    toks = 128
    out = jax.ShapeDtypeStruct
    vmem = pl.BlockSpec(memory_space=pltpu.VMEM)
    return pl.pallas_call(
        attend_kernel,
        in_specs=[pl.BlockSpec(memory_space=pltpu.SMEM)] + [vmem] * 11,
        out_specs=[vmem] * 7,
        out_shape=[out((toks, 768), f32)] * 4
        + [out((4, GROUP, 144, toks), f32)] * 2
        + [out((512, 512), f32)],
        scratch_shapes=[
            pltpu.VMEM((toks, 1408), bf16),
            pltpu.VMEM((2 * toks, 640), bf16),
            pltpu.VMEM((512, 640), bf16),
            pltpu.VMEM((576, 512), bf16),
            pltpu.VMEM((512, 512), bf16),
            pltpu.VMEM((512, 512), bf16),
            pltpu.VMEM((512, 128), f32),
            pltpu.VMEM((512, 128), f32),
            pltpu.VMEM((512, 640), f32),
            pltpu.VMEM((GROUP, 576, 2 * toks), f32),
            pltpu.VMEM((GROUP, 512, 2 * toks), f32),
            pltpu.VMEM((512, 512), f32),
        ],
        compiler_params=pltpu.CompilerParams(vmem_limit_bytes=48 << 20),
        name="attend",
    )(info, *qs, *ks, kother, wk, wv)


def per_device(
    query_main,
    query_rotary,
    latent,
    key_rotary,
    key_weight,
    value_weight,
    head_output,
    output_grad,
    row_logsum,
):
    my_z, my_x, my_c = (lax.axis_index(a) for a in SP)
    planes = lax.axis_size(Z)
    seq = (my_z + 1) // GROUP
    flags = [
        ((my_z >= s) & ((my_z - s + 1) // GROUP == seq)).astype(jnp.int32) for s in range(1, GROUP)
    ]
    info = jnp.stack([*flags, my_x, my_c]).astype(jnp.int32)
    qpack, kpack = pack(
        query_main, query_rotary, output_grad, head_output, row_logsum, latent, key_rotary
    )
    ks = [kpack] + [shift(kpack, Z, s) for s in range(1, GROUP)]
    qs = [qpack] + [shift(qpack, X, s) for s in range(1, GROUP)]
    kother = shift(jnp.stack(ks), C, 1)
    *dqs, own, other, weight = attend(info, qs, ks, kother, key_weight, value_weight)
    back = [dqs[0]] + [shift(dqs[s], X, -s) for s in range(1, GROUP)]
    grad_query = (back[0] + back[1]) + (back[2] + back[3])
    keys = own + shift(other, C, 1)
    keys = exchange(keys, Y).reshape(4, GROUP, 144, 128).sum(axis=0)
    key_t = keys[0]
    for s in range(1, GROUP):
        key_t = key_t + shift(keys[s], Z, -s)
    key_t = exchange(jnp.broadcast_to(key_t[None], (4, 144, 128)), Y)
    grad_key = key_t.reshape(576, 128).T
    weight = weight.reshape(planes, 4, 2, 4, 512)
    mine = lax.dynamic_index_in_dim(weight, my_c, 2, keepdims=False)
    theirs = lax.dynamic_index_in_dim(weight, 1 - my_c, 2, keepdims=False)
    weight = mine + shift(theirs, C, 1)
    weight = exchange(jnp.moveaxis(weight, 1, 0), X).sum(axis=0)
    near = [[a * 4 + b for b in range(4)] for a in range(planes // 4)]
    far = [[a * 4 + b for a in range(4)] for b in range(planes // 4)]
    weight = exchange(jnp.moveaxis(weight.reshape(4, 4, 4, 512), 1, 0), Z, near).sum(axis=0)
    weight = exchange(weight, Z, far).sum(axis=0)
    return (
        grad_query[:, 0:512],
        grad_query[:, 512:768],
        grad_key[:, 0:512],
        grad_key[:, 512:576],
        weight,
    )


def solution(mesh):
    finer = Mesh(mesh.devices.reshape(16, 4, 2, mesh.shape["tp"]), (Z, X, C, Y))
    return jax.shard_map(
        per_device,
        mesh=finer,
        in_specs=(
            P(SP, "tp"),
            P(SP, "tp"),
            P(SP, None),
            P(SP, None),
            P(None, "tp"),
            P(None, "tp"),
            P(SP, "tp"),
            P(SP, "tp"),
            P("tp", SP),
        ),
        out_specs=(P(SP, "tp"), P(SP, "tp"), P(SP, None), P(SP, None), P(SP, "tp")),
        check_vma=False,
    )
```

time: 744 us -> 197 us (0.26)
  the two profiles are of different devices: /device:TPU:8 before, /device:TPU:34 now
where the time goes in v1:
time: 197 us; the launch traced here: 196 us
  starting transfers between devices  86.4 us (44%)
  waiting for transfers between devices  67.5 us (34%)
  Pallas kernels  21 us (11%)
  local copies, waits for them, and re-layouts  11.6 us (6%)
  other arithmetic  8.33 us (4%)
    ppermute x15, starting transfers between devices, shift(): lax.ppermute(block, axis, [(i, (i + by) % peers) for i in range(peers)])  63.3 us
    all_to_all x5, waiting for transfers between devices, exchange(): lax.all_to_all(tiles, axis, 0, 0, tiled=True, axis_index_groups=groups)  37 us
    ppermute x15, waiting for transfers between devices, shift(): lax.ppermute(block, axis, [(i, (i + by) % peers) for i in range(peers)])  30.6 us
    all_to_all x5, starting transfers between devices, exchange(): lax.all_to_all(tiles, axis, 0, 0, tiled=True, axis_index_groups=groups)  23.1 us
    pallas_call x1, Pallas kernels, attend(): pl.pallas_call(attend_kernel, in_specs=[pl.BlockSpec(memory_space=pltpu.S...  18.6 us
    unnamed x26, local copies, waits for them, and re-layouts  6.36 us
  transfers between devices with their start and end apart: 20, of which 9 were waited for; matrix products, arithmetic and copies ran while one was open for 5% of the time, Pallas kernels for 0%

profile of v1, /device:TPU:34, one launch (start us, length us, event | category | flops | bytes accessed | tf_op | source)
XLA Modules:
  0.0 195.8 jit_solution(4152068332253194192)
XLA Ops:
  0.7 1.5 copy.25.rot
  2.2 2.3 %pack.1 = (bf16[128,1408]{1,0:T(8,128)(2,1)}, bf16[128,640]{1,0:T(8,128)(2,1)}) custom-call(bf16[128,512]{1,0:T(8,128)(2,1)} %qm.1, bf16[128,256]{1,0:T(8,128)(2,1)} %qr.1, bf16[128,512]{1,0:T(8,128)(2,1)} %og.1, bf16[128,512]{1,0:T(8,128)(2,1)} %ho.1, f32[4,128]{1,0:T(4,128)} %logs.1, bf16[128,512]{1,0:T(8,128)(2,1)} %lat.1, bf16[128,64]{1,0:T(8,128)(2,1)} %copy.25.rot), custom_call_target="tpu_custom_call" | custom-call | tf_op jit(solution)/shard_map/pack/pallas_call | solution.py:54
  4.5 4.0 %collective-permute-start.3 = (bf16[128,640]{1,0:T(8,128)(2,1)}, bf16[128,640]{1,0:T(8,128)(2,1)S(1)}, u32[]{:S(2)}, u32[]{:S(2)}) collective-permute-start(bf16[128,640]{1,0:T(8,128)(2,1)} %get-tuple-element.15.k0), channel_id=1, source_target_pairs={{0,32},{32,64},{64,96},{96,128},{128,160},{160,192},{192,224},{224... | collective-permute-start | bytes 491528 | tf_op jit(solution)/shard_map/ppermute | solution.py:18
  8.5 6.4 %collective-permute-start.4 = (bf16[128,640]{1,0:T(8,128)(2,1)}, bf16[128,640]{1,0:T(8,128)(2,1)S(1)}, u32[]{:S(2)}, u32[]{:S(2)}) collective-permute-start(bf16[128,640]{1,0:T(8,128)(2,1)} %get-tuple-element.15.k0), channel_id=1, source_target_pairs={{0,64},{32,96},{64,128},{96,160},{128,192},{160,224},{192,256},{22... | collective-permute-start | bytes 491528 | tf_op jit(solution)/shard_map/ppermute | solution.py:18
  14.9 6.5 %collective-permute-start.5 = (bf16[128,640]{1,0:T(8,128)(2,1)}, bf16[128,640]{1,0:T(8,128)(2,1)S(1)}, u32[]{:S(2)}, u32[]{:S(2)}) collective-permute-start(bf16[128,640]{1,0:T(8,128)(2,1)} %get-tuple-element.15.k0), channel_id=1, source_target_pairs={{0,96},{32,128},{64,160},{96,192},{128,224},{160,256},{192,288},{2... | collective-permute-start | bytes 491528 | tf_op jit(solution)/shard_map/ppermute | solution.py:18
  21.4 0.0 collective-permute-done.3.k1
  21.4 6.9 %collective-permute-done.4.k2 = bf16[128,640]{1,0:T(8,128)(2,1)S(1)} collective-permute-done((bf16[128,640]{1,0:T(8,128)(2,1)}, bf16[128,640]{1,0:T(8,128)(2,1)S(1)}, u32[]{:S(2)}, u32[]{:S(2)}) %collective-permute-start.4) | collective-permute-done | bytes 163872 | tf_op jit(solution)/shard_map/ppermute | solution.py:18
  28.3 9.9 %collective-permute-done.5.k3 = bf16[128,640]{1,0:T(8,128)(2,1)S(1)} collective-permute-done((bf16[128,640]{1,0:T(8,128)(2,1)}, bf16[128,640]{1,0:T(8,128)(2,1)S(1)}, u32[]{:S(2)}, u32[]{:S(2)}) %collective-permute-start.5) | collective-permute-done | bytes 163872 | tf_op jit(solution)/shard_map/ppermute | solution.py:18
  38.2 1.9 pad_maximum_fusion
  40.0 1.9 collective-permute-start.6
  42.0 3.4 %collective-permute-start = (bf16[128,1408]{1,0:T(8,128)(2,1)S(1)}, bf16[128,1408]{1,0:T(8,128)(2,1)S(1)}, u32[]{:S(2)}, u32[]{:S(2)}) collective-permute-start(bf16[128,1408]{1,0:T(8,128)(2,1)S(1)} %copy-done.3), channel_id=1, source_target_pairs={{0,8},{8,16},{16,24},{24,0},{1,9},{9,17},{17,25},{25,1},{2,10},{10... | collective-permute-start | bytes 1081352 | tf_op jit(solution)/shard_map/ppermute | solution.py:18
  45.4 3.3 %collective-permute-start.1 = (bf16[128,1408]{1,0:T(8,128)(2,1)S(1)}, bf16[128,1408]{1,0:T(8,128)(2,1)S(1)}, u32[]{:S(2)}, u32[]{:S(2)}) collective-permute-start(bf16[128,1408]{1,0:T(8,128)(2,1)S(1)} %copy-done.3), channel_id=1, source_target_pairs={{0,16},{8,24},{16,0},{24,8},{1,17},{9,25},{17,1},{25,9},{2,18},{10... | collective-permute-start | bytes 1081352 | tf_op jit(solution)/shard_map/ppermute | solution.py:18
  48.7 3.8 %collective-permute-start.2 = (bf16[128,1408]{1,0:T(8,128)(2,1)S(1)}, bf16[128,1408]{1,0:T(8,128)(2,1)}, u32[]{:S(2)}, u32[]{:S(2)}) collective-permute-start(bf16[128,1408]{1,0:T(8,128)(2,1)S(1)} %copy-done.3), channel_id=1, source_target_pairs={{0,24},{8,0},{16,8},{24,16},{1,25},{9,1},{17,9},{25,17},{2,26},{10... | collective-permute-start | bytes 1081352 | tf_op jit(solution)/shard_map/ppermute | solution.py:18
  52.6 0.1 stack.50.info
  52.6 2.5 %collective-permute-done.q1 = bf16[128,1408]{1,0:T(8,128)(2,1)S(1)} collective-permute-done((bf16[128,1408]{1,0:T(8,128)(2,1)S(1)}, bf16[128,1408]{1,0:T(8,128)(2,1)S(1)}, u32[]{:S(2)}, u32[]{:S(2)}) %collective-permute-start) | collective-permute-done | bytes 360480 | tf_op jit(solution)/shard_map/ppermute | solution.py:18
  55.1 5.0 %collective-permute-done.1.q2 = bf16[128,1408]{1,0:T(8,128)(2,1)S(1)} collective-permute-done((bf16[128,1408]{1,0:T(8,128)(2,1)S(1)}, bf16[128,1408]{1,0:T(8,128)(2,1)S(1)}, u32[]{:S(2)}, u32[]{:S(2)}) %collective-permute-start.1) | collective-permute-done | bytes 360480 | tf_op jit(solution)/shard_map/ppermute | solution.py:18
  60.1 0.7 copy-done.4
  60.9 6.3 %collective-permute-done.2.q3 = bf16[128,1408]{1,0:T(8,128)(2,1)} collective-permute-done((bf16[128,1408]{1,0:T(8,128)(2,1)S(1)}, bf16[128,1408]{1,0:T(8,128)(2,1)}, u32[]{:S(2)}, u32[]{:S(2)}) %collective-permute-start.2) | collective-permute-done | bytes 360480 | tf_op jit(solution)/shard_map/ppermute | solution.py:18
  67.1 0.0 collective-permute-done.6.kother
  67.2 1.0 copy-done.5
  68.1 18.6 %attend.1 = (f32[128,768]{1,0:T(8,128)S(1)}, f32[128,768]{1,0:T(8,128)S(1)}, f32[128,768]{1,0:T(8,128)S(1)}, f32[128,768]{1,0:T(8,128)S(1)}, f32[4,4,144,128]{3,...) custom-call(s32[5]{0:T(128)S(1)} %stack.50.info, bf16[128,1408]{1,0:T(8,128)(2,1)S(1)} %copy-done.3, ...), custom_call_target="tpu_custom_call" | custom-call | tf_op jit(solution)/shard_map/attend/pallas_call | solution.py:173
  86.8 0.7 copy-done.6
  87.5 0.8 copy-done.8
  88.3 0.8 copy-done.10
  89.0 1.5 reshape.21
  90.6 0.1 constant_dynamic-slice_fusion.1
  90.7 1.9 collective-permute-start.14
  92.7 2.4 %collective-permute-start.10 = (f32[4,4,144,128]{3,2,1,0:T(8,128)}, f32[4,4,144,128]{3,2,1,0:T(8,128)}, u32[]{:S(2)}, u32[]{:S(2)}) collective-permute-start(f32[4,4,144,128]{3,2,1,0:T(8,128)} %get-tuple-element.21), channel_id=1, source_target_pairs={{0,4},{4,0},{1,5},{5,1},{2,6},{6,2},{3,7},{7,3},{8,12},{12,8},{9,1... | collective-permute-start | bytes 3538952 | tf_op jit(solution)/shard_map/ppermute | solution.py:18
  95.1 0.0 collective-permute-done.14
  95.1 0.9 fusion
  96.0 4.6 %all-to-all-start.2 = ((f32[4,16,4,512]{3,2,1,0:T(4,128)}), f32[4,16,4,512]{3,2,1,0:T(4,128)S(1)}, u32[]{:S(2)}, u32[]{:S(2)}) async-start(f32[4,16,4,512]{3,2,1,0:T(4,128)} %fusion), calls=%async_computation.2 | async-start | bytes 1048576 | tf_op jit(solution)/shard_map/all_to_all | solution.py:22
  100.6 0.0 collective-permute-done.10
  100.6 2.8 %add.61 = f32[4,4,144,128]{3,2,1,0:T(8,128)} add(f32[4,4,144,128]{3,2,1,0:T(8,128)} %get-tuple-element.20, f32[4,4,144,128]{3,2,1,0:T(8,128)} %collective-permute-done.10) | non-fusion elementwise | flops 294912 | bytes 3538944 | tf_op jit(solution)/shard_map/add | solution.py:226
  103.4 5.7 %all-to-all-done.2 = f32[4,16,4,512]{3,2,1,0:T(4,128)S(1)} async-done(((f32[4,16,4,512]{3,2,1,0:T(4,128)}), f32[4,16,4,512]{3,2,1,0:T(4,128)S(1)}, u32[]{:S(2)}, u32[]{:S(2)}) %all-to-all-start.2) | async-done | bytes 524320 | tf_op jit(solution)/shard_map/all_to_all | solution.py:22
  109.1 4.1 %all-to-all-start = ((f32[4,4,144,128]{3,2,1,0:T(8,128)}), f32[4,4,144,128]{3,2,1,0:T(8,128)S(1)}, u32[]{:S(2)}, u32[]{:S(2)}) async-start(f32[4,4,144,128]{3,2,1,0:T(8,128)} %add.61), calls=%async_computation | async-start | bytes 2359296 | tf_op jit(solution)/shard_map/all_to_all | solution.py:22
  113.3 0.1 reduce_sum.37
  113.4 0.7 copy.28
  114.0 15.0 %all-to-all-done = f32[4,4,144,128]{3,2,1,0:T(8,128)S(1)} async-done(((f32[4,4,144,128]{3,2,1,0:T(8,128)}), f32[4,4,144,128]{3,2,1,0:T(8,128)S(1)}, u32[]{:S(2)}, u32[]{:S(2)}) %all-to-all-start) | async-done | bytes 1179680 | tf_op jit(solution)/shard_map/all_to_all | solution.py:22
  129.1 5.0 %all-to-all-start.3 = ((f32[4,4,4,512]{3,2,1,0:T(4,128)}), f32[4,4,4,512]{3,2,1,0:T(4,128)S(1)}, u32[]{:S(2)}, u32[]{:S(2)}) async-start(f32[4,4,4,512]{3,2,1,0:T(4,128)} %copy.28), calls=%async_computation.3 | async-start | bytes 262144 | tf_op jit(solution)/shard_map/all_to_all | solution.py:22
  134.1 3.4 %collective-permute-start.7 = (f32[128,768]{1,0:T(8,128)S(1)}, f32[128,768]{1,0:T(8,128)}, u32[]{:S(2)}, u32[]{:S(2)}) collective-permute-start(f32[128,768]{1,0:T(8,128)S(1)} %copy-done.11), channel_id=1, source_target_pairs={{0,24},{8,0},{16,8},{24,16},{1,25},{9,1},{17,9},{25,17},{2,26},{10... | collective-permute-start | bytes 1179656 | tf_op jit(solution)/shard_map/ppermute | solution.py:18
  137.5 1.9 collective-permute-start.8
  139.4 4.5 %collective-permute-start.9 = (f32[128,768]{1,0:T(8,128)S(1)}, f32[128,768]{1,0:T(8,128)}, u32[]{:S(2)}, u32[]{:S(2)}) collective-permute-start(f32[128,768]{1,0:T(8,128)S(1)} %copy-done.7), channel_id=1, source_target_pairs={{0,8},{8,16},{16,24},{24,0},{1,9},{9,17},{17,25},{25,1},{2,10},{10... | collective-permute-start | bytes 1179656 | tf_op jit(solution)/shard_map/ppermute | solution.py:18
  144.0 0.1 reduce_sum.36
  144.1 1.9 collective-permute-start.11
  146.0 13.5 %collective-permute-start.12 = (f32[144,128]{1,0:T(8,128)S(1)}, f32[144,128]{1,0:T(8,128)S(1)}, u32[]{:S(2)}, u32[]{:S(2)}) collective-permute-start(f32[144,128]{1,0:T(8,128)S(1)} %get-tuple-element.47), channel_id=1, source_target_pairs={{0,448},{32,480},{64,0},{96,32},{128,64},{160,96},{192,128},{224,1... | collective-permute-start | bytes 221192 | tf_op jit(solution)/shard_map/ppermute | solution.py:18
  159.5 0.0 collective-permute-done.11
  159.5 4.5 %collective-permute-start.13 = (f32[144,128]{1,0:T(8,128)S(1)}, f32[144,128]{1,0:T(8,128)S(1)}, u32[]{:S(2)}, u32[]{:S(2)}) collective-permute-start(f32[144,128]{1,0:T(8,128)S(1)} %get-tuple-element.46), channel_id=1, source_target_pairs={{0,416},{32,448},{64,480},{96,0},{128,32},{160,64},{192,96},{224,1... | collective-permute-start | bytes 221192 | tf_op jit(solution)/shard_map/ppermute | solution.py:18
  164.0 0.0 all-to-all-done.3
  164.1 0.6 reduce_sum.38
  164.7 5.9 %all-to-all-start.4 = ((f32[4,4,512]{2,1,0:T(4,128)}), f32[4,4,512]{2,1,0:T(4,128)S(1)}, u32[]{:S(2)}, u32[]{:S(2)}) async-start(f32[4,4,512]{2,1,0:T(4,128)} %reduce_sum.38), calls=%async_computation.4 | async-start | bytes 65536 | tf_op jit(solution)/shard_map/all_to_all | solution.py:22
  170.6 0.0 collective-permute-done.12
  170.6 0.0 collective-permute-done.13
  170.6 12.8 %all-to-all-done.4 = f32[4,4,512]{2,1,0:T(4,128)S(1)} async-done(((f32[4,4,512]{2,1,0:T(4,128)}), f32[4,4,512]{2,1,0:T(4,128)S(1)}, u32[]{:S(2)}, u32[]{:S(2)}) %all-to-all-start.4) | async-done | bytes 32800 | tf_op jit(solution)/shard_map/all_to_all | solution.py:22
  183.4 0.7 broadcast_in_dim.2
  184.1 3.5 %all-to-all-start.1 = ((f32[4,144,128]{2,1,0:T(8,128)}), f32[4,144,128]{2,1,0:T(8,128)S(1)}, u32[]{:S(2)}, u32[]{:S(2)}) async-start(f32[4,144,128]{2,1,0:T(8,128)} %broadcast_in_dim.2), calls=%async_computation.1 | async-start | bytes 589824 | tf_op jit(solution)/shard_map/all_to_all | solution.py:22
  187.6 0.0 collective-permute-done.7
  187.6 0.0 collective-permute-done.8
  187.6 1.3 add_add_fusion
  188.9 0.7 slice.32
  189.6 0.7 slice.33
  190.3 0.6 reduce_sum.39
  190.9 3.5 %all-to-all-done.1 = f32[4,144,128]{2,1,0:T(8,128)S(1)} async-done(((f32[4,144,128]{2,1,0:T(8,128)}), f32[4,144,128]{2,1,0:T(8,128)S(1)}, u32[]{:S(2)}, u32[]{:S(2)}) %all-to-all-start.1) | async-done | bytes 294944 | tf_op jit(solution)/shard_map/all_to_all | solution.py:22
  194.4 0.6 slice.39
  195.0 0.8 copy.29
  (24 shorter events, 0.1 us)
Async XLA Ops:
  0.6 66.5 %copy-start.1 = (bf16[512,512]{1,0:T(8,128)(2,1)S(1)}, bf16[512,512]{1,0:T(8,128)(2,1)}, u32[]{:S(2)}) copy-start(bf16[512,512]{1,0:T(8,128)(2,1)} %wk.1) | copy-start | bytes 1572868
  0.6 66.5 %copy-start.2 = (bf16[512,512]{1,0:T(8,128)(2,1)S(1)}, bf16[512,512]{1,0:T(8,128)(2,1)}, u32[]{:S(2)}) copy-start(bf16[512,512]{1,0:T(8,128)(2,1)} %wv.1) | copy-start | bytes 1572868
  4.5 37.5 %copy-start.3 = (bf16[128,1408]{1,0:T(8,128)(2,1)S(1)}, bf16[128,1408]{1,0:T(8,128)(2,1)}, u32[]{:S(2)}) copy-start(bf16[128,1408]{1,0:T(8,128)(2,1)} %get-tuple-element.14.q0) | copy-start | bytes 1081348
  4.5 62.6 %copy-start = (bf16[128,640]{1,0:T(8,128)(2,1)S(1)}, bf16[128,640]{1,0:T(8,128)(2,1)}, u32[]{:S(2)}) copy-start(bf16[128,640]{1,0:T(8,128)(2,1)} %get-tuple-element.15.k0) | copy-start | bytes 491524
  4.5 16.9 %collective-permute-start.3 = (bf16[128,640]{1,0:T(8,128)(2,1)}, bf16[128,640]{1,0:T(8,128)(2,1)S(1)}, u32[]{:S(2)}, u32[]{:S(2)}) collective-permute-start(bf16[128,640]{1,0:T(8,128)(2,1)} %get-tuple-element.15.k0), channel_id=1, source_target_pairs={{0,32},{32,64},{64,96},{96,128},{128,160},{160,192},{192,224},{224... | collective-permute-start | bytes 491528 | tf_op jit(solution)/shard_map/ppermute | solution.py:18
  8.5 19.8 %collective-permute-start.4 = (bf16[128,640]{1,0:T(8,128)(2,1)}, bf16[128,640]{1,0:T(8,128)(2,1)S(1)}, u32[]{:S(2)}, u32[]{:S(2)}) collective-permute-start(bf16[128,640]{1,0:T(8,128)(2,1)} %get-tuple-element.15.k0), channel_id=1, source_target_pairs={{0,64},{32,96},{64,128},{96,160},{128,192},{160,224},{192,256},{22... | collective-permute-start | bytes 491528 | tf_op jit(solution)/shard_map/ppermute | solution.py:18
  14.9 23.3 %collective-permute-start.5 = (bf16[128,640]{1,0:T(8,128)(2,1)}, bf16[128,640]{1,0:T(8,128)(2,1)S(1)}, u32[]{:S(2)}, u32[]{:S(2)}) collective-permute-start(bf16[128,640]{1,0:T(8,128)(2,1)} %get-tuple-element.15.k0), channel_id=1, source_target_pairs={{0,96},{32,128},{64,160},{96,192},{128,224},{160,256},{192,288},{2... | collective-permute-start | bytes 491528 | tf_op jit(solution)/shard_map/ppermute | solution.py:18
  40.0 27.1 %collective-permute-start.6 = (bf16[4,128,640]{2,1,0:T(8,128)(2,1)}, bf16[4,128,640]{2,1,0:T(8,128)(2,1)S(1)}, u32[]{:S(2)}, u32[]{:S(2)}) collective-permute-start(bf16[4,128,640]{2,1,0:T(8,128)(2,1)} %pad_maximum_fusion), channel_id=1, source_target_pairs={{0,4},{4,0},{1,5},{5,1},{2,6},{6,2},{3,7},{7,3},{8,12},{12,8},{9,1... | collective-permute-start | bytes 1966088 | tf_op jit(solution)/shard_map/ppermute | solution.py:18
  42.0 13.2 %collective-permute-start = (bf16[128,1408]{1,0:T(8,128)(2,1)S(1)}, bf16[128,1408]{1,0:T(8,128)(2,1)S(1)}, u32[]{:S(2)}, u32[]{:S(2)}) collective-permute-start(bf16[128,1408]{1,0:T(8,128)(2,1)S(1)} %copy-done.3), channel_id=1, source_target_pairs={{0,8},{8,16},{16,24},{24,0},{1,9},{9,17},{17,25},{25,1},{2,10},{10... | collective-permute-start | bytes 1081352 | tf_op jit(solution)/shard_map/ppermute | solution.py:18
  45.4 14.7 %collective-permute-start.1 = (bf16[128,1408]{1,0:T(8,128)(2,1)S(1)}, bf16[128,1408]{1,0:T(8,128)(2,1)S(1)}, u32[]{:S(2)}, u32[]{:S(2)}) collective-permute-start(bf16[128,1408]{1,0:T(8,128)(2,1)S(1)} %copy-done.3), channel_id=1, source_target_pairs={{0,16},{8,24},{16,0},{24,8},{1,17},{9,25},{17,1},{25,9},{2,18},{10... | collective-permute-start | bytes 1081352 | tf_op jit(solution)/shard_map/ppermute | solution.py:18
  48.7 18.4 %collective-permute-start.2 = (bf16[128,1408]{1,0:T(8,128)(2,1)S(1)}, bf16[128,1408]{1,0:T(8,128)(2,1)}, u32[]{:S(2)}, u32[]{:S(2)}) collective-permute-start(bf16[128,1408]{1,0:T(8,128)(2,1)S(1)} %copy-done.3), channel_id=1, source_target_pairs={{0,24},{8,0},{16,8},{24,16},{1,25},{9,1},{17,9},{25,17},{2,26},{10... | collective-permute-start | bytes 1081352 | tf_op jit(solution)/shard_map/ppermute | solution.py:18
  60.1 0.7 copy-start.4
  67.2 1.0 copy-start.5
  86.8 0.7 copy-start.6
  87.5 0.8 copy-start.8
  88.3 0.8 copy-start.10
  90.7 4.3 %collective-permute-start.14 = (f32[16,4,4,512]{3,2,0,1:T(4,128)S(1)}, f32[16,4,4,512]{3,2,0,1:T(4,128)S(1)}, u32[]{:S(2)}, u32[]{:S(2)}) collective-permute-start(f32[16,4,4,512]{3,2,0,1:T(4,128)S(1)} %bitcast.44), channel_id=1, source_target_pairs={{0,4},{4,0},{1,5},{5,1},{2,6},{6,2},{3,7},{7,3},{8,12},{12,8},{9,1... | collective-permute-start | bytes 1572872 | tf_op jit(solution)/shard_map/ppermute | solution.py:18
  92.7 8.0 %collective-permute-start.10 = (f32[4,4,144,128]{3,2,1,0:T(8,128)}, f32[4,4,144,128]{3,2,1,0:T(8,128)}, u32[]{:S(2)}, u32[]{:S(2)}) collective-permute-start(f32[4,4,144,128]{3,2,1,0:T(8,128)} %get-tuple-element.21), channel_id=1, source_target_pairs={{0,4},{4,0},{1,5},{5,1},{2,6},{6,2},{3,7},{7,3},{8,12},{12,8},{9,1... | collective-permute-start | bytes 3538952 | tf_op jit(solution)/shard_map/ppermute | solution.py:18
  96.0 13.1 %all-to-all-start.2 = ((f32[4,16,4,512]{3,2,1,0:T(4,128)}), f32[4,16,4,512]{3,2,1,0:T(4,128)S(1)}, u32[]{:S(2)}, u32[]{:S(2)}) async-start(f32[4,16,4,512]{3,2,1,0:T(4,128)} %fusion), calls=%async_computation.2 | async-start | bytes 1048576 | tf_op jit(solution)/shard_map/all_to_all | solution.py:22
  109.1 20.0 %all-to-all-start = ((f32[4,4,144,128]{3,2,1,0:T(8,128)}), f32[4,4,144,128]{3,2,1,0:T(8,128)S(1)}, u32[]{:S(2)}, u32[]{:S(2)}) async-start(f32[4,4,144,128]{3,2,1,0:T(8,128)} %add.61), calls=%async_computation | async-start | bytes 2359296 | tf_op jit(solution)/shard_map/all_to_all | solution.py:22
  113.2 20.9 %copy-start.11 = (f32[128,768]{1,0:T(8,128)S(1)}, f32[128,768]{1,0:T(8,128)}, u32[]{:S(2)}) copy-start(f32[128,768]{1,0:T(8,128)} %copy-done.10) | copy-start | bytes 1179652
  113.3 24.2 %copy-start.9 = (f32[128,768]{1,0:T(8,128)S(1)}, f32[128,768]{1,0:T(8,128)}, u32[]{:S(2)}) copy-start(f32[128,768]{1,0:T(8,128)} %copy-done.8) | copy-start | bytes 1179652
  113.3 26.2 %copy-start.7 = (f32[128,768]{1,0:T(8,128)S(1)}, f32[128,768]{1,0:T(8,128)}, u32[]{:S(2)}) copy-start(f32[128,768]{1,0:T(8,128)} %copy-done.6) | copy-start | bytes 1179652
  129.1 35.0 %all-to-all-start.3 = ((f32[4,4,4,512]{3,2,1,0:T(4,128)}), f32[4,4,4,512]{3,2,1,0:T(4,128)S(1)}, u32[]{:S(2)}, u32[]{:S(2)}) async-start(f32[4,4,4,512]{3,2,1,0:T(4,128)} %copy.28), calls=%async_computation.3 | async-start | bytes 262144 | tf_op jit(solution)/shard_map/all_to_all | solution.py:22
  134.1 53.4 %collective-permute-start.7 = (f32[128,768]{1,0:T(8,128)S(1)}, f32[128,768]{1,0:T(8,128)}, u32[]{:S(2)}, u32[]{:S(2)}) collective-permute-start(f32[128,768]{1,0:T(8,128)S(1)} %copy-done.11), channel_id=1, source_target_pairs={{0,24},{8,0},{16,8},{24,16},{1,25},{9,1},{17,9},{25,17},{2,26},{10... | collective-permute-start | bytes 1179656 | tf_op jit(solution)/shard_map/ppermute | solution.py:18
  137.5 50.1 %collective-permute-start.8 = (f32[128,768]{1,0:T(8,128)S(1)}, f32[128,768]{1,0:T(8,128)}, u32[]{:S(2)}, u32[]{:S(2)}) collective-permute-start(f32[128,768]{1,0:T(8,128)S(1)} %copy-done.9), channel_id=1, source_target_pairs={{0,16},{8,24},{16,0},{24,8},{1,17},{9,25},{17,1},{25,9},{2,18},{10... | collective-permute-start | bytes 1179656 | tf_op jit(solution)/shard_map/ppermute | solution.py:18
  139.4 48.1 %collective-permute-start.9 = (f32[128,768]{1,0:T(8,128)S(1)}, f32[128,768]{1,0:T(8,128)}, u32[]{:S(2)}, u32[]{:S(2)}) collective-permute-start(f32[128,768]{1,0:T(8,128)S(1)} %copy-done.7), channel_id=1, source_target_pairs={{0,8},{8,16},{16,24},{24,0},{1,9},{9,17},{17,25},{25,1},{2,10},{10... | collective-permute-start | bytes 1179656 | tf_op jit(solution)/shard_map/ppermute | solution.py:18
  144.1 15.5 %collective-permute-start.11 = (f32[144,128]{1,0:T(8,128)S(1)}, f32[144,128]{1,0:T(8,128)S(1)}, u32[]{:S(2)}, u32[]{:S(2)}) collective-permute-start(f32[144,128]{1,0:T(8,128)S(1)} %get-tuple-element.45), channel_id=1, source_target_pairs={{0,480},{32,0},{64,32},{96,64},{128,96},{160,128},{192,160},{224,1... | collective-permute-start | bytes 221192 | tf_op jit(solution)/shard_map/ppermute | solution.py:18
  146.0 24.6 %collective-permute-start.12 = (f32[144,128]{1,0:T(8,128)S(1)}, f32[144,128]{1,0:T(8,128)S(1)}, u32[]{:S(2)}, u32[]{:S(2)}) collective-permute-start(f32[144,128]{1,0:T(8,128)S(1)} %get-tuple-element.47), channel_id=1, source_target_pairs={{0,448},{32,480},{64,0},{96,32},{128,64},{160,96},{192,128},{224,1... | collective-permute-start | bytes 221192 | tf_op jit(solution)/shard_map/ppermute | solution.py:18
  159.5 11.0 %collective-permute-start.13 = (f32[144,128]{1,0:T(8,128)S(1)}, f32[144,128]{1,0:T(8,128)S(1)}, u32[]{:S(2)}, u32[]{:S(2)}) collective-permute-start(f32[144,128]{1,0:T(8,128)S(1)} %get-tuple-element.46), channel_id=1, source_target_pairs={{0,416},{32,448},{64,480},{96,0},{128,32},{160,64},{192,96},{224,1... | collective-permute-start | bytes 221192 | tf_op jit(solution)/shard_map/ppermute | solution.py:18
  164.7 18.7 %all-to-all-start.4 = ((f32[4,4,512]{2,1,0:T(4,128)}), f32[4,4,512]{2,1,0:T(4,128)S(1)}, u32[]{:S(2)}, u32[]{:S(2)}) async-start(f32[4,4,512]{2,1,0:T(4,128)} %reduce_sum.38), calls=%async_computation.4 | async-start | bytes 65536 | tf_op jit(solution)/shard_map/all_to_all | solution.py:22
  184.1 10.3 %all-to-all-start.1 = ((f32[4,144,128]{2,1,0:T(8,128)}), f32[4,144,128]{2,1,0:T(8,128)S(1)}, u32[]{:S(2)}, u32[]{:S(2)}) async-start(f32[4,144,128]{2,1,0:T(8,128)} %broadcast_in_dim.2), calls=%async_computation.1 | async-start | bytes 589824 | tf_op jit(solution)/shard_map/all_to_all | solution.py:22

commit v2 on v1

--- a/solution.py
+++ b/solution.py
@@ -6,6 +6,7 @@
 from jax.sharding import Mesh
 from jax.sharding import PartitionSpec as P
 
+
 Z, X, C, Y = "sp_0", "sp_1", "sp_2", "tp"
 SP = (Z, X, C)
 GROUP = 4
@@ -18,8 +19,11 @@
     return lax.ppermute(block, axis, [(i, (i + by) % peers) for i in range(peers)])
 
 
-def exchange(tiles, axis, groups=None):
-    return lax.all_to_all(tiles, axis, 0, 0, tiled=True, axis_index_groups=groups)
+def onward(block, by):
+    planes = lax.axis_size(Z)
+    ends = [(i, i + by) for i in range(planes)]
+    pairs = [(i, j) for i, j in ends if 0 <= j < planes and (i + 1) // GROUP == (j + 1) // GROUP]
+    return lax.ppermute(block, Z, pairs)
 
 
 def dot(a, b, dims):
@@ -29,9 +33,6 @@
 def pack_kernel(qm, qr, og, ho, logs, lat, rot, qpack, kpack):
     heads, toks = logs.shape
     width = qm.shape[1] // heads
-    qpack[:, 0:512] = qm[...]
-    qpack[:, 512:768] = qr[...]
-    qpack[:, 768:1280] = og[...]
     lane = lax.broadcasted_iota(jnp.int32, (toks, 128), 1)
     extra = jnp.zeros((toks, 128), f32)
     logs_t = logs[...].T
@@ -43,14 +44,17 @@
                 piece = value.astype(bf16).astype(f32)
                 value = value - piece
                 extra = jnp.where(lane == (h * 2 + k) * 3 + part, piece, extra)
+    qpack[:, 0:512] = qm[...]
+    qpack[:, 512:768] = qr[...]
+    qpack[:, 768:1280] = og[...]
     qpack[:, 1280:1408] = extra.astype(bf16)
     kpack[:, 0:512] = lat[...]
-    kpack[:, 512:576] = rot[...]
+    kpack[:, 512:576] = rot[...].T
     kpack[:, 576:640] = jnp.zeros((toks, 64), bf16)
 
 
-def pack(qm, qr, og, ho, logs, lat, rot):
-    toks = qm.shape[0]
+def pack(*args):
+    toks = args[0].shape[0]
     return pl.pallas_call(
         pack_kernel,
         out_shape=(
@@ -58,13 +62,13 @@
             jax.ShapeDtypeStruct((toks, 640), bf16),
         ),
         name="pack",
-    )(qm, qr, og, ho, logs, lat, rot)
+    )(*args)
 
 
 def attend_kernel(
     info, q0, q1, q2, q3, k0, k1, k2, k3, kother, wk, wv,
-    d0, d1, d2, d3, own, other, wout,
-    qcur, kcur, q_s, qt_s, g_s, gt_s, log_s, term_s, acc, ds_acc, w_acc, wt_acc,
+    back, mine, theirs,
+    qcur, kcur, q_s, qt_s, g_s, gt_s, log_s, term_s, acc, ds_acc, w_acc, wt_acc, back_s,
 ):
     heads, toks, width = 4, 128, 128
     factor = 192.0**-0.5
@@ -146,24 +150,40 @@
             rots.append(factor * acc[rows, 512:576])
             qm_h = qcur[:, cols]
             wt_acc[cols, :] += dot(qm_h, high, ((0,), (0,))) + dot(qm_h, low, ((0,), (0,)))
-        for i, ref in enumerate((d0, d1, d2, d3)):
-
-            @pl.when(g == i)
-            def _(ref=ref):
-                ref[:, 0:512] = jnp.concatenate(mains, axis=1)
-                ref[:, 512:768] = jnp.concatenate(rots, axis=1)
-
+        for h in range(heads):
+            back_s[from_x, h * toks : (h + 1) * toks, :] = mains[h]
+        for h in range(2):
+            pair = jnp.concatenate(rots[2 * h : 2 * h + 2], axis=1)
+            back_s[from_x, (heads + h) * toks : (heads + h + 1) * toks, :] = pair
         return 0
 
     lax.fori_loop(0, GROUP, chunk, 0)
     for p in range(GROUP):
-        lat_t = factor * ds_acc[p, 0:512, :] + w_acc[p]
-        rot_t = factor * ds_acc[p, 512:576, :]
-        both = jnp.concatenate([lat_t, rot_t], axis=0)
-        for y in range(4):
-            own[y, p] = both[y * 144 : (y + 1) * 144, 0:toks]
-            other[y, p] = both[y * 144 : (y + 1) * 144, toks : 2 * toks]
-    wout[...] = factor * wt_acc[...].T
+        for rows in (slice(0, 512), slice(512, 576)):
+            both = factor * ds_acc[p, rows, :]
+            if rows.start == 0:
+                both = both + w_acc[p]
+            mine[p, rows, :] = both[:, 0:toks]
+            theirs[p, rows, :] = both[:, toks : 2 * toks]
+    wt_acc[...] = factor * wt_acc[...].T
+    upper = lax.broadcasted_iota(jnp.int32, (8, 512), 0) < 4
+    for x in range(4):
+        for b in range(4):
+            for pair in range(2):
+                one, two = (
+                    wt_acc[(((8 * pair + 4 * g + b + 15) % 16) * 4 + x) * 8 :][:8] for g in range(2)
+                )
+                even = jnp.where(upper, one, pltpu.roll(two, 4, 0))
+                odd = jnp.where(upper, pltpu.roll(one, 4, 0), two)
+                at = 768 + (b * 2 + pair) * 32
+                for first, tile in enumerate(
+                    (jnp.where(my_c == 0, even, odd), jnp.where(my_c == 0, odd, even))
+                ):
+                    for k in range(4):
+                        lanes = slice(k * 128, (k + 1) * 128)
+                        rows = slice(at + first * 256 + k * 8, at + first * 256 + k * 8 + 8)
+                        back_s[x, rows, :] = tile[:, lanes]
+    back[...] = back_s[...].astype(bf16)
 
 
 def attend(info, qs, ks, kother, wk, wv):
@@ -173,10 +193,12 @@
     return pl.pallas_call(
         attend_kernel,
         in_specs=[pl.BlockSpec(memory_space=pltpu.SMEM)] + [vmem] * 11,
-        out_specs=[vmem] * 7,
-        out_shape=[out((toks, 768), f32)] * 4
-        + [out((4, GROUP, 144, toks), f32)] * 2
-        + [out((512, 512), f32)],
+        out_specs=[vmem] * 3,
+        out_shape=[
+            out((4, 1280, 128), bf16),
+            out((GROUP, 576, toks), f32),
+            out((GROUP, 576, toks), f32),
+        ],
         scratch_shapes=[
             pltpu.VMEM((toks, 1408), bf16),
             pltpu.VMEM((2 * toks, 640), bf16),
@@ -190,10 +212,91 @@
             pltpu.VMEM((GROUP, 576, 2 * toks), f32),
             pltpu.VMEM((GROUP, 512, 2 * toks), f32),
             pltpu.VMEM((512, 512), f32),
+            pltpu.VMEM((4, 1280, 128), f32),
         ],
-        compiler_params=pltpu.CompilerParams(vmem_limit_bytes=48 << 20),
+        compiler_params=pltpu.CompilerParams(vmem_limit_bytes=60 << 20),
         name="attend",
     )(info, *qs, *ks, kother, wk, wv)
+
+
+def local(body, shapes, *args, scalars=0, scratch=(), aliases=None):
+    vmem = pl.BlockSpec(memory_space=pltpu.VMEM)
+    smem = pl.BlockSpec(memory_space=pltpu.SMEM)
+    return pl.pallas_call(
+        body,
+        in_specs=[smem] * scalars + [vmem] * (len(args) - scalars),
+        out_specs=[vmem] * len(shapes),
+        out_shape=[jax.ShapeDtypeStruct(s, t) for s, t in shapes],
+        scratch_shapes=list(scratch),
+        input_output_aliases=aliases or {},
+        compiler_params=pltpu.CompilerParams(vmem_limit_bytes=4 << 20),
+    )(*args)
+
+
+def stack_kernel(k0, k1, k2, k3, out):
+    for i, k in enumerate((k0, k1, k2, k3)):
+        out[i] = k[...]
+
+
+def pair_kernel(mine, theirs, z0, z1, z2, z3):
+    for p, out in enumerate((z0, z1, z2, z3)):
+        out[...] = (mine[p] + theirs[p]).astype(out.dtype)
+
+
+def added(parts):
+    return (parts[0] + parts[1]) + (parts[2] + parts[3])
+
+
+def back_kernel(back, main, rotary, mine, theirs):
+    def rows(start, count):
+        return added([back[i, start : start + count, :].astype(f32) for i in range(4)])
+
+    for h in range(4):
+        main[:, h * 128 : (h + 1) * 128] = rows(h * 128, 128)
+    for h in range(2):
+        rotary[:, h * 128 : (h + 1) * 128] = rows(512 + h * 128, 128)
+    for b in range(4):
+        mine[b] = rows(768 + b * 64, 64)
+        theirs[b] = rows(1024 + b * 64, 64)
+
+
+def weight_kernel(mine, theirs, total):
+    total[...] = mine[...] + theirs[...]
+
+
+def key_kernel(z0, z1, z2, z3, key):
+    key[...] = added([z[...].astype(f32) for z in (z0, z1, z2, z3)])
+
+
+def far_kernel(near, far):
+    total = added([near[i] for i in range(4)])
+    for pair in range(2):
+        for k in range(4):
+            tile = total[pair * 32 + k * 8 :][:8]
+            far[2 * pair, k * 8 : k * 8 + 8, :] = tile
+            far[2 * pair + 1, k * 8 : k * 8 + 8, :] = pltpu.roll(tile, 4, 0)
+
+
+def last_kernel(info, a0, a1, a2, a3, far, lat, rot, weight, keys):
+    for s, a in enumerate((a0, a1, a2, a3)):
+        keys[(info[6] - s + 4) % 4] = a[...]
+    total = added([keys[y] for y in range(4)])
+    lat[...] = total[0:512, :].T
+    rot[...] = total[512:576, :]
+    for k in range(4):
+        part = added([far[i, k * 8 : k * 8 + 4, :] for i in range(4)])
+        weight[:, k * 128 : (k + 1) * 128] = part
+
+
+def exchange(tiles, axis, groups=None):
+    return lax.all_to_all(tiles, axis, 0, 0, tiled=True, axis_index_groups=groups)
+
+
+def spread(blocks, axis):
+    got = [blocks[0]]
+    for s in range(1, 4):
+        got.append(shift(blocks[s], axis, s))
+    return got
 
 
 def per_device(
@@ -213,39 +316,42 @@
     flags = [
         ((my_z >= s) & ((my_z - s + 1) // GROUP == seq)).astype(jnp.int32) for s in range(1, GROUP)
     ]
-    info = jnp.stack([*flags, my_x, my_c]).astype(jnp.int32)
+    turns = [my_x, my_c, (my_z + 1) % GROUP, lax.axis_index(Y), seq % 4]
+    info = jnp.stack([*flags, *turns]).astype(jnp.int32)
     qpack, kpack = pack(
-        query_main, query_rotary, output_grad, head_output, row_logsum, latent, key_rotary
+        query_main, query_rotary, output_grad, head_output, row_logsum, latent, key_rotary.T
     )
-    ks = [kpack] + [shift(kpack, Z, s) for s in range(1, GROUP)]
-    qs = [qpack] + [shift(qpack, X, s) for s in range(1, GROUP)]
-    kother = shift(jnp.stack(ks), C, 1)
-    *dqs, own, other, weight = attend(info, qs, ks, kother, key_weight, value_weight)
-    back = [dqs[0]] + [shift(dqs[s], X, -s) for s in range(1, GROUP)]
-    grad_query = (back[0] + back[1]) + (back[2] + back[3])
-    keys = own + shift(other, C, 1)
-    keys = exchange(keys, Y).reshape(4, GROUP, 144, 128).sum(axis=0)
-    key_t = keys[0]
+    ks = [kpack]
     for s in range(1, GROUP):
-        key_t = key_t + shift(keys[s], Z, -s)
-    key_t = exchange(jnp.broadcast_to(key_t[None], (4, 144, 128)), Y)
-    grad_key = key_t.reshape(576, 128).T
-    weight = weight.reshape(planes, 4, 2, 4, 512)
-    mine = lax.dynamic_index_in_dim(weight, my_c, 2, keepdims=False)
-    theirs = lax.dynamic_index_in_dim(weight, 1 - my_c, 2, keepdims=False)
-    weight = mine + shift(theirs, C, 1)
-    weight = exchange(jnp.moveaxis(weight, 1, 0), X).sum(axis=0)
-    near = [[a * 4 + b for b in range(4)] for a in range(planes // 4)]
-    far = [[a * 4 + b for a in range(4)] for b in range(planes // 4)]
-    weight = exchange(jnp.moveaxis(weight.reshape(4, 4, 4, 512), 1, 0), Z, near).sum(axis=0)
-    weight = exchange(weight, Z, far).sum(axis=0)
-    return (
-        grad_query[:, 0:512],
-        grad_query[:, 512:768],
-        grad_key[:, 0:512],
-        grad_key[:, 512:576],
-        weight,
+        ks.append(onward(kpack, s))
+    qs = spread([qpack] * 4, X)
+    (stacked,) = local(stack_kernel, [((4, *kpack.shape), bf16)], *ks)
+    kother = shift(stacked, C, 1)
+    back, mine, theirs = attend(info, qs, ks, kother, key_weight, value_weight)
+    back = exchange(back, X)
+    theirs = shift(theirs, C, 1)
+    shapes = [((576, 128), f32)] + [((576, 128), bf16)] * 3
+    planes = local(pair_kernel, shapes, mine, theirs)
+    planes = list(planes)
+    for s in range(1, 4):
+        planes[s] = onward(planes[s], -s)
+    toks = key_rotary.shape[0]
+    shapes = [((toks, 512), f32), ((toks, 256), f32)] + [((4, 64, 128), f32)] * 2
+    main, rotary, mine, theirs = local(back_kernel, shapes, back)
+    theirs = shift(theirs, C, 1)
+    (weight,) = local(weight_kernel, [((4, 64, 128), f32)], mine, theirs)
+    near = [[(4 * g + b - 1) % 16 for b in range(4)] for g in range(4)]
+    weight = exchange(weight, Z, near)
+    (key,) = local(key_kernel, [((576, 128), f32)], *planes)
+    keys = spread([key] * 4, Y)
+    (weight,) = local(far_kernel, [((4, 32, 128), f32)], weight)
+    weight = exchange(weight, Z, [list(z) for z in zip(*near)])
+    shapes = [((toks, 512), f32), ((64, toks), f32), ((4, 512), f32)]
+    lat, rot, weight = local(
+        last_kernel, shapes, info, *keys, weight,
+        scalars=1, scratch=[pltpu.VMEM((4, 576, 128), f32)],
     )
+    return main, rotary, lat, rot.T, weight
 
 
 def solution(mesh):

time: 197 us -> 173 us (0.88)
  the two profiles are of different devices: /device:TPU:34 before, /device:TPU:8 now
where the time goes in v2:
time: 173 us; the launch traced here: 172 us
  starting transfers between devices  84.4 us (49%)
  waiting for transfers between devices  60.2 us (35%)
  Pallas kernels  23.1 us (13%)
  local copies, waits for them, and re-layouts  3.12 us (2%)
    all_to_all x3, starting transfers between devices, exchange(): lax.all_to_all(tiles, axis, 0, 0, tiled=True, axis_index_groups=groups)  47.2 us
    all_to_all x3, waiting for transfers between devices, exchange(): lax.all_to_all(tiles, axis, 0, 0, tiled=True, axis_index_groups=groups)  29.5 us
    ppermute x9, starting transfers between devices, shift(): lax.ppermute(block, axis, [(i, (i + by) % peers) for i in range(peers)])  26.9 us
    ppermute x9, waiting for transfers between devices, shift(): lax.ppermute(block, axis, [(i, (i + by) % peers) for i in range(peers)])  16.7 us
    pallas_call x1, Pallas kernels, attend(): pl.pallas_call(attend_kernel, in_specs=[pl.BlockSpec(memory_space=pltpu.S...  15.7 us
    ppermute x6, waiting for transfers between devices, onward(): return lax.ppermute(block, Z, pairs)  14 us
    ppermute x6, starting transfers between devices, onward(): return lax.ppermute(block, Z, pairs)  10.4 us
    pallas_call x7, Pallas kernels, local(): pl.pallas_call(body, in_specs=[smem] * scalars + [vmem] * (len(args) - sc...  5.1 us
  transfers between devices with their start and end apart: 18, of which 9 were waited for; matrix products, arithmetic and copies ran while one was open for 0% of the time, Pallas kernels for 2%

profile of v2, /device:TPU:8, one launch (start us, length us, event | category | flops | bytes accessed | tf_op | source)
XLA Modules:
  0.0 171.8 jit_solution(1051503521094681883)
XLA Ops:
  0.6 2.4 %pack.1 = (bf16[128,1408]{1,0:T(8,128)(2,1)}, bf16[128,640]{1,0:T(8,128)(2,1)}) custom-call(bf16[128,512]{1,0:T(8,128)(2,1)} %qm.1, bf16[128,256]{1,0:T(8,128)(2,1)} %qr.1, bf16[128,512]{1,0:T(8,128)(2,1)} %og.1, bf16[128,512]{1,0:T(8,128)(2,1)} %ho.1, f32[4,128]{1,0:T(4,128)} %logs.1, bf16[128,512]{1,0:T(8,128)(2,1)} %lat.1, bf16[64,128]{1,0:T(8,128)(2,1)} %bitcast.10), custom_call_target="tpu_custom_call" | custom-call | tf_op jit(solution)/shard_map/pack/pallas_call | solution.py:58
  3.0 0.7 collective-permute-start.5
  3.7 5.2 %collective-permute-start.4 = (bf16[128,640]{1,0:T(8,128)(2,1)}, bf16[128,640]{1,0:T(8,128)(2,1)S(1)}, u32[]{:S(2)}, u32[]{:S(2)}) collective-permute-start(bf16[128,640]{1,0:T(8,128)(2,1)} %get-tuple-element.22.k0), channel_id=1, source_target_pairs={{0,64},{96,160},{128,192},{224,288},{256,320},{352,416},{384,448},... | collective-permute-start | bytes 491528 | tf_op jit(solution)/shard_map/ppermute | solution.py:26
  8.9 1.3 collective-permute-start.3
  10.2 0.0 collective-permute-done.5.k3
  10.2 0.0 copy-start.2
  10.2 3.6 %collective-permute-done.4.k2 = bf16[128,640]{1,0:T(8,128)(2,1)S(1)} collective-permute-done((bf16[128,640]{1,0:T(8,128)(2,1)}, bf16[128,640]{1,0:T(8,128)(2,1)S(1)}, u32[]{:S(2)}, u32[]{:S(2)}) %collective-permute-start.4) | collective-permute-done | bytes 163872 | tf_op jit(solution)/shard_map/ppermute | solution.py:26
  13.8 0.0 copy-start.3
  13.8 2.4 %collective-permute-done.3.k1 = bf16[128,640]{1,0:T(8,128)(2,1)S(1)} collective-permute-done((bf16[128,640]{1,0:T(8,128)(2,1)}, bf16[128,640]{1,0:T(8,128)(2,1)S(1)}, u32[]{:S(2)}, u32[]{:S(2)}) %collective-permute-start.3) | collective-permute-done | bytes 163872 | tf_op jit(solution)/shard_map/ppermute | solution.py:26
  16.2 0.0 copy-start.1
  16.2 0.9 copy-done.1
  17.1 0.0 copy-start.4
  17.1 0.0 copy-start.7
  17.1 0.1 shard_map.128
  17.1 2.1 %collective-permute-start.6 = (bf16[4,128,640]{2,1,0:T(8,128)(2,1)S(1)}, bf16[4,128,640]{2,1,0:T(8,128)(2,1)S(1)}, u32[]{:S(2)}, u32[]{:S(2)}) collective-permute-start(bf16[4,128,640]{2,1,0:T(8,128)(2,1)S(1)} %shard_map.128), channel_id=1, source_target_pairs={{0,4},{4,0},{1,5},{5,1},{2,6},{6,2},{3,7},{7,3},{8,12},{12,8},{9,1... | collective-permute-start | bytes 1966088 | tf_op jit(solution)/shard_map/ppermute | solution.py:19
  19.2 0.0 copy-done.7
  19.2 4.7 %collective-permute-start.2 = (bf16[128,1408]{1,0:T(8,128)(2,1)S(1)}, bf16[128,1408]{1,0:T(8,128)(2,1)S(1)}, u32[]{:S(2)}, u32[]{:S(2)}) collective-permute-start(bf16[128,1408]{1,0:T(8,128)(2,1)S(1)} %copy-done.7), channel_id=1, source_target_pairs={{0,24},{8,0},{16,8},{24,16},{1,25},{9,1},{17,9},{25,17},{2,26},{10... | collective-permute-start | bytes 1081352 | tf_op jit(solution)/shard_map/ppermute | solution.py:19
  23.9 2.7 %collective-permute-start.1 = (bf16[128,1408]{1,0:T(8,128)(2,1)S(1)}, bf16[128,1408]{1,0:T(8,128)(2,1)S(1)}, u32[]{:S(2)}, u32[]{:S(2)}) collective-permute-start(bf16[128,1408]{1,0:T(8,128)(2,1)S(1)} %copy-done.7), channel_id=1, source_target_pairs={{0,16},{8,24},{16,0},{24,8},{1,17},{9,25},{17,1},{25,9},{2,18},{10... | collective-permute-start | bytes 1081352 | tf_op jit(solution)/shard_map/ppermute | solution.py:19
  26.6 2.8 %collective-permute-start = (bf16[128,1408]{1,0:T(8,128)(2,1)S(1)}, bf16[128,1408]{1,0:T(8,128)(2,1)S(1)}, u32[]{:S(2)}, u32[]{:S(2)}) collective-permute-start(bf16[128,1408]{1,0:T(8,128)(2,1)S(1)} %copy-done.7), channel_id=1, source_target_pairs={{0,8},{8,16},{16,24},{24,0},{1,9},{9,17},{17,25},{25,1},{2,10},{10... | collective-permute-start | bytes 1081352 | tf_op jit(solution)/shard_map/ppermute | solution.py:19
  29.5 0.6 stack.47.info
  30.1 9.8 %collective-permute-done.2.q3 = bf16[128,1408]{1,0:T(8,128)(2,1)S(1)} collective-permute-done((bf16[128,1408]{1,0:T(8,128)(2,1)S(1)}, bf16[128,1408]{1,0:T(8,128)(2,1)S(1)}, u32[]{:S(2)}, u32[]{:S(2)}) %collective-permute-start.2) | collective-permute-done | bytes 360480 | tf_op jit(solution)/shard_map/ppermute | solution.py:19
  39.9 0.0 collective-permute-done.1.q2
  40.0 5.6 %collective-permute-done.q1 = bf16[128,1408]{1,0:T(8,128)(2,1)S(1)} collective-permute-done((bf16[128,1408]{1,0:T(8,128)(2,1)S(1)}, bf16[128,1408]{1,0:T(8,128)(2,1)S(1)}, u32[]{:S(2)}, u32[]{:S(2)}) %collective-permute-start) | collective-permute-done | bytes 360480 | tf_op jit(solution)/shard_map/ppermute | solution.py:19
  45.5 0.0 collective-permute-done.6.kother
  45.5 0.0 copy-done.2
  45.5 0.0 copy-done.3
  45.6 0.0 copy-done.4
  45.6 0.0 copy-done.8
  45.6 0.0 copy-done.9
  45.6 0.7 copy-done.10
  46.3 0.8 copy-done.6
  47.1 15.7 %attend.1 = (bf16[4,1280,128]{2,1,0:T(8,128)(2,1)}, f32[4,576,128]{2,1,0:T(8,128)}, f32[4,576,128]{2,1,0:T(8,128)}) custom-call(s32[8]{0:T(128)} %stack.47.info, bf16[128,1408]{1,0:T(8,128)(2,1)} %get-tuple-element.21.q0, bf16[128,1408]{1,0:T(8,128)(2,1)} %copy-done.10, bf16[128,1408]{1,0:T(8,128)(2,1)} %copy-done.9, bf16[128,1408]{1,0:T(8,128)(2,1)} %copy-done.8, ...), custom_call_target="tpu_custom_call" | custom-call | tf_op jit(solution)/shard_map/attend/pallas_call | solution.py:193
  62.8 3.5 %all-to-all-start = ((bf16[4,1280,128]{2,1,0:T(8,128)(2,1)}), bf16[4,1280,128]{2,1,0:T(8,128)(2,1)S(1)}, u32[]{:S(2)}, u32[]{:S(2)}) async-start(bf16[4,1280,128]{2,1,0:T(8,128)(2,1)} %get-tuple-element.23), calls=%async_computation | async-start | bytes 2621440 | tf_op jit(solution)/shard_map/all_to_all | solution.py:292
  66.4 0.0 copy-start
  66.4 2.1 %collective-permute-start.7 = (f32[4,576,128]{2,1,0:T(8,128)}, f32[4,576,128]{2,1,0:T(8,128)}, u32[]{:S(2)}, u32[]{:S(2)}) collective-permute-start(f32[4,576,128]{2,1,0:T(8,128)} %get-tuple-element.27), channel_id=1, source_target_pairs={{0,4},{4,0},{1,5},{5,1},{2,6},{6,2},{3,7},{7,3},{8,12},{12,8},{9,1... | collective-permute-start | bytes 3538952 | tf_op jit(solution)/shard_map/ppermute | solution.py:19
  68.4 16.3 %all-to-all-done.back = bf16[4,1280,128]{2,1,0:T(8,128)(2,1)S(1)} async-done(((bf16[4,1280,128]{2,1,0:T(8,128)(2,1)}), bf16[4,1280,128]{2,1,0:T(8,128)(2,1)S(1)}, u32[]{:S(2)}, u32[]{:S(2)}) %all-to-all-start) | async-done | bytes 1310752 | tf_op jit(solution)/shard_map/all_to_all | solution.py:292
  84.7 0.8 shard_map.129
  85.5 1.9 %collective-permute-start.14 = (f32[4,64,128]{2,1,0:T(8,128)S(1)}, f32[4,64,128]{2,1,0:T(8,128)S(1)}, u32[]{:S(2)}, u32[]{:S(2)}) collective-permute-start(f32[4,64,128]{2,1,0:T(8,128)S(1)} %get-tuple-element.33), channel_id=1, source_target_pairs={{0,4},{4,0},{1,5},{5,1},{2,6},{6,2},{3,7},{7,3},{8,12},{12,8},{9,1... | collective-permute-start | bytes 393224 | tf_op jit(solution)/shard_map/ppermute | solution.py:19
  87.4 1.3 collective-permute-done.14.theirs
  88.7 0.7 shard_map.132
  89.4 16.8 %all-to-all-start.1 = ((f32[4,64,128]{2,1,0:T(8,128)}), f32[4,64,128]{2,1,0:T(8,128)S(1)}, u32[]{:S(2)}, u32[]{:S(2)}) async-start(f32[4,64,128]{2,1,0:T(8,128)} %shard_map.132), calls=%async_computation.1 | async-start | bytes 262144 | tf_op jit(solution)/shard_map/all_to_all | solution.py:292
  106.2 0.0 collective-permute-done.7.theirs
  106.2 0.0 copy-done
  106.2 1.4 shard_map.130
  107.6 0.0 copy-start.5
  107.6 1.3 collective-permute-start.8
  108.9 1.3 collective-permute-start.9
  110.2 0.7 collective-permute-start.10
  110.9 4.4 %collective-permute-done.8.z1 = bf16[576,128]{1,0:T(8,128)(2,1)S(1)} collective-permute-done((bf16[576,128]{1,0:T(8,128)(2,1)S(1)}, bf16[576,128]{1,0:T(8,128)(2,1)S(1)}, u32[]{:S(2)}, u32[]{:S(2)}) %collective-permute-start.8) | collective-permute-done | bytes 147488 | tf_op jit(solution)/shard_map/ppermute | solution.py:26
  115.3 3.6 %collective-permute-done.9.z2 = bf16[576,128]{1,0:T(8,128)(2,1)S(1)} collective-permute-done((bf16[576,128]{1,0:T(8,128)(2,1)S(1)}, bf16[576,128]{1,0:T(8,128)(2,1)S(1)}, u32[]{:S(2)}, u32[]{:S(2)}) %collective-permute-start.9) | collective-permute-done | bytes 147488 | tf_op jit(solution)/shard_map/ppermute | solution.py:26
  118.9 0.0 collective-permute-done.10.z3
  118.9 0.1 shard_map.131.a0
  119.0 2.3 %collective-permute-start.13 = (f32[576,128]{1,0:T(8,128)S(1)}, f32[576,128]{1,0:T(8,128)S(1)}, u32[]{:S(2)}, u32[]{:S(2)}) collective-permute-start(f32[576,128]{1,0:T(8,128)S(1)} %shard_map.131.a0), channel_id=1, source_target_pairs={{0,3},{1,0},{2,1},{3,2},{4,7},{5,4},{6,5},{7,6},{8,11},{9,8},{10,9... | collective-permute-start | bytes 884744 | tf_op jit(solution)/shard_map/ppermute | solution.py:19
  121.3 4.5 %collective-permute-start.12 = (f32[576,128]{1,0:T(8,128)S(1)}, f32[576,128]{1,0:T(8,128)S(1)}, u32[]{:S(2)}, u32[]{:S(2)}) collective-permute-start(f32[576,128]{1,0:T(8,128)S(1)} %shard_map.131.a0), channel_id=1, source_target_pairs={{0,2},{1,3},{2,0},{3,1},{4,6},{5,7},{6,4},{7,5},{8,10},{9,11},{10,... | collective-permute-start | bytes 884744 | tf_op jit(solution)/shard_map/ppermute | solution.py:19
  125.8 3.8 %collective-permute-start.11 = (f32[576,128]{1,0:T(8,128)S(1)}, f32[576,128]{1,0:T(8,128)S(1)}, u32[]{:S(2)}, u32[]{:S(2)}) collective-permute-start(f32[576,128]{1,0:T(8,128)S(1)} %shard_map.131.a0), channel_id=1, source_target_pairs={{0,1},{1,2},{2,3},{3,0},{4,5},{5,6},{6,7},{7,4},{8,9},{9,10},{10,1... | collective-permute-start | bytes 884744 | tf_op jit(solution)/shard_map/ppermute | solution.py:19
  129.6 0.0 all-to-all-done.1.near
  129.7 0.6 shard_map.133
  130.3 26.8 %all-to-all-start.2 = ((f32[4,32,128]{2,1,0:T(8,128)}), f32[4,32,128]{2,1,0:T(8,128)S(1)}, u32[]{:S(2)}, u32[]{:S(2)}) async-start(f32[4,32,128]{2,1,0:T(8,128)} %shard_map.133), calls=%async_computation.2 | async-start | bytes 131072 | tf_op jit(solution)/shard_map/all_to_all | solution.py:292
  157.1 0.0 collective-permute-done.13.a3
  157.1 0.0 collective-permute-done.12.a2
  157.1 0.0 collective-permute-done.11.a1
  157.2 13.2 %all-to-all-done.2.far = f32[4,32,128]{2,1,0:T(8,128)S(1)} async-done(((f32[4,32,128]{2,1,0:T(8,128)}), f32[4,32,128]{2,1,0:T(8,128)S(1)}, u32[]{:S(2)}, u32[]{:S(2)}) %all-to-all-start.2) | async-done | bytes 65568 | tf_op jit(solution)/shard_map/all_to_all | solution.py:292
  170.4 0.0 copy-done.5
  170.4 1.5 shard_map.134
  (4 shorter events, 0.0 us)
Async XLA Ops:
  3.0 7.2 %collective-permute-start.5 = (bf16[128,640]{1,0:T(8,128)(2,1)}, bf16[128,640]{1,0:T(8,128)(2,1)S(1)}, u32[]{:S(2)}, u32[]{:S(2)}) collective-permute-start(bf16[128,640]{1,0:T(8,128)(2,1)} %get-tuple-element.22.k0), channel_id=1, source_target_pairs={{96,192},{224,320},{352,448},{97,193},{225,321},{353,449},{98,194}... | collective-permute-start | bytes 491528 | tf_op jit(solution)/shard_map/ppermute | solution.py:26
  3.7 10.1 %collective-permute-start.4 = (bf16[128,640]{1,0:T(8,128)(2,1)}, bf16[128,640]{1,0:T(8,128)(2,1)S(1)}, u32[]{:S(2)}, u32[]{:S(2)}) collective-permute-start(bf16[128,640]{1,0:T(8,128)(2,1)} %get-tuple-element.22.k0), channel_id=1, source_target_pairs={{0,64},{96,160},{128,192},{224,288},{256,320},{352,416},{384,448},... | collective-permute-start | bytes 491528 | tf_op jit(solution)/shard_map/ppermute | solution.py:26
  8.9 7.3 %collective-permute-start.3 = (bf16[128,640]{1,0:T(8,128)(2,1)}, bf16[128,640]{1,0:T(8,128)(2,1)S(1)}, u32[]{:S(2)}, u32[]{:S(2)}) collective-permute-start(bf16[128,640]{1,0:T(8,128)(2,1)} %get-tuple-element.22.k0), channel_id=1, source_target_pairs={{0,32},{32,64},{96,128},{128,160},{160,192},{224,256},{256,288},{2... | collective-permute-start | bytes 491528 | tf_op jit(solution)/shard_map/ppermute | solution.py:26
  10.2 35.4 %copy-start.2 = (bf16[128,640]{1,0:T(8,128)(2,1)}, bf16[128,640]{1,0:T(8,128)(2,1)S(1)}, u32[]{:S(2)}) copy-start(bf16[128,640]{1,0:T(8,128)(2,1)S(1)} %collective-permute-done.5.k3) | copy-start | bytes 491524
  13.8 31.8 %copy-start.3 = (bf16[128,640]{1,0:T(8,128)(2,1)}, bf16[128,640]{1,0:T(8,128)(2,1)S(1)}, u32[]{:S(2)}) copy-start(bf16[128,640]{1,0:T(8,128)(2,1)S(1)} %collective-permute-done.4.k2) | copy-start | bytes 491524
  16.2 0.9 copy-start.1
  17.1 28.5 %copy-start.4 = (bf16[128,640]{1,0:T(8,128)(2,1)}, bf16[128,640]{1,0:T(8,128)(2,1)S(1)}, u32[]{:S(2)}) copy-start(bf16[128,640]{1,0:T(8,128)(2,1)S(1)} %collective-permute-done.3.k1) | copy-start | bytes 491524
  17.1 2.1 %copy-start.7 = (bf16[128,1408]{1,0:T(8,128)(2,1)S(1)}, bf16[128,1408]{1,0:T(8,128)(2,1)}, u32[]{:S(2)}) copy-start(bf16[128,1408]{1,0:T(8,128)(2,1)} %get-tuple-element.21.q0) | copy-start | bytes 1081348
  17.1 28.4 %collective-permute-start.6 = (bf16[4,128,640]{2,1,0:T(8,128)(2,1)S(1)}, bf16[4,128,640]{2,1,0:T(8,128)(2,1)S(1)}, u32[]{:S(2)}, u32[]{:S(2)}) collective-permute-start(bf16[4,128,640]{2,1,0:T(8,128)(2,1)S(1)} %shard_map.128), channel_id=1, source_target_pairs={{0,4},{4,0},{1,5},{5,1},{2,6},{6,2},{3,7},{7,3},{8,12},{12,8},{9,1... | collective-permute-start | bytes 1966088 | tf_op jit(solution)/shard_map/ppermute | solution.py:19
  19.2 20.7 %collective-permute-start.2 = (bf16[128,1408]{1,0:T(8,128)(2,1)S(1)}, bf16[128,1408]{1,0:T(8,128)(2,1)S(1)}, u32[]{:S(2)}, u32[]{:S(2)}) collective-permute-start(bf16[128,1408]{1,0:T(8,128)(2,1)S(1)} %copy-done.7), channel_id=1, source_target_pairs={{0,24},{8,0},{16,8},{24,16},{1,25},{9,1},{17,9},{25,17},{2,26},{10... | collective-permute-start | bytes 1081352 | tf_op jit(solution)/shard_map/ppermute | solution.py:19
  23.9 16.1 %collective-permute-start.1 = (bf16[128,1408]{1,0:T(8,128)(2,1)S(1)}, bf16[128,1408]{1,0:T(8,128)(2,1)S(1)}, u32[]{:S(2)}, u32[]{:S(2)}) collective-permute-start(bf16[128,1408]{1,0:T(8,128)(2,1)S(1)} %copy-done.7), channel_id=1, source_target_pairs={{0,16},{8,24},{16,0},{24,8},{1,17},{9,25},{17,1},{25,9},{2,18},{10... | collective-permute-start | bytes 1081352 | tf_op jit(solution)/shard_map/ppermute | solution.py:19
  26.6 18.9 %collective-permute-start = (bf16[128,1408]{1,0:T(8,128)(2,1)S(1)}, bf16[128,1408]{1,0:T(8,128)(2,1)S(1)}, u32[]{:S(2)}, u32[]{:S(2)}) collective-permute-start(bf16[128,1408]{1,0:T(8,128)(2,1)S(1)} %copy-done.7), channel_id=1, source_target_pairs={{0,8},{8,16},{16,24},{24,0},{1,9},{9,17},{17,25},{25,1},{2,10},{10... | collective-permute-start | bytes 1081352 | tf_op jit(solution)/shard_map/ppermute | solution.py:19
  39.9 5.6 %copy-start.8 = (bf16[128,1408]{1,0:T(8,128)(2,1)}, bf16[128,1408]{1,0:T(8,128)(2,1)S(1)}, u32[]{:S(2)}) copy-start(bf16[128,1408]{1,0:T(8,128)(2,1)S(1)} %collective-permute-done.2.q3) | copy-start | bytes 1081348
  39.9 5.6 %copy-start.9 = (bf16[128,1408]{1,0:T(8,128)(2,1)}, bf16[128,1408]{1,0:T(8,128)(2,1)S(1)}, u32[]{:S(2)}) copy-start(bf16[128,1408]{1,0:T(8,128)(2,1)S(1)} %collective-permute-done.1.q2) | copy-start | bytes 1081348
  45.5 0.8 copy-start.10
  46.3 0.8 copy-start.6
  62.8 21.9 %all-to-all-start = ((bf16[4,1280,128]{2,1,0:T(8,128)(2,1)}), bf16[4,1280,128]{2,1,0:T(8,128)(2,1)S(1)}, u32[]{:S(2)}, u32[]{:S(2)}) async-start(bf16[4,1280,128]{2,1,0:T(8,128)(2,1)} %get-tuple-element.23), calls=%async_computation | async-start | bytes 2621440 | tf_op jit(solution)/shard_map/all_to_all | solution.py:292
  66.4 39.9 %copy-start = (f32[4,576,128]{2,1,0:T(8,128)S(1)}, f32[4,576,128]{2,1,0:T(8,128)}, u32[]{:S(2)}) copy-start(f32[4,576,128]{2,1,0:T(8,128)} %get-tuple-element.26.mine) | copy-start | bytes 3538948
  66.4 39.8 %collective-permute-start.7 = (f32[4,576,128]{2,1,0:T(8,128)}, f32[4,576,128]{2,1,0:T(8,128)}, u32[]{:S(2)}, u32[]{:S(2)}) collective-permute-start(f32[4,576,128]{2,1,0:T(8,128)} %get-tuple-element.27), channel_id=1, source_target_pairs={{0,4},{4,0},{1,5},{5,1},{2,6},{6,2},{3,7},{7,3},{8,12},{12,8},{9,1... | collective-permute-start | bytes 3538952 | tf_op jit(solution)/shard_map/ppermute | solution.py:19
  85.5 3.2 %collective-permute-start.14 = (f32[4,64,128]{2,1,0:T(8,128)S(1)}, f32[4,64,128]{2,1,0:T(8,128)S(1)}, u32[]{:S(2)}, u32[]{:S(2)}) collective-permute-start(f32[4,64,128]{2,1,0:T(8,128)S(1)} %get-tuple-element.33), channel_id=1, source_target_pairs={{0,4},{4,0},{1,5},{5,1},{2,6},{6,2},{3,7},{7,3},{8,12},{12,8},{9,1... | collective-permute-start | bytes 393224 | tf_op jit(solution)/shard_map/ppermute | solution.py:19
  89.4 40.2 %all-to-all-start.1 = ((f32[4,64,128]{2,1,0:T(8,128)}), f32[4,64,128]{2,1,0:T(8,128)S(1)}, u32[]{:S(2)}, u32[]{:S(2)}) async-start(f32[4,64,128]{2,1,0:T(8,128)} %shard_map.132), calls=%async_computation.1 | async-start | bytes 262144 | tf_op jit(solution)/shard_map/all_to_all | solution.py:292
  107.6 62.8 %copy-start.5 = (s32[8]{0:T(128)S(1)}, s32[8]{0:T(128)}, u32[]{:S(2)}) copy-start(s32[8]{0:T(128)} %stack.47.info) | copy-start | bytes 100
  107.6 7.7 %collective-permute-start.8 = (bf16[576,128]{1,0:T(8,128)(2,1)S(1)}, bf16[576,128]{1,0:T(8,128)(2,1)S(1)}, u32[]{:S(2)}, u32[]{:S(2)}) collective-permute-start(bf16[576,128]{1,0:T(8,128)(2,1)S(1)} %get-tuple-element.29), channel_id=1, source_target_pairs={{32,0},{64,32},{128,96},{160,128},{192,160},{256,224},{288,256},{3... | collective-permute-start | bytes 442376 | tf_op jit(solution)/shard_map/ppermute | solution.py:26
  108.9 10.0 %collective-permute-start.9 = (bf16[576,128]{1,0:T(8,128)(2,1)S(1)}, bf16[576,128]{1,0:T(8,128)(2,1)S(1)}, u32[]{:S(2)}, u32[]{:S(2)}) collective-permute-start(bf16[576,128]{1,0:T(8,128)(2,1)S(1)} %get-tuple-element.30), channel_id=1, source_target_pairs={{64,0},{160,96},{192,128},{288,224},{320,256},{416,352},{448,384},... | collective-permute-start | bytes 442376 | tf_op jit(solution)/shard_map/ppermute | solution.py:26
  110.2 8.7 %collective-permute-start.10 = (bf16[576,128]{1,0:T(8,128)(2,1)S(1)}, bf16[576,128]{1,0:T(8,128)(2,1)S(1)}, u32[]{:S(2)}, u32[]{:S(2)}) collective-permute-start(bf16[576,128]{1,0:T(8,128)(2,1)S(1)} %get-tuple-element.31), channel_id=1, source_target_pairs={{192,96},{320,224},{448,352},{193,97},{321,225},{449,353},{194,98}... | collective-permute-start | bytes 442376 | tf_op jit(solution)/shard_map/ppermute | solution.py:26
  119.0 38.2 %collective-permute-start.13 = (f32[576,128]{1,0:T(8,128)S(1)}, f32[576,128]{1,0:T(8,128)S(1)}, u32[]{:S(2)}, u32[]{:S(2)}) collective-permute-start(f32[576,128]{1,0:T(8,128)S(1)} %shard_map.131.a0), channel_id=1, source_target_pairs={{0,3},{1,0},{2,1},{3,2},{4,7},{5,4},{6,5},{7,6},{8,11},{9,8},{10,9... | collective-permute-start | bytes 884744 | tf_op jit(solution)/shard_map/ppermute | solution.py:19
  121.3 35.8 %collective-permute-start.12 = (f32[576,128]{1,0:T(8,128)S(1)}, f32[576,128]{1,0:T(8,128)S(1)}, u32[]{:S(2)}, u32[]{:S(2)}) collective-permute-start(f32[576,128]{1,0:T(8,128)S(1)} %shard_map.131.a0), channel_id=1, source_target_pairs={{0,2},{1,3},{2,0},{3,1},{4,6},{5,7},{6,4},{7,5},{8,10},{9,11},{10,... | collective-permute-start | bytes 884744 | tf_op jit(solution)/shard_map/ppermute | solution.py:19
  125.8 31.3 %collective-permute-start.11 = (f32[576,128]{1,0:T(8,128)S(1)}, f32[576,128]{1,0:T(8,128)S(1)}, u32[]{:S(2)}, u32[]{:S(2)}) collective-permute-start(f32[576,128]{1,0:T(8,128)S(1)} %shard_map.131.a0), channel_id=1, source_target_pairs={{0,1},{1,2},{2,3},{3,0},{4,5},{5,6},{6,7},{7,4},{8,9},{9,10},{10,1... | collective-permute-start | bytes 884744 | tf_op jit(solution)/shard_map/ppermute | solution.py:19
  130.3 40.1 %all-to-all-start.2 = ((f32[4,32,128]{2,1,0:T(8,128)}), f32[4,32,128]{2,1,0:T(8,128)S(1)}, u32[]{:S(2)}, u32[]{:S(2)}) async-start(f32[4,32,128]{2,1,0:T(8,128)} %shard_map.133), calls=%async_computation.2 | async-start | bytes 131072 | tf_op jit(solution)/shard_map/all_to_all | solution.py:292

commit v3 on v2

--- a/solution.py
+++ b/solution.py
@@ -44,10 +44,11 @@
                 piece = value.astype(bf16).astype(f32)
                 value = value - piece
                 extra = jnp.where(lane == (h * 2 + k) * 3 + part, piece, extra)
-    qpack[:, 0:512] = qm[...]
-    qpack[:, 512:768] = qr[...]
-    qpack[:, 768:1280] = og[...]
-    qpack[:, 1280:1408] = extra.astype(bf16)
+    for i in range(qpack.shape[0]):
+        qpack[i, :, 0:512] = qm[...]
+        qpack[i, :, 512:768] = qr[...]
+        qpack[i, :, 768:1280] = og[...]
+        qpack[i, :, 1280:1408] = extra.astype(bf16)
     kpack[:, 0:512] = lat[...]
     kpack[:, 512:576] = rot[...].T
     kpack[:, 576:640] = jnp.zeros((toks, 64), bf16)
@@ -58,7 +59,7 @@
     return pl.pallas_call(
         pack_kernel,
         out_shape=(
-            jax.ShapeDtypeStruct((toks, 1408), bf16),
+            jax.ShapeDtypeStruct((4, toks, 1408), bf16),
             jax.ShapeDtypeStruct((toks, 640), bf16),
         ),
         name="pack",
@@ -66,98 +67,105 @@
 
 
 def attend_kernel(
-    info, q0, q1, q2, q3, k0, k1, k2, k3, kother, wk, wv,
+    info, qs, k0, k1, k2, k3, kother, wk, wv,
     back, mine, theirs,
-    qcur, kcur, q_s, qt_s, g_s, gt_s, log_s, term_s, acc, ds_acc, w_acc, wt_acc, back_s,
+    kcur, q_s, qt_s, g_s, gt_s, log_s, term_s, gap_s, acc, ds_acc, w_acc, wt_acc, back_s,
 ):
     heads, toks, width = 4, 128, 128
     factor = 192.0**-0.5
     my_x = info[3]
     my_c = info[4]
+
+    def whole(start, count):
+        return qs[:, :, start : start + count].reshape(GROUP * toks, count)
+
+    acc[...] = jnp.zeros_like(acc)
     ds_acc[...] = jnp.zeros_like(ds_acc)
     w_acc[...] = jnp.zeros_like(w_acc)
-    wt_acc[...] = jnp.zeros_like(wt_acc)
-    q_s[:, 576:640] = jnp.zeros((heads * toks, 64), bf16)
-
-    def chunk(g, _):
-        for i, ref in enumerate((q0, q1, q2, q3)):
-
-            @pl.when(g == i)
-            def _(ref=ref):
-                qcur[...] = ref[...]
-
-        extra = qcur[:, 1280:1408].astype(f32)
-        for h in range(heads):
-            rows = slice(h * toks, (h + 1) * toks)
-            cols = slice(h * width, (h + 1) * width)
-            qm_h = qcur[:, cols]
-            og_h = qcur[:, 768 + h * width : 768 + (h + 1) * width]
-            qr_h = qcur[:, 512 + h * 64 : 512 + (h + 1) * 64]
-            q_s[rows, 0:512] = dot(qm_h, wk[:, cols], ((1,), (1,))).astype(bf16)
-            qt_s[0:512, rows] = dot(wk[:, cols], qm_h, ((1,), (1,))).astype(bf16)
-            g_s[rows, :] = dot(og_h, wv[:, cols], ((1,), (1,))).astype(bf16)
-            gt_s[:, rows] = dot(wv[:, cols], og_h, ((1,), (1,))).astype(bf16)
-            q_s[rows, 512:576] = qr_h
-            qt_s[512:576, rows] = qr_h.T
+    shape = (2 * toks, 2 * toks)
+    gap_s[...] = (
+        lax.broadcasted_iota(jnp.int32, shape, 1) % toks
+        - lax.broadcasted_iota(jnp.int32, shape, 0) % toks
+    )
+    for i in range(GROUP):
+        q_s[i, :, 576:640] = jnp.zeros((heads * toks, 64), bf16)
+    for h in range(heads):
+        rows = slice(h * toks, (h + 1) * toks)
+        cols = slice(h * width, (h + 1) * width)
+        for at, w, plain, turned in ((0, wk, q_s, qt_s), (768, wv, g_s, gt_s)):
+            x_h = whole(at + h * width, width)
+            w_h = w[:, cols]
+            straight = dot(x_h, w_h, ((1,), (1,))).astype(bf16)
+            across = dot(w_h, x_h, ((1,), (1,))).astype(bf16)
+            for i in range(GROUP):
+                plain[i, rows, 0:512] = straight[i * toks : (i + 1) * toks, :]
+                turned[i, 0:512, rows] = across[:, i * toks : (i + 1) * toks]
+        for i in range(GROUP):
+            qr_h = qs[i, :, 512 + h * 64 : 512 + (h + 1) * 64]
+            q_s[i, rows, 512:576] = qr_h
+            qt_s[i, 512:576, rows] = qr_h.T
+            extra = qs[i, :, 1280:1408].astype(f32)
             for k, ref in enumerate((log_s, term_s)):
                 at = (h * 2 + k) * 3
                 value = extra[:, at : at + 1] + extra[:, at + 1 : at + 2] + extra[:, at + 2 : at + 3]
-                ref[rows, :] = jnp.broadcast_to(value, (toks, 128))
-        acc[...] = jnp.zeros_like(acc)
-        from_x = (my_x - g + GROUP) % GROUP
-
-        def plane(p, _):
-            useful = jnp.where(p == 0, from_x >= my_x, info[jnp.maximum(p - 1, 0)] == 1)
-
-            @pl.when(useful)
-            def _():
-                for i, ref in enumerate((k0, k1, k2, k3)):
-
-                    @pl.when(p == i)
-                    def _(ref=ref):
-                        kcur[0:toks, :] = ref[...]
-
-                kcur[toks : 2 * toks, :] = kother[p]
-                scores = dot(q_s[...], kcur[...], ((1,), (1,)))
-                slopes = dot(g_s[...], kcur[:, 0:512], ((1,), (1,)))
-                logs = jnp.concatenate([log_s[...]] * 2, axis=1)
-                terms = jnp.concatenate([term_s[...]] * 2, axis=1)
-                shape = scores.shape
-                row = lax.broadcasted_iota(jnp.int32, shape, 0) % toks
-                col = lax.broadcasted_iota(jnp.int32, shape, 1)
-                key_c = jnp.where(col < toks, my_c, 1 - my_c)
-                key_place = (my_x * 2 + key_c) * toks + col % toks
-                query_place = (from_x * 2 + my_c) * toks + row
-                query_place = query_place + jnp.where(p == 0, 0, 1 << 20)
-                weights = jnp.where(key_place <= query_place, jnp.exp(factor * scores - logs), 0.0)
-                dscores = (weights * (slopes - terms)).astype(bf16)
-                acc[...] += dot(dscores, kcur[...], ((1,), (0,)))
-                ds_acc[p] += dot(qt_s[...], dscores, ((1,), (0,)))
-                w_acc[p] += dot(gt_s[...], weights.astype(bf16), ((1,), (0,)))
-
-            return 0
-
-        lax.fori_loop(0, GROUP, plane, 0)
-        mains, rots = [], []
-        for h in range(heads):
-            rows = slice(h * toks, (h + 1) * toks)
-            cols = slice(h * width, (h + 1) * width)
-            mixed = acc[rows, 0:512]
-            high = mixed.astype(bf16)
-            low = (mixed - high.astype(f32)).astype(bf16)
-            w_h = wk[:, cols]
-            mains.append(factor * (dot(high, w_h, ((1,), (0,))) + dot(low, w_h, ((1,), (0,)))))
-            rots.append(factor * acc[rows, 512:576])
-            qm_h = qcur[:, cols]
-            wt_acc[cols, :] += dot(qm_h, high, ((0,), (0,))) + dot(qm_h, low, ((0,), (0,)))
-        for h in range(heads):
-            back_s[from_x, h * toks : (h + 1) * toks, :] = mains[h]
+                ref[i, rows, :] = jnp.broadcast_to(value, (toks, 128))
+
+    own_key = lax.broadcasted_iota(jnp.int32, (1, 2 * toks), 1) < toks
+    key_c = jnp.where(own_key, my_c, 1 - my_c)
+
+    def plane(p, _):
+        @pl.when((p == 0) | (info[jnp.maximum(p - 1, 0)] == 1))
+        def _():
+            for i, ref in enumerate((k0, k1, k2, k3)):
+
+                @pl.when(p == i)
+                def _(ref=ref):
+                    kcur[0:toks, :] = ref[...]
+
+            kcur[toks : 2 * toks, :] = kother[p]
+
+            def chunk(i, _):
+                ahead = ((i - my_x) * 2 + my_c - key_c) * toks
+                limit = ahead + jnp.where(p == 0, 0, 1 << 20)
+                lows, slopes_low = [], []
+                for half in range(2):
+                    rows = slice(half * 2 * toks, (half + 1) * 2 * toks)
+                    scores = dot(q_s[i, rows, :], kcur[...], ((1,), (1,)))
+                    slopes = dot(g_s[i, rows, :], kcur[:, 0:512], ((1,), (1,)))
+                    logs = jnp.concatenate([log_s[i, rows, :]] * 2, axis=1)
+                    terms = jnp.concatenate([term_s[i, rows, :]] * 2, axis=1)
+                    weights = jnp.exp(factor * scores - logs)
+                    weights = jnp.where(gap_s[...] <= limit, weights, 0.0)
+                    dscores = (weights * (slopes - terms)).astype(bf16)
+                    acc[i, rows, :] += dot(dscores, kcur[...], ((1,), (0,)))
+                    lows.append(weights.astype(bf16))
+                    slopes_low.append(dscores)
+                ds_acc[p] += dot(qt_s[i], jnp.concatenate(slopes_low, axis=0), ((1,), (0,)))
+                w_acc[p] += dot(gt_s[i], jnp.concatenate(lows, axis=0), ((1,), (0,)))
+                return 0
+
+            lax.fori_loop(jnp.where(p == 0, my_x, 0), GROUP, chunk, 0)
+
+        return 0
+
+    lax.fori_loop(0, GROUP, plane, 0)
+    for h in range(heads):
+        rows = slice(h * toks, (h + 1) * toks)
+        cols = slice(h * width, (h + 1) * width)
+        mixed = acc[:, rows, 0:512].reshape(GROUP * toks, 512)
+        high = mixed.astype(bf16)
+        low = (mixed - high.astype(f32)).astype(bf16)
+        w_h = wk[:, cols]
+        main = factor * (dot(high, w_h, ((1,), (0,))) + dot(low, w_h, ((1,), (0,))))
+        x_h = whole(h * width, width)
+        wt_acc[cols, :] = dot(x_h, high, ((0,), (0,))) + dot(x_h, low, ((0,), (0,)))
+        for i in range(GROUP):
+            back_s[i, rows, :] = main[i * toks : (i + 1) * toks, :]
+    for i in range(GROUP):
         for h in range(2):
-            pair = jnp.concatenate(rots[2 * h : 2 * h + 2], axis=1)
-            back_s[from_x, (heads + h) * toks : (heads + h + 1) * toks, :] = pair
-        return 0
-
-    lax.fori_loop(0, GROUP, chunk, 0)
+            pair = [acc[i, (2 * h + k) * toks : (2 * h + k + 1) * toks, 512:576] for k in range(2)]
+            rows = slice((heads + h) * toks, (heads + h + 1) * toks)
+            back_s[i, rows, :] = factor * jnp.concatenate(pair, axis=1)
     for p in range(GROUP):
         for rows in (slice(0, 512), slice(512, 576)):
             both = factor * ds_acc[p, rows, :]
@@ -192,7 +200,7 @@
     vmem = pl.BlockSpec(memory_space=pltpu.VMEM)
     return pl.pallas_call(
         attend_kernel,
-        in_specs=[pl.BlockSpec(memory_space=pltpu.SMEM)] + [vmem] * 11,
+        in_specs=[pl.BlockSpec(memory_space=pltpu.SMEM)] + [vmem] * 8,
         out_specs=[vmem] * 3,
         out_shape=[
             out((4, 1280, 128), bf16),
@@ -200,23 +208,23 @@
             out((GROUP, 576, toks), f32),
         ],
         scratch_shapes=[
-            pltpu.VMEM((toks, 1408), bf16),
             pltpu.VMEM((2 * toks, 640), bf16),
-            pltpu.VMEM((512, 640), bf16),
-            pltpu.VMEM((576, 512), bf16),
-            pltpu.VMEM((512, 512), bf16),
-            pltpu.VMEM((512, 512), bf16),
-            pltpu.VMEM((512, 128), f32),
-            pltpu.VMEM((512, 128), f32),
-            pltpu.VMEM((512, 640), f32),
+            pltpu.VMEM((GROUP, 512, 640), bf16),
+            pltpu.VMEM((GROUP, 576, 512), bf16),
+            pltpu.VMEM((GROUP, 512, 512), bf16),
+            pltpu.VMEM((GROUP, 512, 512), bf16),
+            pltpu.VMEM((GROUP, 512, 128), f32),
+            pltpu.VMEM((GROUP, 512, 128), f32),
+            pltpu.VMEM((2 * toks, 2 * toks), jnp.int32),
+            pltpu.VMEM((GROUP, 512, 640), f32),
             pltpu.VMEM((GROUP, 576, 2 * toks), f32),
             pltpu.VMEM((GROUP, 512, 2 * toks), f32),
             pltpu.VMEM((512, 512), f32),
             pltpu.VMEM((4, 1280, 128), f32),
         ],
-        compiler_params=pltpu.CompilerParams(vmem_limit_bytes=60 << 20),
+        compiler_params=pltpu.CompilerParams(vmem_limit_bytes=52 << 20),
         name="attend",
-    )(info, *qs, *ks, kother, wk, wv)
+    )(info, qs, *ks, kother, wk, wv)
 
 
 def local(body, shapes, *args, scalars=0, scratch=(), aliases=None):
@@ -277,10 +285,8 @@
             far[2 * pair + 1, k * 8 : k * 8 + 8, :] = pltpu.roll(tile, 4, 0)
 
 
-def last_kernel(info, a0, a1, a2, a3, far, lat, rot, weight, keys):
-    for s, a in enumerate((a0, a1, a2, a3)):
-        keys[(info[6] - s + 4) % 4] = a[...]
-    total = added([keys[y] for y in range(4)])
+def last_kernel(keys, other_keys, far, lat, rot, weight):
+    total = keys[...] + other_keys[...]
     lat[...] = total[0:512, :].T
     rot[...] = total[512:576, :]
     for k in range(4):
@@ -288,15 +294,13 @@
         weight[:, k * 128 : (k + 1) * 128] = part
 
 
+def swap(block, axis, bit):
+    pairs = [(i, i ^ bit) for i in range(lax.axis_size(axis))]
+    return lax.ppermute(block, axis, pairs)
+
+
 def exchange(tiles, axis, groups=None):
     return lax.all_to_all(tiles, axis, 0, 0, tiled=True, axis_index_groups=groups)
-
-
-def spread(blocks, axis):
-    got = [blocks[0]]
-    for s in range(1, 4):
-        got.append(shift(blocks[s], axis, s))
-    return got
 
 
 def per_device(
@@ -316,15 +320,14 @@
     flags = [
         ((my_z >= s) & ((my_z - s + 1) // GROUP == seq)).astype(jnp.int32) for s in range(1, GROUP)
     ]
-    turns = [my_x, my_c, (my_z + 1) % GROUP, lax.axis_index(Y), seq % 4]
-    info = jnp.stack([*flags, *turns]).astype(jnp.int32)
+    info = jnp.stack([*flags, my_x, my_c]).astype(jnp.int32)
     qpack, kpack = pack(
         query_main, query_rotary, output_grad, head_output, row_logsum, latent, key_rotary.T
     )
     ks = [kpack]
     for s in range(1, GROUP):
         ks.append(onward(kpack, s))
-    qs = spread([qpack] * 4, X)
+    qs = exchange(qpack, X)
     (stacked,) = local(stack_kernel, [((4, *kpack.shape), bf16)], *ks)
     kother = shift(stacked, C, 1)
     back, mine, theirs = attend(info, qs, ks, kother, key_weight, value_weight)
@@ -343,14 +346,13 @@
     near = [[(4 * g + b - 1) % 16 for b in range(4)] for g in range(4)]
     weight = exchange(weight, Z, near)
     (key,) = local(key_kernel, [((576, 128), f32)], *planes)
-    keys = spread([key] * 4, Y)
+    beside = swap(key, Y, 1)
+    (key,) = local(weight_kernel, [((576, 128), f32)], key, beside)
+    across = swap(key, Y, 2)
     (weight,) = local(far_kernel, [((4, 32, 128), f32)], weight)
     weight = exchange(weight, Z, [list(z) for z in zip(*near)])
     shapes = [((toks, 512), f32), ((64, toks), f32), ((4, 512), f32)]
-    lat, rot, weight = local(
-        last_kernel, shapes, info, *keys, weight,
-        scalars=1, scratch=[pltpu.VMEM((4, 576, 128), f32)],
-    )
+    lat, rot, weight = local(last_kernel, shapes, key, across, weight)
     return main, rotary, lat, rot.T, weight
 
 

time: 173 us -> 140 us (0.81)
  starting transfers between devices: 84.4 us -> 48.7 us
  blocking collectives: 0 us -> 35.5 us
  waiting for transfers between devices: 60.2 us -> 33.6 us
  local copies, waits for them, and re-layouts: 3.12 us -> 0.11 us
  Pallas kernels: 23.1 us -> 20.5 us
    all_to_all x0 -> x1, blocking collectives: none -> 35.5 us  [exchange(): lax.all_to_all(tiles, axis, 0, 0, tiled=True, axis_index_groups=groups)]
    all_to_all x3, starting transfers between devices: 47.2 us -> 25.9 us  [exchange(): lax.all_to_all(tiles, axis, 0, 0, tiled=True, axis_index_groups=groups)]
    ppermute x9 -> x3, starting transfers between devices: 26.9 us -> 5.74 us  [shift(): lax.ppermute(block, axis, [(i, (i + by) % peers) for i in range(peers)])]
    ppermute x9 -> x3, waiting for transfers between devices: 16.7 us -> 3.22 us  [shift(): lax.ppermute(block, axis, [(i, (i + by) % peers) for i in range(peers)])]
    all_to_all x3, waiting for transfers between devices: 29.5 us -> 16.7 us  [exchange(): lax.all_to_all(tiles, axis, 0, 0, tiled=True, axis_index_groups=groups)]
    ppermute x6, waiting for transfers between devices: 14 us -> 5.68 us  [onward(): return lax.ppermute(block, Z, pairs)]
    ppermute x0 -> x2, waiting for transfers between devices: none -> 8.03 us  [swap(): return lax.ppermute(block, axis, pairs)]
    ppermute x0 -> x2, starting transfers between devices: none -> 6.54 us  [swap(): return lax.ppermute(block, axis, pairs)]
  transfers between devices with their start and end apart: 18 -> 14, of which waited for: 9 -> 7; matrix products, arithmetic and copies ran while one was open for 0% -> 0% of each run, Pallas kernels for 2% -> 2%
where the time goes in v3:
time: 140 us; the launch traced here: 139 us
  starting transfers between devices  48.7 us (35%)
  blocking collectives  35.5 us (25%)
  waiting for transfers between devices  33.6 us (24%)
  Pallas kernels  20.5 us (15%)
    all_to_all x1, blocking collectives, exchange(): lax.all_to_all(tiles, axis, 0, 0, tiled=True, axis_index_groups=groups)  35.5 us
    all_to_all x3, starting transfers between devices, exchange(): lax.all_to_all(tiles, axis, 0, 0, tiled=True, axis_index_groups=groups)  25.9 us
    all_to_all x3, waiting for transfers between devices, exchange(): lax.all_to_all(tiles, axis, 0, 0, tiled=True, axis_index_groups=groups)  16.7 us
    pallas_call x1, Pallas kernels, attend(): pl.pallas_call(attend_kernel, in_specs=[pl.BlockSpec(memory_space=pltpu.S...  13.8 us
    ppermute x6, starting transfers between devices, onward(): return lax.ppermute(block, Z, pairs)  10.5 us
    ppermute x2, waiting for transfers between devices, swap(): return lax.ppermute(block, axis, pairs)  8.03 us
    ppermute x2, starting transfers between devices, swap(): return lax.ppermute(block, axis, pairs)  6.54 us
    ppermute x3, starting transfers between devices, shift(): lax.ppermute(block, axis, [(i, (i + by) % peers) for i in range(peers)])  5.74 us
  transfers between devices with their start and end apart: 14, of which 7 were waited for; matrix products, arithmetic and copies ran while one was open for 0% of the time, Pallas kernels for 2%

profile of v3, /device:TPU:8, one launch (start us, length us, event | category | flops | bytes accessed | tf_op | source)
XLA Modules:
  0.0 139.4 jit_solution(6880113255458073052)
XLA Ops:
  0.6 2.8 %pack.1 = (bf16[4,128,1408]{2,1,0:T(8,128)(2,1)}, bf16[128,640]{1,0:T(8,128)(2,1)}) custom-call(bf16[128,512]{1,0:T(8,128)(2,1)} %qm.1, bf16[128,256]{1,0:T(8,128)(2,1)} %qr.1, bf16[128,512]{1,0:T(8,128)(2,1)} %og.1, bf16[128,512]{1,0:T(8,128)(2,1)} %ho.1, f32[4,128]{1,0:T(4,128)} %logs.1, bf16[128,512]{1,0:T(8,128)(2,1)} %lat.1, bf16[64,128]{1,0:T(8,128)(2,1)} %bitcast.7), custom_call_target="tpu_custom_call" | custom-call | tf_op jit(solution)/shard_map/pack/pallas_call | solution.py:59
  3.4 0.0 copy-start.1
  3.4 4.4 %all-to-all-start = ((bf16[4,128,1408]{2,1,0:T(8,128)(2,1)}), bf16[4,128,1408]{2,1,0:T(8,128)(2,1)}, u32[]{:S(2)}, u32[]{:S(2)}) async-start(bf16[4,128,1408]{2,1,0:T(8,128)(2,1)} %get-tuple-element.21), calls=%async_computation | async-start | bytes 2883584 | tf_op jit(solution)/shard_map/all_to_all | solution.py:303
  7.9 0.0 copy-start.2
  7.9 0.0 copy-start.3
  7.9 0.0 copy-done.1
  7.9 0.8 collective-permute-start.2
  8.7 5.2 %collective-permute-start.1 = (bf16[128,640]{1,0:T(8,128)(2,1)S(1)}, bf16[128,640]{1,0:T(8,128)(2,1)S(1)}, u32[]{:S(2)}, u32[]{:S(2)}) collective-permute-start(bf16[128,640]{1,0:T(8,128)(2,1)S(1)} %copy-done.1), channel_id=1, source_target_pairs={{0,64},{96,160},{128,192},{224,288},{256,320},{352,416},{384,448},... | collective-permute-start | bytes 491528 | tf_op jit(solution)/shard_map/ppermute | solution.py:26
  13.9 1.3 collective-permute-start
  15.2 0.0 collective-permute-done.2.k3
  15.2 3.3 %collective-permute-done.1.k2 = bf16[128,640]{1,0:T(8,128)(2,1)S(1)} collective-permute-done((bf16[128,640]{1,0:T(8,128)(2,1)S(1)}, bf16[128,640]{1,0:T(8,128)(2,1)S(1)}, u32[]{:S(2)}, u32[]{:S(2)}) %collective-permute-start.1) | collective-permute-done | bytes 163872 | tf_op jit(solution)/shard_map/ppermute | solution.py:26
  18.5 2.4 %collective-permute-done.k1 = bf16[128,640]{1,0:T(8,128)(2,1)S(1)} collective-permute-done((bf16[128,640]{1,0:T(8,128)(2,1)S(1)}, bf16[128,640]{1,0:T(8,128)(2,1)S(1)}, u32[]{:S(2)}, u32[]{:S(2)}) %collective-permute-start) | collective-permute-done | bytes 163872 | tf_op jit(solution)/shard_map/ppermute | solution.py:26
  20.9 0.1 shard_map.128
  20.9 1.9 %collective-permute-start.3 = (bf16[4,128,640]{2,1,0:T(8,128)(2,1)S(1)}, bf16[4,128,640]{2,1,0:T(8,128)(2,1)S(1)}, u32[]{:S(2)}, u32[]{:S(2)}) collective-permute-start(bf16[4,128,640]{2,1,0:T(8,128)(2,1)S(1)} %shard_map.128), channel_id=1, source_target_pairs={{0,4},{4,0},{1,5},{5,1},{2,6},{6,2},{3,7},{7,3},{8,12},{12,8},{9,1... | collective-permute-start | bytes 1966088 | tf_op jit(solution)/shard_map/ppermute | solution.py:19
  22.9 0.1 stack.35.info
  23.0 1.9 %collective-permute-done.3.kother = bf16[4,128,640]{2,1,0:T(8,128)(2,1)S(1)} collective-permute-done((bf16[4,128,640]{2,1,0:T(8,128)(2,1)S(1)}, bf16[4,128,640]{2,1,0:T(8,128)(2,1)S(1)}, u32[]{:S(2)}, u32[]{:S(2)}) %collective-permute-start.3) | collective-permute-done | bytes 655392 | tf_op jit(solution)/shard_map/ppermute | solution.py:19
  24.9 0.0 copy-start.4
  24.9 2.6 %all-to-all-done.qs = bf16[4,128,1408]{2,1,0:T(8,128)(2,1)} async-done(((bf16[4,128,1408]{2,1,0:T(8,128)(2,1)}), bf16[4,128,1408]{2,1,0:T(8,128)(2,1)}, u32[]{:S(2)}, u32[]{:S(2)}) %all-to-all-start) | async-done | bytes 1441824 | tf_op jit(solution)/shard_map/all_to_all | solution.py:303
  27.5 0.0 copy-done.4
  27.5 0.0 copy-done.2
  27.5 0.0 copy-done.3
  27.5 13.8 %attend.1 = (bf16[4,1280,128]{2,1,0:T(8,128)(2,1)}, f32[4,576,128]{2,1,0:T(8,128)}, f32[4,576,128]{2,1,0:T(8,128)}) custom-call(s32[5]{0:T(128)S(1)} %stack.35.info, bf16[4,128,1408]{2,1,0:T(8,128)(2,1)} %all-to-all-done.qs, bf16[128,640]{1,0:T(8,128)(2,1)S(1)} %copy-done.1, bf16[128,640]{1,0:T(8,128)(2,1)S(1)} %collective-permute-done.k1, ...), custom_call_target="tpu_custom_call" | custom-call | tf_op jit(solution)/shard_map/attend/pallas_call | solution.py:201
  41.4 1.9 %collective-permute-start.4 = (f32[4,576,128]{2,1,0:T(8,128)}, f32[4,576,128]{2,1,0:T(8,128)}, u32[]{:S(2)}, u32[]{:S(2)}) collective-permute-start(f32[4,576,128]{2,1,0:T(8,128)} %get-tuple-element.27), channel_id=1, source_target_pairs={{0,4},{4,0},{1,5},{5,1},{2,6},{6,2},{3,7},{7,3},{8,12},{12,8},{9,1... | collective-permute-start | bytes 3538952 | tf_op jit(solution)/shard_map/ppermute | solution.py:19
  43.3 0.0 copy-start
  43.3 3.7 %all-to-all-start.1 = ((bf16[4,1280,128]{2,1,0:T(8,128)(2,1)}), bf16[4,1280,128]{2,1,0:T(8,128)(2,1)S(1)}, u32[]{:S(2)}, u32[]{:S(2)}) async-start(bf16[4,1280,128]{2,1,0:T(8,128)(2,1)} %get-tuple-element.23), calls=%async_computation.1 | async-start | bytes 2621440 | tf_op jit(solution)/shard_map/all_to_all | solution.py:303
  47.0 0.0 collective-permute-done.4.theirs
  47.0 0.0 copy-done
  47.0 1.4 shard_map.130
  48.4 1.3 collective-permute-start.5
  49.7 1.3 collective-permute-start.6
  51.0 0.7 collective-permute-start.7
  51.7 14.1 %all-to-all-done.1.back = bf16[4,1280,128]{2,1,0:T(8,128)(2,1)S(1)} async-done(((bf16[4,1280,128]{2,1,0:T(8,128)(2,1)}), bf16[4,1280,128]{2,1,0:T(8,128)(2,1)S(1)}, u32[]{:S(2)}, u32[]{:S(2)}) %all-to-all-start.1) | async-done | bytes 1310752 | tf_op jit(solution)/shard_map/all_to_all | solution.py:303
  65.8 0.8 shard_map.129
  66.6 1.9 %collective-permute-start.10 = (f32[4,64,128]{2,1,0:T(8,128)S(1)}, f32[4,64,128]{2,1,0:T(8,128)S(1)}, u32[]{:S(2)}, u32[]{:S(2)}) collective-permute-start(f32[4,64,128]{2,1,0:T(8,128)S(1)} %get-tuple-element.33), channel_id=1, source_target_pairs={{0,4},{4,0},{1,5},{5,1},{2,6},{6,2},{3,7},{7,3},{8,12},{12,8},{9,1... | collective-permute-start | bytes 393224 | tf_op jit(solution)/shard_map/ppermute | solution.py:19
  68.5 1.3 collective-permute-done.10.theirs
  69.8 0.7 shard_map.133
  70.5 17.8 %all-to-all-start.2 = ((f32[4,64,128]{2,1,0:T(8,128)}), f32[4,64,128]{2,1,0:T(8,128)S(1)}, u32[]{:S(2)}, u32[]{:S(2)}) async-start(f32[4,64,128]{2,1,0:T(8,128)} %shard_map.133), calls=%async_computation.2 | async-start | bytes 262144 | tf_op jit(solution)/shard_map/all_to_all | solution.py:303
  88.3 0.0 collective-permute-done.5.z1
  88.3 0.0 collective-permute-done.6.z2
  88.3 0.0 collective-permute-done.7.z3
  88.3 0.1 shard_map.131.mine
  88.4 2.4 %collective-permute-start.8 = (f32[576,128]{1,0:T(8,128)S(1)}, f32[576,128]{1,0:T(8,128)S(1)}, u32[]{:S(2)}, u32[]{:S(2)}) collective-permute-start(f32[576,128]{1,0:T(8,128)S(1)} %shard_map.131.mine), channel_id=1, source_target_pairs={{0,1},{1,0},{2,3},{3,2},{4,5},{5,4},{6,7},{7,6},{8,9},{9,8},{10,11... | collective-permute-start | bytes 884744 | tf_op jit(solution)/shard_map/ppermute | solution.py:299
  90.8 8.0 %collective-permute-done.8.theirs = f32[576,128]{1,0:T(8,128)S(1)} collective-permute-done((f32[576,128]{1,0:T(8,128)S(1)}, f32[576,128]{1,0:T(8,128)S(1)}, u32[]{:S(2)}, u32[]{:S(2)}) %collective-permute-start.8) | collective-permute-done | bytes 294944 | tf_op jit(solution)/shard_map/ppermute | solution.py:299
  98.8 4.2 %collective-permute-start.9 = (f32[576,128]{1,0:T(8,128)S(1)}, f32[576,128]{1,0:T(8,128)S(1)}, u32[]{:S(2)}, u32[]{:S(2)}) collective-permute-start(f32[576,128]{1,0:T(8,128)S(1)} %shard_map.132.keys), channel_id=1, source_target_pairs={{0,2},{1,3},{2,0},{3,1},{4,6},{5,7},{6,4},{7,5},{8,10},{9,11},{10,... | collective-permute-start | bytes 884744 | tf_op jit(solution)/shard_map/ppermute | solution.py:299
  103.0 0.0 all-to-all-done.2.near
  103.0 35.5 %all_to_all.20.far = f32[4,32,128]{2,1,0:T(8,128)S(1)} all-to-all(f32[4,32,128]{2,1,0:T(8,128)S(1)} %shard_map.134), channel_id=1, replica_groups={{480,96,224,352},{0,128,256,384},{32,160,288,416},{64,192,320,448},{481..., dimensions={0} | all-to-all | bytes 131072 | tf_op jit(solution)/shard_map/all_to_all | solution.py:303
  138.5 0.0 collective-permute-done.9.other_keys
  138.5 0.8 shard_map.135
  (2 shorter events, 0.0 us)
Async XLA Ops:
  3.4 4.5 %copy-start.1 = (bf16[128,640]{1,0:T(8,128)(2,1)S(1)}, bf16[128,640]{1,0:T(8,128)(2,1)}, u32[]{:S(2)}) copy-start(bf16[128,640]{1,0:T(8,128)(2,1)} %get-tuple-element.22.k0) | copy-start | bytes 491524
  3.4 24.1 %all-to-all-start = ((bf16[4,128,1408]{2,1,0:T(8,128)(2,1)}), bf16[4,128,1408]{2,1,0:T(8,128)(2,1)}, u32[]{:S(2)}, u32[]{:S(2)}) async-start(bf16[4,128,1408]{2,1,0:T(8,128)(2,1)} %get-tuple-element.21), calls=%async_computation | async-start | bytes 2883584 | tf_op jit(solution)/shard_map/all_to_all | solution.py:303
  7.9 19.7 %copy-start.2 = (bf16[512,512]{1,0:T(8,128)(2,1)S(1)}, bf16[512,512]{1,0:T(8,128)(2,1)}, u32[]{:S(2)}) copy-start(bf16[512,512]{1,0:T(8,128)(2,1)} %wk.1) | copy-start | bytes 1572868
  7.9 19.6 %copy-start.3 = (bf16[512,512]{1,0:T(8,128)(2,1)S(1)}, bf16[512,512]{1,0:T(8,128)(2,1)}, u32[]{:S(2)}) copy-start(bf16[512,512]{1,0:T(8,128)(2,1)} %wv.1) | copy-start | bytes 1572868
  7.9 7.3 %collective-permute-start.2 = (bf16[128,640]{1,0:T(8,128)(2,1)S(1)}, bf16[128,640]{1,0:T(8,128)(2,1)S(1)}, u32[]{:S(2)}, u32[]{:S(2)}) collective-permute-start(bf16[128,640]{1,0:T(8,128)(2,1)S(1)} %copy-done.1), channel_id=1, source_target_pairs={{96,192},{224,320},{352,448},{97,193},{225,321},{353,449},{98,194}... | collective-permute-start | bytes 491528 | tf_op jit(solution)/shard_map/ppermute | solution.py:26
  8.7 9.8 %collective-permute-start.1 = (bf16[128,640]{1,0:T(8,128)(2,1)S(1)}, bf16[128,640]{1,0:T(8,128)(2,1)S(1)}, u32[]{:S(2)}, u32[]{:S(2)}) collective-permute-start(bf16[128,640]{1,0:T(8,128)(2,1)S(1)} %copy-done.1), channel_id=1, source_target_pairs={{0,64},{96,160},{128,192},{224,288},{256,320},{352,416},{384,448},... | collective-permute-start | bytes 491528 | tf_op jit(solution)/shard_map/ppermute | solution.py:26
  13.9 7.0 %collective-permute-start = (bf16[128,640]{1,0:T(8,128)(2,1)S(1)}, bf16[128,640]{1,0:T(8,128)(2,1)S(1)}, u32[]{:S(2)}, u32[]{:S(2)}) collective-permute-start(bf16[128,640]{1,0:T(8,128)(2,1)S(1)} %copy-done.1), channel_id=1, source_target_pairs={{0,32},{32,64},{96,128},{128,160},{160,192},{224,256},{256,288},{2... | collective-permute-start | bytes 491528 | tf_op jit(solution)/shard_map/ppermute | solution.py:26
  20.9 4.0 %collective-permute-start.3 = (bf16[4,128,640]{2,1,0:T(8,128)(2,1)S(1)}, bf16[4,128,640]{2,1,0:T(8,128)(2,1)S(1)}, u32[]{:S(2)}, u32[]{:S(2)}) collective-permute-start(bf16[4,128,640]{2,1,0:T(8,128)(2,1)S(1)} %shard_map.128), channel_id=1, source_target_pairs={{0,4},{4,0},{1,5},{5,1},{2,6},{6,2},{3,7},{7,3},{8,12},{12,8},{9,1... | collective-permute-start | bytes 1966088 | tf_op jit(solution)/shard_map/ppermute | solution.py:19
  24.9 2.6 %copy-start.4 = (bf16[4,128,640]{2,1,0:T(8,128)(2,1)}, bf16[4,128,640]{2,1,0:T(8,128)(2,1)S(1)}, u32[]{:S(2)}) copy-start(bf16[4,128,640]{2,1,0:T(8,128)(2,1)S(1)} %collective-permute-done.3.kother) | copy-start | bytes 1966084
  41.4 5.6 %collective-permute-start.4 = (f32[4,576,128]{2,1,0:T(8,128)}, f32[4,576,128]{2,1,0:T(8,128)}, u32[]{:S(2)}, u32[]{:S(2)}) collective-permute-start(f32[4,576,128]{2,1,0:T(8,128)} %get-tuple-element.27), channel_id=1, source_target_pairs={{0,4},{4,0},{1,5},{5,1},{2,6},{6,2},{3,7},{7,3},{8,12},{12,8},{9,1... | collective-permute-start | bytes 3538952 | tf_op jit(solution)/shard_map/ppermute | solution.py:19
  43.3 3.7 %copy-start = (f32[4,576,128]{2,1,0:T(8,128)S(1)}, f32[4,576,128]{2,1,0:T(8,128)}, u32[]{:S(2)}) copy-start(f32[4,576,128]{2,1,0:T(8,128)} %get-tuple-element.26.mine) | copy-start | bytes 3538948
  43.3 22.5 %all-to-all-start.1 = ((bf16[4,1280,128]{2,1,0:T(8,128)(2,1)}), bf16[4,1280,128]{2,1,0:T(8,128)(2,1)S(1)}, u32[]{:S(2)}, u32[]{:S(2)}) async-start(bf16[4,1280,128]{2,1,0:T(8,128)(2,1)} %get-tuple-element.23), calls=%async_computation.1 | async-start | bytes 2621440 | tf_op jit(solution)/shard_map/all_to_all | solution.py:303
  48.4 39.9 %collective-permute-start.5 = (bf16[576,128]{1,0:T(8,128)(2,1)S(1)}, bf16[576,128]{1,0:T(8,128)(2,1)S(1)}, u32[]{:S(2)}, u32[]{:S(2)}) collective-permute-start(bf16[576,128]{1,0:T(8,128)(2,1)S(1)} %get-tuple-element.29), channel_id=1, source_target_pairs={{32,0},{64,32},{128,96},{160,128},{192,160},{256,224},{288,256},{3... | collective-permute-start | bytes 442376 | tf_op jit(solution)/shard_map/ppermute | solution.py:26
  49.7 38.6 %collective-permute-start.6 = (bf16[576,128]{1,0:T(8,128)(2,1)S(1)}, bf16[576,128]{1,0:T(8,128)(2,1)S(1)}, u32[]{:S(2)}, u32[]{:S(2)}) collective-permute-start(bf16[576,128]{1,0:T(8,128)(2,1)S(1)} %get-tuple-element.30), channel_id=1, source_target_pairs={{64,0},{160,96},{192,128},{288,224},{320,256},{416,352},{448,384},... | collective-permute-start | bytes 442376 | tf_op jit(solution)/shard_map/ppermute | solution.py:26
  51.0 37.3 %collective-permute-start.7 = (bf16[576,128]{1,0:T(8,128)(2,1)S(1)}, bf16[576,128]{1,0:T(8,128)(2,1)S(1)}, u32[]{:S(2)}, u32[]{:S(2)}) collective-permute-start(bf16[576,128]{1,0:T(8,128)(2,1)S(1)} %get-tuple-element.31), channel_id=1, source_target_pairs={{192,96},{320,224},{448,352},{193,97},{321,225},{449,353},{194,98}... | collective-permute-start | bytes 442376 | tf_op jit(solution)/shard_map/ppermute | solution.py:26
  66.6 3.2 %collective-permute-start.10 = (f32[4,64,128]{2,1,0:T(8,128)S(1)}, f32[4,64,128]{2,1,0:T(8,128)S(1)}, u32[]{:S(2)}, u32[]{:S(2)}) collective-permute-start(f32[4,64,128]{2,1,0:T(8,128)S(1)} %get-tuple-element.33), channel_id=1, source_target_pairs={{0,4},{4,0},{1,5},{5,1},{2,6},{6,2},{3,7},{7,3},{8,12},{12,8},{9,1... | collective-permute-start | bytes 393224 | tf_op jit(solution)/shard_map/ppermute | solution.py:19
  70.5 32.5 %all-to-all-start.2 = ((f32[4,64,128]{2,1,0:T(8,128)}), f32[4,64,128]{2,1,0:T(8,128)S(1)}, u32[]{:S(2)}, u32[]{:S(2)}) async-start(f32[4,64,128]{2,1,0:T(8,128)} %shard_map.133), calls=%async_computation.2 | async-start | bytes 262144 | tf_op jit(solution)/shard_map/all_to_all | solution.py:303
  88.4 10.4 %collective-permute-start.8 = (f32[576,128]{1,0:T(8,128)S(1)}, f32[576,128]{1,0:T(8,128)S(1)}, u32[]{:S(2)}, u32[]{:S(2)}) collective-permute-start(f32[576,128]{1,0:T(8,128)S(1)} %shard_map.131.mine), channel_id=1, source_target_pairs={{0,1},{1,0},{2,3},{3,2},{4,5},{5,4},{6,7},{7,6},{8,9},{9,8},{10,11... | collective-permute-start | bytes 884744 | tf_op jit(solution)/shard_map/ppermute | solution.py:299
  98.8 39.7 %collective-permute-start.9 = (f32[576,128]{1,0:T(8,128)S(1)}, f32[576,128]{1,0:T(8,128)S(1)}, u32[]{:S(2)}, u32[]{:S(2)}) collective-permute-start(f32[576,128]{1,0:T(8,128)S(1)} %shard_map.132.keys), channel_id=1, source_target_pairs={{0,2},{1,3},{2,0},{3,1},{4,6},{5,7},{6,4},{7,5},{8,10},{9,11},{10,... | collective-permute-start | bytes 884744 | tf_op jit(solution)/shard_map/ppermute | solution.py:299

commit v4 on v3

--- a/solution.py
+++ b/solution.py
@@ -184,9 +184,7 @@
                 even = jnp.where(upper, one, pltpu.roll(two, 4, 0))
                 odd = jnp.where(upper, pltpu.roll(one, 4, 0), two)
                 at = 768 + (b * 2 + pair) * 32
-                for first, tile in enumerate(
-                    (jnp.where(my_c == 0, even, odd), jnp.where(my_c == 0, odd, even))
-                ):
+                for first, tile in enumerate((even, odd)):
                     for k in range(4):
                         lanes = slice(k * 128, (k + 1) * 128)
                         rows = slice(at + first * 256 + k * 8, at + first * 256 + k * 8 + 8)
@@ -255,7 +253,7 @@
     return (parts[0] + parts[1]) + (parts[2] + parts[3])
 
 
-def back_kernel(back, main, rotary, mine, theirs):
+def back_kernel(back, main, rotary, near):
     def rows(start, count):
         return added([back[i, start : start + count, :].astype(f32) for i in range(4)])
 
@@ -264,20 +262,20 @@
     for h in range(2):
         rotary[:, h * 128 : (h + 1) * 128] = rows(512 + h * 128, 128)
     for b in range(4):
-        mine[b] = rows(768 + b * 64, 64)
-        theirs[b] = rows(1024 + b * 64, 64)
-
-
-def weight_kernel(mine, theirs, total):
-    total[...] = mine[...] + theirs[...]
+        for c in range(2):
+            near[2 * b + c] = rows(768 + c * 256 + b * 64, 64)
+
+
+def couple_kernel(mine, theirs, total):
+    total[...] = (mine[...].astype(f32) + theirs[...].astype(f32)).astype(bf16)
 
 
 def key_kernel(z0, z1, z2, z3, key):
-    key[...] = added([z[...].astype(f32) for z in (z0, z1, z2, z3)])
+    key[...] = added([z[...].astype(f32) for z in (z0, z1, z2, z3)]).astype(bf16)
 
 
 def far_kernel(near, far):
-    total = added([near[i] for i in range(4)])
+    total = added([near[i] + near[i + 4] for i in range(4)])
     for pair in range(2):
         for k in range(4):
             tile = total[pair * 32 + k * 8 :][:8]
@@ -286,7 +284,7 @@
 
 
 def last_kernel(keys, other_keys, far, lat, rot, weight):
-    total = keys[...] + other_keys[...]
+    total = keys[...].astype(f32) + other_keys[...].astype(f32)
     lat[...] = total[0:512, :].T
     rot[...] = total[512:576, :]
     for k in range(4):
@@ -339,15 +337,14 @@
     for s in range(1, 4):
         planes[s] = onward(planes[s], -s)
     toks = key_rotary.shape[0]
-    shapes = [((toks, 512), f32), ((toks, 256), f32)] + [((4, 64, 128), f32)] * 2
-    main, rotary, mine, theirs = local(back_kernel, shapes, back)
-    theirs = shift(theirs, C, 1)
-    (weight,) = local(weight_kernel, [((4, 64, 128), f32)], mine, theirs)
+    shapes = [((toks, 512), f32), ((toks, 256), f32), ((8, 64, 128), f32)]
+    main, rotary, weight = local(back_kernel, shapes, back)
     near = [[(4 * g + b - 1) % 16 for b in range(4)] for g in range(4)]
-    weight = exchange(weight, Z, near)
-    (key,) = local(key_kernel, [((576, 128), f32)], *planes)
+    pairs = [[2 * z + c for z in zs for c in range(2)] for zs in near]
+    weight = exchange(weight, (Z, C), pairs)
+    (key,) = local(key_kernel, [((576, 128), bf16)], *planes)
     beside = swap(key, Y, 1)
-    (key,) = local(weight_kernel, [((576, 128), f32)], key, beside)
+    (key,) = local(couple_kernel, [((576, 128), bf16)], key, beside)
     across = swap(key, Y, 2)
     (weight,) = local(far_kernel, [((4, 32, 128), f32)], weight)
     weight = exchange(weight, Z, [list(z) for z in zip(*near)])

time: 140 us -> 141 us (level)
  the two profiles are of different devices: /device:TPU:8 before, /device:TPU:32 now
where the time goes in v4:
time: 141 us
  starting transfers between devices  71.4 us (51%)
  waiting for transfers between devices  42.3 us (30%)
  Pallas kernels  25.8 us (18%)
    all_to_all x4, starting transfers between devices, exchange(): lax.all_to_all(tiles, axis, 0, 0, tiled=True, axis_index_groups=groups)  49.4 us
    all_to_all x4, waiting for transfers between devices, exchange(): lax.all_to_all(tiles, axis, 0, 0, tiled=True, axis_index_groups=groups)  21.7 us
    pallas_call x1, Pallas kernels, attend(): pl.pallas_call(attend_kernel, in_specs=[pl.BlockSpec(memory_space=pltpu.S...  19.1 us
    ppermute x6, waiting for transfers between devices, onward(): return lax.ppermute(block, Z, pairs)  15 us
    ppermute x6, starting transfers between devices, onward(): return lax.ppermute(block, Z, pairs)  9.73 us
    ppermute x2, starting transfers between devices, swap(): return lax.ppermute(block, axis, pairs)  8.33 us
    ppermute x2, starting transfers between devices, shift(): lax.ppermute(block, axis, [(i, (i + by) % peers) for i in range(peers)])  3.97 us
    pallas_call x7, Pallas kernels, local(): pl.pallas_call(body, in_specs=[smem] * scalars + [vmem] * (len(args) - sc...  3.94 us
  transfers between devices with their start and end apart: 14, of which 7 were waited for; matrix products, arithmetic and copies ran while one was open for 0% of the time, Pallas kernels for 2%

profile of v4, /device:TPU:32, one launch (start us, length us, event | category | flops | bytes accessed | tf_op | source)
XLA Modules:
  0.0 140.6 jit_solution(14501489757533535847)
XLA Ops:
  0.6 2.8 %pack.1 = (bf16[4,128,1408]{2,1,0:T(8,128)(2,1)}, bf16[128,640]{1,0:T(8,128)(2,1)}) custom-call(bf16[128,512]{1,0:T(8,128)(2,1)} %qm.1, bf16[128,256]{1,0:T(8,128)(2,1)} %qr.1, bf16[128,512]{1,0:T(8,128)(2,1)} %og.1, bf16[128,512]{1,0:T(8,128)(2,1)} %ho.1, f32[4,128]{1,0:T(4,128)} %logs.1, bf16[128,512]{1,0:T(8,128)(2,1)} %lat.1, bf16[64,128]{1,0:T(8,128)(2,1)} %bitcast.7), custom_call_target="tpu_custom_call" | custom-call | tf_op jit(solution)/shard_map/pack/pallas_call | solution.py:59
  3.4 0.0 copy-start.1
  3.4 4.4 %all-to-all-start = ((bf16[4,128,1408]{2,1,0:T(8,128)(2,1)}), bf16[4,128,1408]{2,1,0:T(8,128)(2,1)}, u32[]{:S(2)}, u32[]{:S(2)}) async-start(bf16[4,128,1408]{2,1,0:T(8,128)(2,1)} %get-tuple-element.20), calls=%async_computation | async-start | bytes 2883584 | tf_op jit(solution)/shard_map/all_to_all | solution.py:301
  7.9 0.0 copy-start.2
  7.9 0.0 copy-start.3
  7.9 0.0 copy-done.1
  7.9 0.8 collective-permute-start.2
  8.7 0.7 collective-permute-start.1
  9.4 4.4 %collective-permute-start = (bf16[128,640]{1,0:T(8,128)(2,1)S(1)}, bf16[128,640]{1,0:T(8,128)(2,1)S(1)}, u32[]{:S(2)}, u32[]{:S(2)}) collective-permute-start(bf16[128,640]{1,0:T(8,128)(2,1)S(1)} %copy-done.1), channel_id=1, source_target_pairs={{0,32},{32,64},{96,128},{128,160},{160,192},{224,256},{256,288},{2... | collective-permute-start | bytes 491528 | tf_op jit(solution)/shard_map/ppermute | solution.py:26
  13.8 0.0 collective-permute-done.2.k3
  13.8 0.0 collective-permute-done.1.k2
  13.9 7.5 %collective-permute-done.k1 = bf16[128,640]{1,0:T(8,128)(2,1)S(1)} collective-permute-done((bf16[128,640]{1,0:T(8,128)(2,1)S(1)}, bf16[128,640]{1,0:T(8,128)(2,1)S(1)}, u32[]{:S(2)}, u32[]{:S(2)}) %collective-permute-start) | collective-permute-done | bytes 163872 | tf_op jit(solution)/shard_map/ppermute | solution.py:26
  21.4 0.1 shard_map.128
  21.5 1.9 %collective-permute-start.3 = (bf16[4,128,640]{2,1,0:T(8,128)(2,1)S(1)}, bf16[4,128,640]{2,1,0:T(8,128)(2,1)S(1)}, u32[]{:S(2)}, u32[]{:S(2)}) collective-permute-start(bf16[4,128,640]{2,1,0:T(8,128)(2,1)S(1)} %shard_map.128), channel_id=1, source_target_pairs={{0,4},{4,0},{1,5},{5,1},{2,6},{6,2},{3,7},{7,3},{8,12},{12,8},{9,1... | collective-permute-start | bytes 1966088 | tf_op jit(solution)/shard_map/ppermute | solution.py:19
  23.5 0.1 stack.35.info
  23.5 1.9 %collective-permute-done.3.kother = bf16[4,128,640]{2,1,0:T(8,128)(2,1)S(1)} collective-permute-done((bf16[4,128,640]{2,1,0:T(8,128)(2,1)S(1)}, bf16[4,128,640]{2,1,0:T(8,128)(2,1)S(1)}, u32[]{:S(2)}, u32[]{:S(2)}) %collective-permute-start.3) | collective-permute-done | bytes 655392 | tf_op jit(solution)/shard_map/ppermute | solution.py:19
  25.4 0.0 copy-start.4
  25.4 2.1 %all-to-all-done.qs = bf16[4,128,1408]{2,1,0:T(8,128)(2,1)} async-done(((bf16[4,128,1408]{2,1,0:T(8,128)(2,1)}), bf16[4,128,1408]{2,1,0:T(8,128)(2,1)}, u32[]{:S(2)}, u32[]{:S(2)}) %all-to-all-start) | async-done | bytes 1441824 | tf_op jit(solution)/shard_map/all_to_all | solution.py:301
  27.5 0.0 copy-done.4
  27.5 0.0 copy-done.2
  27.5 0.0 copy-done.3
  27.5 19.1 %attend.1 = (bf16[4,1280,128]{2,1,0:T(8,128)(2,1)}, f32[4,576,128]{2,1,0:T(8,128)}, f32[4,576,128]{2,1,0:T(8,128)}) custom-call(s32[5]{0:T(128)S(1)} %stack.35.info, bf16[4,128,1408]{2,1,0:T(8,128)(2,1)} %all-to-all-done.qs, bf16[128,640]{1,0:T(8,128)(2,1)S(1)} %copy-done.1, bf16[128,640]{1,0:T(8,128)(2,1)S(1)} %collective-permute-done.k1, ...), custom_call_target="tpu_custom_call" | custom-call | tf_op jit(solution)/shard_map/attend/pallas_call | solution.py:199
  46.6 3.5 %all-to-all-start.1 = ((bf16[4,1280,128]{2,1,0:T(8,128)(2,1)}), bf16[4,1280,128]{2,1,0:T(8,128)(2,1)S(1)}, u32[]{:S(2)}, u32[]{:S(2)}) async-start(bf16[4,1280,128]{2,1,0:T(8,128)(2,1)} %get-tuple-element.22), calls=%async_computation.1 | async-start | bytes 2621440 | tf_op jit(solution)/shard_map/all_to_all | solution.py:301
  50.2 0.0 copy-start
  50.2 2.1 %collective-permute-start.4 = (f32[4,576,128]{2,1,0:T(8,128)}, f32[4,576,128]{2,1,0:T(8,128)}, u32[]{:S(2)}, u32[]{:S(2)}) collective-permute-start(f32[4,576,128]{2,1,0:T(8,128)} %get-tuple-element.26), channel_id=1, source_target_pairs={{0,4},{4,0},{1,5},{5,1},{2,6},{6,2},{3,7},{7,3},{8,12},{12,8},{9,1... | collective-permute-start | bytes 3538952 | tf_op jit(solution)/shard_map/ppermute | solution.py:19
  52.2 15.2 %all-to-all-done.1.back = bf16[4,1280,128]{2,1,0:T(8,128)(2,1)S(1)} async-done(((bf16[4,1280,128]{2,1,0:T(8,128)(2,1)}), bf16[4,1280,128]{2,1,0:T(8,128)(2,1)S(1)}, u32[]{:S(2)}, u32[]{:S(2)}) %all-to-all-start.1) | async-done | bytes 1310752 | tf_op jit(solution)/shard_map/all_to_all | solution.py:301
  67.5 0.9 shard_map.129
  68.4 12.0 %all-to-all-start.2 = ((f32[8,64,128]{2,1,0:T(8,128)}), f32[8,64,128]{2,1,0:T(8,128)S(1)}, u32[]{:S(2)}, u32[]{:S(2)}) async-start(f32[8,64,128]{2,1,0:T(8,128)} %get-tuple-element.31), calls=%async_computation.2 | async-start | bytes 524288 | tf_op jit(solution)/shard_map/all_to_all | solution.py:301
  80.4 0.0 collective-permute-done.4.theirs
  80.4 0.0 copy-done
  80.4 1.4 shard_map.130
  81.8 2.5 %collective-permute-start.5 = (bf16[576,128]{1,0:T(8,128)(2,1)S(1)}, bf16[576,128]{1,0:T(8,128)(2,1)S(1)}, u32[]{:S(2)}, u32[]{:S(2)}) collective-permute-start(bf16[576,128]{1,0:T(8,128)(2,1)S(1)} %get-tuple-element.28), channel_id=1, source_target_pairs={{32,0},{64,32},{128,96},{160,128},{192,160},{256,224},{288,256},{3... | collective-permute-start | bytes 442376 | tf_op jit(solution)/shard_map/ppermute | solution.py:26
  84.3 0.7 collective-permute-start.6
  85.0 0.7 collective-permute-start.7
  85.6 7.5 %collective-permute-done.5.z1 = bf16[576,128]{1,0:T(8,128)(2,1)S(1)} collective-permute-done((bf16[576,128]{1,0:T(8,128)(2,1)S(1)}, bf16[576,128]{1,0:T(8,128)(2,1)S(1)}, u32[]{:S(2)}, u32[]{:S(2)}) %collective-permute-start.5) | collective-permute-done | bytes 147488 | tf_op jit(solution)/shard_map/ppermute | solution.py:26
  93.1 0.0 collective-permute-done.6.z2
  93.1 0.0 collective-permute-done.7.z3
  93.1 0.1 shard_map.131.mine
  93.2 3.5 %collective-permute-start.8 = (bf16[576,128]{1,0:T(8,128)(2,1)S(1)}, bf16[576,128]{1,0:T(8,128)(2,1)S(1)}, u32[]{:S(2)}, u32[]{:S(2)}) collective-permute-start(bf16[576,128]{1,0:T(8,128)(2,1)S(1)} %shard_map.131.mine), channel_id=1, source_target_pairs={{0,1},{1,0},{2,3},{3,2},{4,5},{5,4},{6,7},{7,6},{8,9},{9,8},{10,11... | collective-permute-start | bytes 442376 | tf_op jit(solution)/shard_map/ppermute | solution.py:297
  96.7 0.0 all-to-all-done.2.near
  96.7 0.6 shard_map.133
  97.4 29.4 %all-to-all-start.3 = ((f32[4,32,128]{2,1,0:T(8,128)}), f32[4,32,128]{2,1,0:T(8,128)S(1)}, u32[]{:S(2)}, u32[]{:S(2)}) async-start(f32[4,32,128]{2,1,0:T(8,128)} %shard_map.133), calls=%async_computation.3 | async-start | bytes 131072 | tf_op jit(solution)/shard_map/all_to_all | solution.py:301
  126.7 0.0 collective-permute-done.8.theirs
  126.8 4.8 %collective-permute-start.9 = (bf16[576,128]{1,0:T(8,128)(2,1)S(1)}, bf16[576,128]{1,0:T(8,128)(2,1)S(1)}, u32[]{:S(2)}, u32[]{:S(2)}) collective-permute-start(bf16[576,128]{1,0:T(8,128)(2,1)S(1)} %shard_map.132.keys), channel_id=1, source_target_pairs={{0,2},{1,3},{2,0},{3,1},{4,6},{5,7},{6,4},{7,5},{8,10},{9,11},{10,... | collective-permute-start | bytes 442376 | tf_op jit(solution)/shard_map/ppermute | solution.py:297
  131.6 3.7 %collective-permute-done.9.other_keys = bf16[576,128]{1,0:T(8,128)(2,1)S(1)} collective-permute-done((bf16[576,128]{1,0:T(8,128)(2,1)S(1)}, bf16[576,128]{1,0:T(8,128)(2,1)S(1)}, u32[]{:S(2)}, u32[]{:S(2)}) %collective-permute-start.9) | collective-permute-done | bytes 147488 | tf_op jit(solution)/shard_map/ppermute | solution.py:297
  135.3 4.4 %all-to-all-done.3.far = f32[4,32,128]{2,1,0:T(8,128)S(1)} async-done(((f32[4,32,128]{2,1,0:T(8,128)}), f32[4,32,128]{2,1,0:T(8,128)S(1)}, u32[]{:S(2)}, u32[]{:S(2)}) %all-to-all-start.3) | async-done | bytes 65568 | tf_op jit(solution)/shard_map/all_to_all | solution.py:301
  139.7 0.8 shard_map.134
  (1 shorter events, 0.0 us)
Async XLA Ops:
  3.4 4.5 %copy-start.1 = (bf16[128,640]{1,0:T(8,128)(2,1)S(1)}, bf16[128,640]{1,0:T(8,128)(2,1)}, u32[]{:S(2)}) copy-start(bf16[128,640]{1,0:T(8,128)(2,1)} %get-tuple-element.21.k0) | copy-start | bytes 491524
  3.4 24.1 %all-to-all-start = ((bf16[4,128,1408]{2,1,0:T(8,128)(2,1)}), bf16[4,128,1408]{2,1,0:T(8,128)(2,1)}, u32[]{:S(2)}, u32[]{:S(2)}) async-start(bf16[4,128,1408]{2,1,0:T(8,128)(2,1)} %get-tuple-element.20), calls=%async_computation | async-start | bytes 2883584 | tf_op jit(solution)/shard_map/all_to_all | solution.py:301
  7.9 19.7 %copy-start.2 = (bf16[512,512]{1,0:T(8,128)(2,1)S(1)}, bf16[512,512]{1,0:T(8,128)(2,1)}, u32[]{:S(2)}) copy-start(bf16[512,512]{1,0:T(8,128)(2,1)} %wk.1) | copy-start | bytes 1572868
  7.9 19.6 %copy-start.3 = (bf16[512,512]{1,0:T(8,128)(2,1)S(1)}, bf16[512,512]{1,0:T(8,128)(2,1)}, u32[]{:S(2)}) copy-start(bf16[512,512]{1,0:T(8,128)(2,1)} %wv.1) | copy-start | bytes 1572868
  7.9 5.9 %collective-permute-start.2 = (bf16[128,640]{1,0:T(8,128)(2,1)S(1)}, bf16[128,640]{1,0:T(8,128)(2,1)S(1)}, u32[]{:S(2)}, u32[]{:S(2)}) collective-permute-start(bf16[128,640]{1,0:T(8,128)(2,1)S(1)} %copy-done.1), channel_id=1, source_target_pairs={{96,192},{224,320},{352,448},{97,193},{225,321},{353,449},{98,194}... | collective-permute-start | bytes 491528 | tf_op jit(solution)/shard_map/ppermute | solution.py:26
  8.7 5.1 %collective-permute-start.1 = (bf16[128,640]{1,0:T(8,128)(2,1)S(1)}, bf16[128,640]{1,0:T(8,128)(2,1)S(1)}, u32[]{:S(2)}, u32[]{:S(2)}) collective-permute-start(bf16[128,640]{1,0:T(8,128)(2,1)S(1)} %copy-done.1), channel_id=1, source_target_pairs={{0,64},{96,160},{128,192},{224,288},{256,320},{352,416},{384,448},... | collective-permute-start | bytes 491528 | tf_op jit(solution)/shard_map/ppermute | solution.py:26
  9.4 12.0 %collective-permute-start = (bf16[128,640]{1,0:T(8,128)(2,1)S(1)}, bf16[128,640]{1,0:T(8,128)(2,1)S(1)}, u32[]{:S(2)}, u32[]{:S(2)}) collective-permute-start(bf16[128,640]{1,0:T(8,128)(2,1)S(1)} %copy-done.1), channel_id=1, source_target_pairs={{0,32},{32,64},{96,128},{128,160},{160,192},{224,256},{256,288},{2... | collective-permute-start | bytes 491528 | tf_op jit(solution)/shard_map/ppermute | solution.py:26
  21.5 4.0 %collective-permute-start.3 = (bf16[4,128,640]{2,1,0:T(8,128)(2,1)S(1)}, bf16[4,128,640]{2,1,0:T(8,128)(2,1)S(1)}, u32[]{:S(2)}, u32[]{:S(2)}) collective-permute-start(bf16[4,128,640]{2,1,0:T(8,128)(2,1)S(1)} %shard_map.128), channel_id=1, source_target_pairs={{0,4},{4,0},{1,5},{5,1},{2,6},{6,2},{3,7},{7,3},{8,12},{12,8},{9,1... | collective-permute-start | bytes 1966088 | tf_op jit(solution)/shard_map/ppermute | solution.py:19
  25.4 2.1 %copy-start.4 = (bf16[4,128,640]{2,1,0:T(8,128)(2,1)}, bf16[4,128,640]{2,1,0:T(8,128)(2,1)S(1)}, u32[]{:S(2)}) copy-start(bf16[4,128,640]{2,1,0:T(8,128)(2,1)S(1)} %collective-permute-done.3.kother) | copy-start | bytes 1966084
  46.6 20.8 %all-to-all-start.1 = ((bf16[4,1280,128]{2,1,0:T(8,128)(2,1)}), bf16[4,1280,128]{2,1,0:T(8,128)(2,1)S(1)}, u32[]{:S(2)}, u32[]{:S(2)}) async-start(bf16[4,1280,128]{2,1,0:T(8,128)(2,1)} %get-tuple-element.22), calls=%async_computation.1 | async-start | bytes 2621440 | tf_op jit(solution)/shard_map/all_to_all | solution.py:301
  50.2 30.2 %copy-start = (f32[4,576,128]{2,1,0:T(8,128)S(1)}, f32[4,576,128]{2,1,0:T(8,128)}, u32[]{:S(2)}) copy-start(f32[4,576,128]{2,1,0:T(8,128)} %get-tuple-element.25.mine) | copy-start | bytes 3538948
  50.2 30.2 %collective-permute-start.4 = (f32[4,576,128]{2,1,0:T(8,128)}, f32[4,576,128]{2,1,0:T(8,128)}, u32[]{:S(2)}, u32[]{:S(2)}) collective-permute-start(f32[4,576,128]{2,1,0:T(8,128)} %get-tuple-element.26), channel_id=1, source_target_pairs={{0,4},{4,0},{1,5},{5,1},{2,6},{6,2},{3,7},{7,3},{8,12},{12,8},{9,1... | collective-permute-start | bytes 3538952 | tf_op jit(solution)/shard_map/ppermute | solution.py:19
  68.4 28.3 %all-to-all-start.2 = ((f32[8,64,128]{2,1,0:T(8,128)}), f32[8,64,128]{2,1,0:T(8,128)S(1)}, u32[]{:S(2)}, u32[]{:S(2)}) async-start(f32[8,64,128]{2,1,0:T(8,128)} %get-tuple-element.31), calls=%async_computation.2 | async-start | bytes 524288 | tf_op jit(solution)/shard_map/all_to_all | solution.py:301
  81.8 11.3 %collective-permute-start.5 = (bf16[576,128]{1,0:T(8,128)(2,1)S(1)}, bf16[576,128]{1,0:T(8,128)(2,1)S(1)}, u32[]{:S(2)}, u32[]{:S(2)}) collective-permute-start(bf16[576,128]{1,0:T(8,128)(2,1)S(1)} %get-tuple-element.28), channel_id=1, source_target_pairs={{32,0},{64,32},{128,96},{160,128},{192,160},{256,224},{288,256},{3... | collective-permute-start | bytes 442376 | tf_op jit(solution)/shard_map/ppermute | solution.py:26
  84.3 8.8 %collective-permute-start.6 = (bf16[576,128]{1,0:T(8,128)(2,1)S(1)}, bf16[576,128]{1,0:T(8,128)(2,1)S(1)}, u32[]{:S(2)}, u32[]{:S(2)}) collective-permute-start(bf16[576,128]{1,0:T(8,128)(2,1)S(1)} %get-tuple-element.29), channel_id=1, source_target_pairs={{64,0},{160,96},{192,128},{288,224},{320,256},{416,352},{448,384},... | collective-permute-start | bytes 442376 | tf_op jit(solution)/shard_map/ppermute | solution.py:26
  85.0 8.1 %collective-permute-start.7 = (bf16[576,128]{1,0:T(8,128)(2,1)S(1)}, bf16[576,128]{1,0:T(8,128)(2,1)S(1)}, u32[]{:S(2)}, u32[]{:S(2)}) collective-permute-start(bf16[576,128]{1,0:T(8,128)(2,1)S(1)} %get-tuple-element.30), channel_id=1, source_target_pairs={{192,96},{320,224},{448,352},{193,97},{321,225},{449,353},{194,98}... | collective-permute-start | bytes 442376 | tf_op jit(solution)/shard_map/ppermute | solution.py:26
  93.2 33.6 %collective-permute-start.8 = (bf16[576,128]{1,0:T(8,128)(2,1)S(1)}, bf16[576,128]{1,0:T(8,128)(2,1)S(1)}, u32[]{:S(2)}, u32[]{:S(2)}) collective-permute-start(bf16[576,128]{1,0:T(8,128)(2,1)S(1)} %shard_map.131.mine), channel_id=1, source_target_pairs={{0,1},{1,0},{2,3},{3,2},{4,5},{5,4},{6,7},{7,6},{8,9},{9,8},{10,11... | collective-permute-start | bytes 442376 | tf_op jit(solution)/shard_map/ppermute | solution.py:297
  97.4 42.4 %all-to-all-start.3 = ((f32[4,32,128]{2,1,0:T(8,128)}), f32[4,32,128]{2,1,0:T(8,128)S(1)}, u32[]{:S(2)}, u32[]{:S(2)}) async-start(f32[4,32,128]{2,1,0:T(8,128)} %shard_map.133), calls=%async_computation.3 | async-start | bytes 131072 | tf_op jit(solution)/shard_map/all_to_all | solution.py:301
  126.8 8.5 %collective-permute-start.9 = (bf16[576,128]{1,0:T(8,128)(2,1)S(1)}, bf16[576,128]{1,0:T(8,128)(2,1)S(1)}, u32[]{:S(2)}, u32[]{:S(2)}) collective-permute-start(bf16[576,128]{1,0:T(8,128)(2,1)S(1)} %shard_map.132.keys), channel_id=1, source_target_pairs={{0,2},{1,3},{2,0},{3,1},{4,6},{5,7},{6,4},{7,5},{8,10},{9,11},{10,... | collective-permute-start | bytes 442376 | tf_op jit(solution)/shard_map/ppermute | solution.py:297

commit v5 on v4

--- a/solution.py
+++ b/solution.py
@@ -82,7 +82,7 @@
     acc[...] = jnp.zeros_like(acc)
     ds_acc[...] = jnp.zeros_like(ds_acc)
     w_acc[...] = jnp.zeros_like(w_acc)
-    shape = (2 * toks, 2 * toks)
+    shape = (heads * toks, 2 * toks)
     gap_s[...] = (
         lax.broadcasted_iota(jnp.int32, shape, 1) % toks
         - lax.broadcasted_iota(jnp.int32, shape, 0) % toks
@@ -99,11 +99,13 @@
             across = dot(w_h, x_h, ((1,), (1,))).astype(bf16)
             for i in range(GROUP):
                 plain[i, rows, 0:512] = straight[i * toks : (i + 1) * toks, :]
-                turned[i, 0:512, rows] = across[:, i * toks : (i + 1) * toks]
+                lanes = slice((i % 2 * heads + h) * toks, (i % 2 * heads + h + 1) * toks)
+                turned[i // 2, 0:512, lanes] = across[:, i * toks : (i + 1) * toks]
         for i in range(GROUP):
             qr_h = qs[i, :, 512 + h * 64 : 512 + (h + 1) * 64]
             q_s[i, rows, 512:576] = qr_h
-            qt_s[i, 512:576, rows] = qr_h.T
+            lanes = slice((i % 2 * heads + h) * toks, (i % 2 * heads + h + 1) * toks)
+            qt_s[i // 2, 512:576, lanes] = qr_h.T
             extra = qs[i, :, 1280:1408].astype(f32)
             for k, ref in enumerate((log_s, term_s)):
                 at = (h * 2 + k) * 3
@@ -124,27 +126,27 @@
 
             kcur[toks : 2 * toks, :] = kother[p]
 
-            def chunk(i, _):
-                ahead = ((i - my_x) * 2 + my_c - key_c) * toks
-                limit = ahead + jnp.where(p == 0, 0, 1 << 20)
+            def chunks(j, _):
                 lows, slopes_low = [], []
                 for half in range(2):
-                    rows = slice(half * 2 * toks, (half + 1) * 2 * toks)
-                    scores = dot(q_s[i, rows, :], kcur[...], ((1,), (1,)))
-                    slopes = dot(g_s[i, rows, :], kcur[:, 0:512], ((1,), (1,)))
-                    logs = jnp.concatenate([log_s[i, rows, :]] * 2, axis=1)
-                    terms = jnp.concatenate([term_s[i, rows, :]] * 2, axis=1)
+                    i = 2 * j + half
+                    ahead = ((i - my_x) * 2 + my_c - key_c) * toks
+                    limit = ahead + jnp.where(p == 0, 0, 1 << 20)
+                    scores = dot(q_s[i], kcur[...], ((1,), (1,)))
+                    slopes = dot(g_s[i], kcur[:, 0:512], ((1,), (1,)))
+                    logs = jnp.concatenate([log_s[i]] * 2, axis=1)
+                    terms = jnp.concatenate([term_s[i]] * 2, axis=1)
                     weights = jnp.exp(factor * scores - logs)
                     weights = jnp.where(gap_s[...] <= limit, weights, 0.0)
                     dscores = (weights * (slopes - terms)).astype(bf16)
-                    acc[i, rows, :] += dot(dscores, kcur[...], ((1,), (0,)))
+                    acc[i] += dot(dscores, kcur[...], ((1,), (0,)))
                     lows.append(weights.astype(bf16))
                     slopes_low.append(dscores)
-                ds_acc[p] += dot(qt_s[i], jnp.concatenate(slopes_low, axis=0), ((1,), (0,)))
-                w_acc[p] += dot(gt_s[i], jnp.concatenate(lows, axis=0), ((1,), (0,)))
+                ds_acc[p] += dot(qt_s[j], jnp.concatenate(slopes_low, axis=0), ((1,), (0,)))
+                w_acc[p] += dot(gt_s[j], jnp.concatenate(lows, axis=0), ((1,), (0,)))
                 return 0
 
-            lax.fori_loop(jnp.where(p == 0, my_x, 0), GROUP, chunk, 0)
+            lax.fori_loop(jnp.where((p == 0) & (my_x >= 2), 1, 0), GROUP // 2, chunks, 0)
 
         return 0
 
@@ -208,12 +210,12 @@
         scratch_shapes=[
             pltpu.VMEM((2 * toks, 640), bf16),
             pltpu.VMEM((GROUP, 512, 640), bf16),
-            pltpu.VMEM((GROUP, 576, 512), bf16),
+            pltpu.VMEM((GROUP // 2, 576, 1024), bf16),
             pltpu.VMEM((GROUP, 512, 512), bf16),
-            pltpu.VMEM((GROUP, 512, 512), bf16),
+            pltpu.VMEM((GROUP // 2, 512, 1024), bf16),
             pltpu.VMEM((GROUP, 512, 128), f32),
             pltpu.VMEM((GROUP, 512, 128), f32),
-            pltpu.VMEM((2 * toks, 2 * toks), jnp.int32),
+            pltpu.VMEM((512, 2 * toks), jnp.int32),
             pltpu.VMEM((GROUP, 512, 640), f32),
             pltpu.VMEM((GROUP, 576, 2 * toks), f32),
             pltpu.VMEM((GROUP, 512, 2 * toks), f32),

time: 141 us -> 137 us (0.972)
  starting transfers between devices: 71.4 us -> 69.3 us
  Pallas kernels: 25.8 us -> 23.7 us
    pallas_call x1, Pallas kernels: 19.1 us -> 17 us  [attend(): pl.pallas_call(attend_kernel, in_specs=[pl.BlockSpec(memory_space=pltpu.S...]
    all_to_all x4, starting transfers between devices: 49.4 us -> 47.3 us  [exchange(): lax.all_to_all(tiles, axis, 0, 0, tiled=True, axis_index_groups=groups)]
where the time goes in v5:
time: 137 us; the launch traced here: 136 us
  starting transfers between devices  69.3 us (51%)
  waiting for transfers between devices  42.3 us (31%)
  Pallas kernels  23.7 us (17%)
    all_to_all x4, starting transfers between devices, exchange(): lax.all_to_all(tiles, axis, 0, 0, tiled=True, axis_index_groups=groups)  47.3 us
    all_to_all x4, waiting for transfers between devices, exchange(): lax.all_to_all(tiles, axis, 0, 0, tiled=True, axis_index_groups=groups)  21.7 us
    pallas_call x1, Pallas kernels, attend(): pl.pallas_call(attend_kernel, in_specs=[pl.BlockSpec(memory_space=pltpu.S...  17 us
    ppermute x6, waiting for transfers between devices, onward(): return lax.ppermute(block, Z, pairs)  15 us
    ppermute x6, starting transfers between devices, onward(): return lax.ppermute(block, Z, pairs)  9.73 us
    ppermute x2, starting transfers between devices, swap(): return lax.ppermute(block, axis, pairs)  8.28 us
    ppermute x2, starting transfers between devices, shift(): lax.ppermute(block, axis, [(i, (i + by) % peers) for i in range(peers)])  3.97 us
    pallas_call x7, Pallas kernels, local(): pl.pallas_call(body, in_specs=[smem] * scalars + [vmem] * (len(args) - sc...  3.94 us
  transfers between devices with their start and end apart: 14, of which 7 were waited for; matrix products, arithmetic and copies ran while one was open for 0% of the time, Pallas kernels for 2%

profile of v5, /device:TPU:32, one launch (start us, length us, event | category | flops | bytes accessed | tf_op | source)
XLA Modules:
  0.0 136.3 jit_solution(16640536567838476977)
XLA Ops:
  0.6 2.8 %pack.1 = (bf16[4,128,1408]{2,1,0:T(8,128)(2,1)}, bf16[128,640]{1,0:T(8,128)(2,1)}) custom-call(bf16[128,512]{1,0:T(8,128)(2,1)} %qm.1, bf16[128,256]{1,0:T(8,128)(2,1)} %qr.1, bf16[128,512]{1,0:T(8,128)(2,1)} %og.1, bf16[128,512]{1,0:T(8,128)(2,1)} %ho.1, f32[4,128]{1,0:T(4,128)} %logs.1, bf16[128,512]{1,0:T(8,128)(2,1)} %lat.1, bf16[64,128]{1,0:T(8,128)(2,1)} %bitcast.7), custom_call_target="tpu_custom_call" | custom-call | tf_op jit(solution)/shard_map/pack/pallas_call | solution.py:59
  3.4 0.0 copy-start.1
  3.4 4.4 %all-to-all-start = ((bf16[4,128,1408]{2,1,0:T(8,128)(2,1)}), bf16[4,128,1408]{2,1,0:T(8,128)(2,1)}, u32[]{:S(2)}, u32[]{:S(2)}) async-start(bf16[4,128,1408]{2,1,0:T(8,128)(2,1)} %get-tuple-element.20), calls=%async_computation | async-start | bytes 2883584 | tf_op jit(solution)/shard_map/all_to_all | solution.py:303
  7.9 0.0 copy-start.2
  7.9 0.0 copy-start.3
  7.9 0.0 copy-done.1
  7.9 0.8 collective-permute-start.2
  8.7 0.7 collective-permute-start.1
  9.4 4.4 %collective-permute-start = (bf16[128,640]{1,0:T(8,128)(2,1)S(1)}, bf16[128,640]{1,0:T(8,128)(2,1)S(1)}, u32[]{:S(2)}, u32[]{:S(2)}) collective-permute-start(bf16[128,640]{1,0:T(8,128)(2,1)S(1)} %copy-done.1), channel_id=1, source_target_pairs={{0,32},{32,64},{96,128},{128,160},{160,192},{224,256},{256,288},{2... | collective-permute-start | bytes 491528 | tf_op jit(solution)/shard_map/ppermute | solution.py:26
  13.8 0.0 collective-permute-done.2.k3
  13.8 0.0 collective-permute-done.1.k2
  13.9 7.5 %collective-permute-done.k1 = bf16[128,640]{1,0:T(8,128)(2,1)S(1)} collective-permute-done((bf16[128,640]{1,0:T(8,128)(2,1)S(1)}, bf16[128,640]{1,0:T(8,128)(2,1)S(1)}, u32[]{:S(2)}, u32[]{:S(2)}) %collective-permute-start) | collective-permute-done | bytes 163872 | tf_op jit(solution)/shard_map/ppermute | solution.py:26
  21.4 0.1 shard_map.128
  21.5 1.9 %collective-permute-start.3 = (bf16[4,128,640]{2,1,0:T(8,128)(2,1)S(1)}, bf16[4,128,640]{2,1,0:T(8,128)(2,1)S(1)}, u32[]{:S(2)}, u32[]{:S(2)}) collective-permute-start(bf16[4,128,640]{2,1,0:T(8,128)(2,1)S(1)} %shard_map.128), channel_id=1, source_target_pairs={{0,4},{4,0},{1,5},{5,1},{2,6},{6,2},{3,7},{7,3},{8,12},{12,8},{9,1... | collective-permute-start | bytes 1966088 | tf_op jit(solution)/shard_map/ppermute | solution.py:19
  23.5 0.1 stack.35.info
  23.5 1.9 %collective-permute-done.3.kother = bf16[4,128,640]{2,1,0:T(8,128)(2,1)S(1)} collective-permute-done((bf16[4,128,640]{2,1,0:T(8,128)(2,1)S(1)}, bf16[4,128,640]{2,1,0:T(8,128)(2,1)S(1)}, u32[]{:S(2)}, u32[]{:S(2)}) %collective-permute-start.3) | collective-permute-done | bytes 655392 | tf_op jit(solution)/shard_map/ppermute | solution.py:19
  25.4 0.0 copy-start.4
  25.4 2.1 %all-to-all-done.qs = bf16[4,128,1408]{2,1,0:T(8,128)(2,1)} async-done(((bf16[4,128,1408]{2,1,0:T(8,128)(2,1)}), bf16[4,128,1408]{2,1,0:T(8,128)(2,1)}, u32[]{:S(2)}, u32[]{:S(2)}) %all-to-all-start) | async-done | bytes 1441824 | tf_op jit(solution)/shard_map/all_to_all | solution.py:303
  27.5 0.0 copy-done.4
  27.5 0.0 copy-done.2
  27.5 0.0 copy-done.3
  27.5 17.0 %attend.1 = (bf16[4,1280,128]{2,1,0:T(8,128)(2,1)}, f32[4,576,128]{2,1,0:T(8,128)}, f32[4,576,128]{2,1,0:T(8,128)}) custom-call(s32[5]{0:T(128)S(1)} %stack.35.info, bf16[4,128,1408]{2,1,0:T(8,128)(2,1)} %all-to-all-done.qs, bf16[128,640]{1,0:T(8,128)(2,1)S(1)} %copy-done.1, bf16[128,640]{1,0:T(8,128)(2,1)S(1)} %collective-permute-done.k1, ...), custom_call_target="tpu_custom_call" | custom-call | tf_op jit(solution)/shard_map/attend/pallas_call | solution.py:201
  44.5 3.5 %all-to-all-start.1 = ((bf16[4,1280,128]{2,1,0:T(8,128)(2,1)}), bf16[4,1280,128]{2,1,0:T(8,128)(2,1)S(1)}, u32[]{:S(2)}, u32[]{:S(2)}) async-start(bf16[4,1280,128]{2,1,0:T(8,128)(2,1)} %get-tuple-element.22), calls=%async_computation.1 | async-start | bytes 2621440 | tf_op jit(solution)/shard_map/all_to_all | solution.py:303
  48.0 0.0 copy-start
  48.0 2.1 %collective-permute-start.4 = (f32[4,576,128]{2,1,0:T(8,128)}, f32[4,576,128]{2,1,0:T(8,128)}, u32[]{:S(2)}, u32[]{:S(2)}) collective-permute-start(f32[4,576,128]{2,1,0:T(8,128)} %get-tuple-element.26), channel_id=1, source_target_pairs={{0,4},{4,0},{1,5},{5,1},{2,6},{6,2},{3,7},{7,3},{8,12},{12,8},{9,1... | collective-permute-start | bytes 3538952 | tf_op jit(solution)/shard_map/ppermute | solution.py:19
  50.1 15.2 %all-to-all-done.1.back = bf16[4,1280,128]{2,1,0:T(8,128)(2,1)S(1)} async-done(((bf16[4,1280,128]{2,1,0:T(8,128)(2,1)}), bf16[4,1280,128]{2,1,0:T(8,128)(2,1)S(1)}, u32[]{:S(2)}, u32[]{:S(2)}) %all-to-all-start.1) | async-done | bytes 1310752 | tf_op jit(solution)/shard_map/all_to_all | solution.py:303
  65.3 0.9 shard_map.129
  66.2 11.0 %all-to-all-start.2 = ((f32[8,64,128]{2,1,0:T(8,128)}), f32[8,64,128]{2,1,0:T(8,128)S(1)}, u32[]{:S(2)}, u32[]{:S(2)}) async-start(f32[8,64,128]{2,1,0:T(8,128)} %get-tuple-element.31), calls=%async_computation.2 | async-start | bytes 524288 | tf_op jit(solution)/shard_map/all_to_all | solution.py:303
  77.2 0.0 collective-permute-done.4.theirs
  77.2 0.0 copy-done
  77.2 1.4 %shard_map.130 = (f32[576,128]{1,0:T(8,128)S(1)}, bf16[576,128]{1,0:T(8,128)(2,1)S(1)}, bf16[576,128]{1,0:T(8,128)(2,1)S(1)}, bf16[576,128]{1,0:T(8,128)(2,1)S(1)}) custom-call(f32[4,576,128]{2,1,0:T(8,128)S(1)} %copy-done, f32[4,576,128]{2,1,0:T(8,128)} %collective-permute-done.4.theirs), custom_call_target="tpu_custom_call" | custom-call | tf_op jit(solution)/shard_map/pallas_call | solution.py:233
  78.6 2.5 %collective-permute-start.5 = (bf16[576,128]{1,0:T(8,128)(2,1)S(1)}, bf16[576,128]{1,0:T(8,128)(2,1)S(1)}, u32[]{:S(2)}, u32[]{:S(2)}) collective-permute-start(bf16[576,128]{1,0:T(8,128)(2,1)S(1)} %get-tuple-element.28), channel_id=1, source_target_pairs={{32,0},{64,32},{128,96},{160,128},{192,160},{256,224},{288,256},{3... | collective-permute-start | bytes 442376 | tf_op jit(solution)/shard_map/ppermute | solution.py:26
  81.0 0.7 collective-permute-start.6
  81.7 0.7 collective-permute-start.7
  82.4 7.5 %collective-permute-done.5.z1 = bf16[576,128]{1,0:T(8,128)(2,1)S(1)} collective-permute-done((bf16[576,128]{1,0:T(8,128)(2,1)S(1)}, bf16[576,128]{1,0:T(8,128)(2,1)S(1)}, u32[]{:S(2)}, u32[]{:S(2)}) %collective-permute-start.5) | collective-permute-done | bytes 147488 | tf_op jit(solution)/shard_map/ppermute | solution.py:26
  89.9 0.0 collective-permute-done.6.z2
  89.9 0.0 collective-permute-done.7.z3
  89.9 0.1 shard_map.131.mine
  89.9 3.5 %collective-permute-start.8 = (bf16[576,128]{1,0:T(8,128)(2,1)S(1)}, bf16[576,128]{1,0:T(8,128)(2,1)S(1)}, u32[]{:S(2)}, u32[]{:S(2)}) collective-permute-start(bf16[576,128]{1,0:T(8,128)(2,1)S(1)} %shard_map.131.mine), channel_id=1, source_target_pairs={{0,1},{1,0},{2,3},{3,2},{4,5},{5,4},{6,7},{7,6},{8,9},{9,8},{10,11... | collective-permute-start | bytes 442376 | tf_op jit(solution)/shard_map/ppermute | solution.py:299
  93.4 0.0 all-to-all-done.2.near
  93.4 0.6 shard_map.133
  94.1 28.3 %all-to-all-start.3 = ((f32[4,32,128]{2,1,0:T(8,128)}), f32[4,32,128]{2,1,0:T(8,128)S(1)}, u32[]{:S(2)}, u32[]{:S(2)}) async-start(f32[4,32,128]{2,1,0:T(8,128)} %shard_map.133), calls=%async_computation.3 | async-start | bytes 131072 | tf_op jit(solution)/shard_map/all_to_all | solution.py:303
  122.4 0.0 collective-permute-done.8.theirs
  122.5 4.8 %collective-permute-start.9 = (bf16[576,128]{1,0:T(8,128)(2,1)S(1)}, bf16[576,128]{1,0:T(8,128)(2,1)S(1)}, u32[]{:S(2)}, u32[]{:S(2)}) collective-permute-start(bf16[576,128]{1,0:T(8,128)(2,1)S(1)} %shard_map.132.keys), channel_id=1, source_target_pairs={{0,2},{1,3},{2,0},{3,1},{4,6},{5,7},{6,4},{7,5},{8,10},{9,11},{10,... | collective-permute-start | bytes 442376 | tf_op jit(solution)/shard_map/ppermute | solution.py:299
  127.3 3.7 %collective-permute-done.9.other_keys = bf16[576,128]{1,0:T(8,128)(2,1)S(1)} collective-permute-done((bf16[576,128]{1,0:T(8,128)(2,1)S(1)}, bf16[576,128]{1,0:T(8,128)(2,1)S(1)}, u32[]{:S(2)}, u32[]{:S(2)}) %collective-permute-start.9) | collective-permute-done | bytes 147488 | tf_op jit(solution)/shard_map/ppermute | solution.py:299
  131.0 4.4 %all-to-all-done.3.far = f32[4,32,128]{2,1,0:T(8,128)S(1)} async-done(((f32[4,32,128]{2,1,0:T(8,128)}), f32[4,32,128]{2,1,0:T(8,128)S(1)}, u32[]{:S(2)}, u32[]{:S(2)}) %all-to-all-start.3) | async-done | bytes 65568 | tf_op jit(solution)/shard_map/all_to_all | solution.py:303
  135.4 0.8 shard_map.134
  (1 shorter events, 0.0 us)
Async XLA Ops:
  3.4 4.5 %copy-start.1 = (bf16[128,640]{1,0:T(8,128)(2,1)S(1)}, bf16[128,640]{1,0:T(8,128)(2,1)}, u32[]{:S(2)}) copy-start(bf16[128,640]{1,0:T(8,128)(2,1)} %get-tuple-element.21.k0) | copy-start | bytes 491524
  3.4 24.1 %all-to-all-start = ((bf16[4,128,1408]{2,1,0:T(8,128)(2,1)}), bf16[4,128,1408]{2,1,0:T(8,128)(2,1)}, u32[]{:S(2)}, u32[]{:S(2)}) async-start(bf16[4,128,1408]{2,1,0:T(8,128)(2,1)} %get-tuple-element.20), calls=%async_computation | async-start | bytes 2883584 | tf_op jit(solution)/shard_map/all_to_all | solution.py:303
  7.9 19.7 %copy-start.2 = (bf16[512,512]{1,0:T(8,128)(2,1)S(1)}, bf16[512,512]{1,0:T(8,128)(2,1)}, u32[]{:S(2)}) copy-start(bf16[512,512]{1,0:T(8,128)(2,1)} %wk.1) | copy-start | bytes 1572868
  7.9 19.6 %copy-start.3 = (bf16[512,512]{1,0:T(8,128)(2,1)S(1)}, bf16[512,512]{1,0:T(8,128)(2,1)}, u32[]{:S(2)}) copy-start(bf16[512,512]{1,0:T(8,128)(2,1)} %wv.1) | copy-start | bytes 1572868
  7.9 5.9 %collective-permute-start.2 = (bf16[128,640]{1,0:T(8,128)(2,1)S(1)}, bf16[128,640]{1,0:T(8,128)(2,1)S(1)}, u32[]{:S(2)}, u32[]{:S(2)}) collective-permute-start(bf16[128,640]{1,0:T(8,128)(2,1)S(1)} %copy-done.1), channel_id=1, source_target_pairs={{96,192},{224,320},{352,448},{97,193},{225,321},{353,449},{98,194}... | collective-permute-start | bytes 491528 | tf_op jit(solution)/shard_map/ppermute | solution.py:26
  8.7 5.1 %collective-permute-start.1 = (bf16[128,640]{1,0:T(8,128)(2,1)S(1)}, bf16[128,640]{1,0:T(8,128)(2,1)S(1)}, u32[]{:S(2)}, u32[]{:S(2)}) collective-permute-start(bf16[128,640]{1,0:T(8,128)(2,1)S(1)} %copy-done.1), channel_id=1, source_target_pairs={{0,64},{96,160},{128,192},{224,288},{256,320},{352,416},{384,448},... | collective-permute-start | bytes 491528 | tf_op jit(solution)/shard_map/ppermute | solution.py:26
  9.4 12.0 %collective-permute-start = (bf16[128,640]{1,0:T(8,128)(2,1)S(1)}, bf16[128,640]{1,0:T(8,128)(2,1)S(1)}, u32[]{:S(2)}, u32[]{:S(2)}) collective-permute-start(bf16[128,640]{1,0:T(8,128)(2,1)S(1)} %copy-done.1), channel_id=1, source_target_pairs={{0,32},{32,64},{96,128},{128,160},{160,192},{224,256},{256,288},{2... | collective-permute-start | bytes 491528 | tf_op jit(solution)/shard_map/ppermute | solution.py:26
  21.5 4.0 %collective-permute-start.3 = (bf16[4,128,640]{2,1,0:T(8,128)(2,1)S(1)}, bf16[4,128,640]{2,1,0:T(8,128)(2,1)S(1)}, u32[]{:S(2)}, u32[]{:S(2)}) collective-permute-start(bf16[4,128,640]{2,1,0:T(8,128)(2,1)S(1)} %shard_map.128), channel_id=1, source_target_pairs={{0,4},{4,0},{1,5},{5,1},{2,6},{6,2},{3,7},{7,3},{8,12},{12,8},{9,1... | collective-permute-start | bytes 1966088 | tf_op jit(solution)/shard_map/ppermute | solution.py:19
  25.4 2.1 %copy-start.4 = (bf16[4,128,640]{2,1,0:T(8,128)(2,1)}, bf16[4,128,640]{2,1,0:T(8,128)(2,1)S(1)}, u32[]{:S(2)}) copy-start(bf16[4,128,640]{2,1,0:T(8,128)(2,1)S(1)} %collective-permute-done.3.kother) | copy-start | bytes 1966084
  44.5 20.8 %all-to-all-start.1 = ((bf16[4,1280,128]{2,1,0:T(8,128)(2,1)}), bf16[4,1280,128]{2,1,0:T(8,128)(2,1)S(1)}, u32[]{:S(2)}, u32[]{:S(2)}) async-start(bf16[4,1280,128]{2,1,0:T(8,128)(2,1)} %get-tuple-element.22), calls=%async_computation.1 | async-start | bytes 2621440 | tf_op jit(solution)/shard_map/all_to_all | solution.py:303
  48.0 29.1 %copy-start = (f32[4,576,128]{2,1,0:T(8,128)S(1)}, f32[4,576,128]{2,1,0:T(8,128)}, u32[]{:S(2)}) copy-start(f32[4,576,128]{2,1,0:T(8,128)} %get-tuple-element.25.mine) | copy-start | bytes 3538948
  48.0 29.1 %collective-permute-start.4 = (f32[4,576,128]{2,1,0:T(8,128)}, f32[4,576,128]{2,1,0:T(8,128)}, u32[]{:S(2)}, u32[]{:S(2)}) collective-permute-start(f32[4,576,128]{2,1,0:T(8,128)} %get-tuple-element.26), channel_id=1, source_target_pairs={{0,4},{4,0},{1,5},{5,1},{2,6},{6,2},{3,7},{7,3},{8,12},{12,8},{9,1... | collective-permute-start | bytes 3538952 | tf_op jit(solution)/shard_map/ppermute | solution.py:19
  66.2 27.2 %all-to-all-start.2 = ((f32[8,64,128]{2,1,0:T(8,128)}), f32[8,64,128]{2,1,0:T(8,128)S(1)}, u32[]{:S(2)}, u32[]{:S(2)}) async-start(f32[8,64,128]{2,1,0:T(8,128)} %get-tuple-element.31), calls=%async_computation.2 | async-start | bytes 524288 | tf_op jit(solution)/shard_map/all_to_all | solution.py:303
  78.6 11.3 %collective-permute-start.5 = (bf16[576,128]{1,0:T(8,128)(2,1)S(1)}, bf16[576,128]{1,0:T(8,128)(2,1)S(1)}, u32[]{:S(2)}, u32[]{:S(2)}) collective-permute-start(bf16[576,128]{1,0:T(8,128)(2,1)S(1)} %get-tuple-element.28), channel_id=1, source_target_pairs={{32,0},{64,32},{128,96},{160,128},{192,160},{256,224},{288,256},{3... | collective-permute-start | bytes 442376 | tf_op jit(solution)/shard_map/ppermute | solution.py:26
  81.0 8.8 %collective-permute-start.6 = (bf16[576,128]{1,0:T(8,128)(2,1)S(1)}, bf16[576,128]{1,0:T(8,128)(2,1)S(1)}, u32[]{:S(2)}, u32[]{:S(2)}) collective-permute-start(bf16[576,128]{1,0:T(8,128)(2,1)S(1)} %get-tuple-element.29), channel_id=1, source_target_pairs={{64,0},{160,96},{192,128},{288,224},{320,256},{416,352},{448,384},... | collective-permute-start | bytes 442376 | tf_op jit(solution)/shard_map/ppermute | solution.py:26
  81.7 8.1 %collective-permute-start.7 = (bf16[576,128]{1,0:T(8,128)(2,1)S(1)}, bf16[576,128]{1,0:T(8,128)(2,1)S(1)}, u32[]{:S(2)}, u32[]{:S(2)}) collective-permute-start(bf16[576,128]{1,0:T(8,128)(2,1)S(1)} %get-tuple-element.30), channel_id=1, source_target_pairs={{192,96},{320,224},{448,352},{193,97},{321,225},{449,353},{194,98}... | collective-permute-start | bytes 442376 | tf_op jit(solution)/shard_map/ppermute | solution.py:26
  89.9 32.5 %collective-permute-start.8 = (bf16[576,128]{1,0:T(8,128)(2,1)S(1)}, bf16[576,128]{1,0:T(8,128)(2,1)S(1)}, u32[]{:S(2)}, u32[]{:S(2)}) collective-permute-start(bf16[576,128]{1,0:T(8,128)(2,1)S(1)} %shard_map.131.mine), channel_id=1, source_target_pairs={{0,1},{1,0},{2,3},{3,2},{4,5},{5,4},{6,7},{7,6},{8,9},{9,8},{10,11... | collective-permute-start | bytes 442376 | tf_op jit(solution)/shard_map/ppermute | solution.py:299
  94.1 41.4 %all-to-all-start.3 = ((f32[4,32,128]{2,1,0:T(8,128)}), f32[4,32,128]{2,1,0:T(8,128)S(1)}, u32[]{:S(2)}, u32[]{:S(2)}) async-start(f32[4,32,128]{2,1,0:T(8,128)} %shard_map.133), calls=%async_computation.3 | async-start | bytes 131072 | tf_op jit(solution)/shard_map/all_to_all | solution.py:303
  122.5 8.5 %collective-permute-start.9 = (bf16[576,128]{1,0:T(8,128)(2,1)S(1)}, bf16[576,128]{1,0:T(8,128)(2,1)S(1)}, u32[]{:S(2)}, u32[]{:S(2)}) collective-permute-start(bf16[576,128]{1,0:T(8,128)(2,1)S(1)} %shard_map.132.keys), channel_id=1, source_target_pairs={{0,2},{1,3},{2,0},{3,1},{4,6},{5,7},{6,4},{7,5},{8,10},{9,11},{10,... | collective-permute-start | bytes 442376 | tf_op jit(solution)/shard_map/ppermute | solution.py:299

commit v6 on v5

--- a/solution.py
+++ b/solution.py
@@ -87,8 +87,8 @@
         lax.broadcasted_iota(jnp.int32, shape, 1) % toks
         - lax.broadcasted_iota(jnp.int32, shape, 0) % toks
     )
-    for i in range(GROUP):
-        q_s[i, :, 576:640] = jnp.zeros((heads * toks, 64), bf16)
+    for j in range(GROUP // 2):
+        q_s[j, :, 576:640] = jnp.zeros((2 * heads * toks, 64), bf16)
     for h in range(heads):
         rows = slice(h * toks, (h + 1) * toks)
         cols = slice(h * width, (h + 1) * width)
@@ -98,13 +98,13 @@
             straight = dot(x_h, w_h, ((1,), (1,))).astype(bf16)
             across = dot(w_h, x_h, ((1,), (1,))).astype(bf16)
             for i in range(GROUP):
-                plain[i, rows, 0:512] = straight[i * toks : (i + 1) * toks, :]
                 lanes = slice((i % 2 * heads + h) * toks, (i % 2 * heads + h + 1) * toks)
+                plain[i // 2, lanes, 0:512] = straight[i * toks : (i + 1) * toks, :]
                 turned[i // 2, 0:512, lanes] = across[:, i * toks : (i + 1) * toks]
         for i in range(GROUP):
             qr_h = qs[i, :, 512 + h * 64 : 512 + (h + 1) * 64]
-            q_s[i, rows, 512:576] = qr_h
             lanes = slice((i % 2 * heads + h) * toks, (i % 2 * heads + h + 1) * toks)
+            q_s[i // 2, lanes, 512:576] = qr_h
             qt_s[i // 2, 512:576, lanes] = qr_h.T
             extra = qs[i, :, 1280:1408].astype(f32)
             for k, ref in enumerate((log_s, term_s)):
@@ -128,12 +128,15 @@
 
             def chunks(j, _):
                 lows, slopes_low = [], []
+                both_scores = dot(q_s[j], kcur[...], ((1,), (1,)))
+                both_slopes = dot(g_s[j], kcur[:, 0:512], ((1,), (1,)))
                 for half in range(2):
                     i = 2 * j + half
+                    part = slice(half * heads * toks, (half + 1) * heads * toks)
                     ahead = ((i - my_x) * 2 + my_c - key_c) * toks
                     limit = ahead + jnp.where(p == 0, 0, 1 << 20)
-                    scores = dot(q_s[i], kcur[...], ((1,), (1,)))
-                    slopes = dot(g_s[i], kcur[:, 0:512], ((1,), (1,)))
+                    scores = both_scores[part, :]
+                    slopes = both_slopes[part, :]
                     logs = jnp.concatenate([log_s[i]] * 2, axis=1)
                     terms = jnp.concatenate([term_s[i]] * 2, axis=1)
                     weights = jnp.exp(factor * scores - logs)
@@ -209,9 +212,9 @@
         ],
         scratch_shapes=[
             pltpu.VMEM((2 * toks, 640), bf16),
-            pltpu.VMEM((GROUP, 512, 640), bf16),
+            pltpu.VMEM((GROUP // 2, 1024, 640), bf16),
             pltpu.VMEM((GROUP // 2, 576, 1024), bf16),
-            pltpu.VMEM((GROUP, 512, 512), bf16),
+            pltpu.VMEM((GROUP // 2, 1024, 512), bf16),
             pltpu.VMEM((GROUP // 2, 512, 1024), bf16),
             pltpu.VMEM((GROUP, 512, 128), f32),
             pltpu.VMEM((GROUP, 512, 128), f32),

time: 137 us -> 137 us (level)
  no operation moved by 1% of the time
where the time goes in v6:
time: 137 us
  starting transfers between devices  69.5 us (51%)
  waiting for transfers between devices  42.3 us (31%)
  Pallas kernels  23.8 us (17%)
    all_to_all x4, starting transfers between devices, exchange(): lax.all_to_all(tiles, axis, 0, 0, tiled=True, axis_index_groups=groups)  47.5 us
    all_to_all x4, waiting for transfers between devices, exchange(): lax.all_to_all(tiles, axis, 0, 0, tiled=True, axis_index_groups=groups)  21.7 us
    pallas_call x1, Pallas kernels, attend(): pl.pallas_call(attend_kernel, in_specs=[pl.BlockSpec(memory_space=pltpu.S...  17.1 us
    ppermute x6, waiting for transfers between devices, onward(): return lax.ppermute(block, Z, pairs)  15 us
    ppermute x6, starting transfers between devices, onward(): return lax.ppermute(block, Z, pairs)  9.73 us
    ppermute x2, starting transfers between devices, swap(): return lax.ppermute(block, axis, pairs)  8.29 us
    ppermute x2, starting transfers between devices, shift(): lax.ppermute(block, axis, [(i, (i + by) % peers) for i in range(peers)])  3.97 us
    pallas_call x7, Pallas kernels, local(): pl.pallas_call(body, in_specs=[smem] * scalars + [vmem] * (len(args) - sc...  3.94 us
  transfers between devices with their start and end apart: 14, of which 7 were waited for; matrix products, arithmetic and copies ran while one was open for 0% of the time, Pallas kernels for 2%

profile of v6, /device:TPU:32, one launch (start us, length us, event | category | flops | bytes accessed | tf_op | source)
XLA Modules:
  0.0 136.6 jit_solution(11208748186560065450)
XLA Ops:
  0.6 2.8 %pack.1 = (bf16[4,128,1408]{2,1,0:T(8,128)(2,1)}, bf16[128,640]{1,0:T(8,128)(2,1)}) custom-call(bf16[128,512]{1,0:T(8,128)(2,1)} %qm.1, bf16[128,256]{1,0:T(8,128)(2,1)} %qr.1, bf16[128,512]{1,0:T(8,128)(2,1)} %og.1, bf16[128,512]{1,0:T(8,128)(2,1)} %ho.1, f32[4,128]{1,0:T(4,128)} %logs.1, bf16[128,512]{1,0:T(8,128)(2,1)} %lat.1, bf16[64,128]{1,0:T(8,128)(2,1)} %bitcast.7), custom_call_target="tpu_custom_call" | custom-call | tf_op jit(solution)/shard_map/pack/pallas_call | solution.py:59
  3.4 0.0 copy-start.1
  3.4 4.4 %all-to-all-start = ((bf16[4,128,1408]{2,1,0:T(8,128)(2,1)}), bf16[4,128,1408]{2,1,0:T(8,128)(2,1)}, u32[]{:S(2)}, u32[]{:S(2)}) async-start(bf16[4,128,1408]{2,1,0:T(8,128)(2,1)} %get-tuple-element.20), calls=%async_computation | async-start | bytes 2883584 | tf_op jit(solution)/shard_map/all_to_all | solution.py:306
  7.9 0.0 copy-start.2
  7.9 0.0 copy-start.3
  7.9 0.0 copy-done.1
  7.9 0.8 collective-permute-start.2
  8.7 0.7 collective-permute-start.1
  9.4 4.4 %collective-permute-start = (bf16[128,640]{1,0:T(8,128)(2,1)S(1)}, bf16[128,640]{1,0:T(8,128)(2,1)S(1)}, u32[]{:S(2)}, u32[]{:S(2)}) collective-permute-start(bf16[128,640]{1,0:T(8,128)(2,1)S(1)} %copy-done.1), channel_id=1, source_target_pairs={{0,32},{32,64},{96,128},{128,160},{160,192},{224,256},{256,288},{2... | collective-permute-start | bytes 491528 | tf_op jit(solution)/shard_map/ppermute | solution.py:26
  13.8 0.0 collective-permute-done.2.k3
  13.8 0.0 collective-permute-done.1.k2
  13.9 7.5 %collective-permute-done.k1 = bf16[128,640]{1,0:T(8,128)(2,1)S(1)} collective-permute-done((bf16[128,640]{1,0:T(8,128)(2,1)S(1)}, bf16[128,640]{1,0:T(8,128)(2,1)S(1)}, u32[]{:S(2)}, u32[]{:S(2)}) %collective-permute-start) | collective-permute-done | bytes 163872 | tf_op jit(solution)/shard_map/ppermute | solution.py:26
  21.4 0.1 shard_map.128
  21.5 1.9 %collective-permute-start.3 = (bf16[4,128,640]{2,1,0:T(8,128)(2,1)S(1)}, bf16[4,128,640]{2,1,0:T(8,128)(2,1)S(1)}, u32[]{:S(2)}, u32[]{:S(2)}) collective-permute-start(bf16[4,128,640]{2,1,0:T(8,128)(2,1)S(1)} %shard_map.128), channel_id=1, source_target_pairs={{0,4},{4,0},{1,5},{5,1},{2,6},{6,2},{3,7},{7,3},{8,12},{12,8},{9,1... | collective-permute-start | bytes 1966088 | tf_op jit(solution)/shard_map/ppermute | solution.py:19
  23.5 0.1 stack.35.info
  23.5 1.9 %collective-permute-done.3.kother = bf16[4,128,640]{2,1,0:T(8,128)(2,1)S(1)} collective-permute-done((bf16[4,128,640]{2,1,0:T(8,128)(2,1)S(1)}, bf16[4,128,640]{2,1,0:T(8,128)(2,1)S(1)}, u32[]{:S(2)}, u32[]{:S(2)}) %collective-permute-start.3) | collective-permute-done | bytes 655392 | tf_op jit(solution)/shard_map/ppermute | solution.py:19
  25.4 0.0 copy-start.4
  25.4 2.1 %all-to-all-done.qs = bf16[4,128,1408]{2,1,0:T(8,128)(2,1)} async-done(((bf16[4,128,1408]{2,1,0:T(8,128)(2,1)}), bf16[4,128,1408]{2,1,0:T(8,128)(2,1)}, u32[]{:S(2)}, u32[]{:S(2)}) %all-to-all-start) | async-done | bytes 1441824 | tf_op jit(solution)/shard_map/all_to_all | solution.py:306
  27.5 0.0 copy-done.4
  27.5 0.0 copy-done.2
  27.5 0.0 copy-done.3
  27.5 17.1 %attend.1 = (bf16[4,1280,128]{2,1,0:T(8,128)(2,1)}, f32[4,576,128]{2,1,0:T(8,128)}, f32[4,576,128]{2,1,0:T(8,128)}) custom-call(s32[5]{0:T(128)S(1)} %stack.35.info, bf16[4,128,1408]{2,1,0:T(8,128)(2,1)} %all-to-all-done.qs, bf16[128,640]{1,0:T(8,128)(2,1)S(1)} %copy-done.1, bf16[128,640]{1,0:T(8,128)(2,1)S(1)} %collective-permute-done.k1, ...), custom_call_target="tpu_custom_call" | custom-call | tf_op jit(solution)/shard_map/attend/pallas_call | solution.py:204
  44.6 3.5 %all-to-all-start.1 = ((bf16[4,1280,128]{2,1,0:T(8,128)(2,1)}), bf16[4,1280,128]{2,1,0:T(8,128)(2,1)S(1)}, u32[]{:S(2)}, u32[]{:S(2)}) async-start(bf16[4,1280,128]{2,1,0:T(8,128)(2,1)} %get-tuple-element.22), calls=%async_computation.1 | async-start | bytes 2621440 | tf_op jit(solution)/shard_map/all_to_all | solution.py:306
  48.2 0.0 copy-start
  48.2 2.1 %collective-permute-start.4 = (f32[4,576,128]{2,1,0:T(8,128)}, f32[4,576,128]{2,1,0:T(8,128)}, u32[]{:S(2)}, u32[]{:S(2)}) collective-permute-start(f32[4,576,128]{2,1,0:T(8,128)} %get-tuple-element.26), channel_id=1, source_target_pairs={{0,4},{4,0},{1,5},{5,1},{2,6},{6,2},{3,7},{7,3},{8,12},{12,8},{9,1... | collective-permute-start | bytes 3538952 | tf_op jit(solution)/shard_map/ppermute | solution.py:19
  50.3 15.2 %all-to-all-done.1.back = bf16[4,1280,128]{2,1,0:T(8,128)(2,1)S(1)} async-done(((bf16[4,1280,128]{2,1,0:T(8,128)(2,1)}), bf16[4,1280,128]{2,1,0:T(8,128)(2,1)S(1)}, u32[]{:S(2)}, u32[]{:S(2)}) %all-to-all-start.1) | async-done | bytes 1310752 | tf_op jit(solution)/shard_map/all_to_all | solution.py:306
  65.5 0.9 shard_map.129
  66.4 11.1 %all-to-all-start.2 = ((f32[8,64,128]{2,1,0:T(8,128)}), f32[8,64,128]{2,1,0:T(8,128)S(1)}, u32[]{:S(2)}, u32[]{:S(2)}) async-start(f32[8,64,128]{2,1,0:T(8,128)} %get-tuple-element.31), calls=%async_computation.2 | async-start | bytes 524288 | tf_op jit(solution)/shard_map/all_to_all | solution.py:306
  77.4 0.0 collective-permute-done.4.theirs
  77.4 0.0 copy-done
  77.4 1.4 %shard_map.130 = (f32[576,128]{1,0:T(8,128)S(1)}, bf16[576,128]{1,0:T(8,128)(2,1)S(1)}, bf16[576,128]{1,0:T(8,128)(2,1)S(1)}, bf16[576,128]{1,0:T(8,128)(2,1)S(1)}) custom-call(f32[4,576,128]{2,1,0:T(8,128)S(1)} %copy-done, f32[4,576,128]{2,1,0:T(8,128)} %collective-permute-done.4.theirs), custom_call_target="tpu_custom_call" | custom-call | tf_op jit(solution)/shard_map/pallas_call | solution.py:236
  78.8 2.5 %collective-permute-start.5 = (bf16[576,128]{1,0:T(8,128)(2,1)S(1)}, bf16[576,128]{1,0:T(8,128)(2,1)S(1)}, u32[]{:S(2)}, u32[]{:S(2)}) collective-permute-start(bf16[576,128]{1,0:T(8,128)(2,1)S(1)} %get-tuple-element.28), channel_id=1, source_target_pairs={{32,0},{64,32},{128,96},{160,128},{192,160},{256,224},{288,256},{3... | collective-permute-start | bytes 442376 | tf_op jit(solution)/shard_map/ppermute | solution.py:26
  81.3 0.7 collective-permute-start.6
  82.0 0.7 collective-permute-start.7
  82.7 7.5 %collective-permute-done.5.z1 = bf16[576,128]{1,0:T(8,128)(2,1)S(1)} collective-permute-done((bf16[576,128]{1,0:T(8,128)(2,1)S(1)}, bf16[576,128]{1,0:T(8,128)(2,1)S(1)}, u32[]{:S(2)}, u32[]{:S(2)}) %collective-permute-start.5) | collective-permute-done | bytes 147488 | tf_op jit(solution)/shard_map/ppermute | solution.py:26
  90.1 0.0 collective-permute-done.6.z2
  90.1 0.0 collective-permute-done.7.z3
  90.1 0.1 shard_map.131.mine
  90.2 3.5 %collective-permute-start.8 = (bf16[576,128]{1,0:T(8,128)(2,1)S(1)}, bf16[576,128]{1,0:T(8,128)(2,1)S(1)}, u32[]{:S(2)}, u32[]{:S(2)}) collective-permute-start(bf16[576,128]{1,0:T(8,128)(2,1)S(1)} %shard_map.131.mine), channel_id=1, source_target_pairs={{0,1},{1,0},{2,3},{3,2},{4,5},{5,4},{6,7},{7,6},{8,9},{9,8},{10,11... | collective-permute-start | bytes 442376 | tf_op jit(solution)/shard_map/ppermute | solution.py:302
  93.7 0.0 all-to-all-done.2.near
  93.7 0.6 shard_map.133
  94.3 28.4 %all-to-all-start.3 = ((f32[4,32,128]{2,1,0:T(8,128)}), f32[4,32,128]{2,1,0:T(8,128)S(1)}, u32[]{:S(2)}, u32[]{:S(2)}) async-start(f32[4,32,128]{2,1,0:T(8,128)} %shard_map.133), calls=%async_computation.3 | async-start | bytes 131072 | tf_op jit(solution)/shard_map/all_to_all | solution.py:306
  122.7 0.0 collective-permute-done.8.theirs
  122.8 4.8 %collective-permute-start.9 = (bf16[576,128]{1,0:T(8,128)(2,1)S(1)}, bf16[576,128]{1,0:T(8,128)(2,1)S(1)}, u32[]{:S(2)}, u32[]{:S(2)}) collective-permute-start(bf16[576,128]{1,0:T(8,128)(2,1)S(1)} %shard_map.132.keys), channel_id=1, source_target_pairs={{0,2},{1,3},{2,0},{3,1},{4,6},{5,7},{6,4},{7,5},{8,10},{9,11},{10,... | collective-permute-start | bytes 442376 | tf_op jit(solution)/shard_map/ppermute | solution.py:302
  127.6 3.7 %collective-permute-done.9.other_keys = bf16[576,128]{1,0:T(8,128)(2,1)S(1)} collective-permute-done((bf16[576,128]{1,0:T(8,128)(2,1)S(1)}, bf16[576,128]{1,0:T(8,128)(2,1)S(1)}, u32[]{:S(2)}, u32[]{:S(2)}) %collective-permute-start.9) | collective-permute-done | bytes 147488 | tf_op jit(solution)/shard_map/ppermute | solution.py:302
  131.3 4.4 %all-to-all-done.3.far = f32[4,32,128]{2,1,0:T(8,128)S(1)} async-done(((f32[4,32,128]{2,1,0:T(8,128)}), f32[4,32,128]{2,1,0:T(8,128)S(1)}, u32[]{:S(2)}, u32[]{:S(2)}) %all-to-all-start.3) | async-done | bytes 65568 | tf_op jit(solution)/shard_map/all_to_all | solution.py:306
  135.8 0.8 shard_map.134
  (1 shorter events, 0.0 us)
Async XLA Ops:
  3.4 4.5 %copy-start.1 = (bf16[128,640]{1,0:T(8,128)(2,1)S(1)}, bf16[128,640]{1,0:T(8,128)(2,1)}, u32[]{:S(2)}) copy-start(bf16[128,640]{1,0:T(8,128)(2,1)} %get-tuple-element.21.k0) | copy-start | bytes 491524
  3.4 24.1 %all-to-all-start = ((bf16[4,128,1408]{2,1,0:T(8,128)(2,1)}), bf16[4,128,1408]{2,1,0:T(8,128)(2,1)}, u32[]{:S(2)}, u32[]{:S(2)}) async-start(bf16[4,128,1408]{2,1,0:T(8,128)(2,1)} %get-tuple-element.20), calls=%async_computation | async-start | bytes 2883584 | tf_op jit(solution)/shard_map/all_to_all | solution.py:306
  7.9 19.7 %copy-start.2 = (bf16[512,512]{1,0:T(8,128)(2,1)S(1)}, bf16[512,512]{1,0:T(8,128)(2,1)}, u32[]{:S(2)}) copy-start(bf16[512,512]{1,0:T(8,128)(2,1)} %wk.1) | copy-start | bytes 1572868
  7.9 19.6 %copy-start.3 = (bf16[512,512]{1,0:T(8,128)(2,1)S(1)}, bf16[512,512]{1,0:T(8,128)(2,1)}, u32[]{:S(2)}) copy-start(bf16[512,512]{1,0:T(8,128)(2,1)} %wv.1) | copy-start | bytes 1572868
  7.9 5.9 %collective-permute-start.2 = (bf16[128,640]{1,0:T(8,128)(2,1)S(1)}, bf16[128,640]{1,0:T(8,128)(2,1)S(1)}, u32[]{:S(2)}, u32[]{:S(2)}) collective-permute-start(bf16[128,640]{1,0:T(8,128)(2,1)S(1)} %copy-done.1), channel_id=1, source_target_pairs={{96,192},{224,320},{352,448},{97,193},{225,321},{353,449},{98,194}... | collective-permute-start | bytes 491528 | tf_op jit(solution)/shard_map/ppermute | solution.py:26
  8.7 5.1 %collective-permute-start.1 = (bf16[128,640]{1,0:T(8,128)(2,1)S(1)}, bf16[128,640]{1,0:T(8,128)(2,1)S(1)}, u32[]{:S(2)}, u32[]{:S(2)}) collective-permute-start(bf16[128,640]{1,0:T(8,128)(2,1)S(1)} %copy-done.1), channel_id=1, source_target_pairs={{0,64},{96,160},{128,192},{224,288},{256,320},{352,416},{384,448},... | collective-permute-start | bytes 491528 | tf_op jit(solution)/shard_map/ppermute | solution.py:26
  9.4 12.0 %collective-permute-start = (bf16[128,640]{1,0:T(8,128)(2,1)S(1)}, bf16[128,640]{1,0:T(8,128)(2,1)S(1)}, u32[]{:S(2)}, u32[]{:S(2)}) collective-permute-start(bf16[128,640]{1,0:T(8,128)(2,1)S(1)} %copy-done.1), channel_id=1, source_target_pairs={{0,32},{32,64},{96,128},{128,160},{160,192},{224,256},{256,288},{2... | collective-permute-start | bytes 491528 | tf_op jit(solution)/shard_map/ppermute | solution.py:26
  21.5 4.0 %collective-permute-start.3 = (bf16[4,128,640]{2,1,0:T(8,128)(2,1)S(1)}, bf16[4,128,640]{2,1,0:T(8,128)(2,1)S(1)}, u32[]{:S(2)}, u32[]{:S(2)}) collective-permute-start(bf16[4,128,640]{2,1,0:T(8,128)(2,1)S(1)} %shard_map.128), channel_id=1, source_target_pairs={{0,4},{4,0},{1,5},{5,1},{2,6},{6,2},{3,7},{7,3},{8,12},{12,8},{9,1... | collective-permute-start | bytes 1966088 | tf_op jit(solution)/shard_map/ppermute | solution.py:19
  25.4 2.1 %copy-start.4 = (bf16[4,128,640]{2,1,0:T(8,128)(2,1)}, bf16[4,128,640]{2,1,0:T(8,128)(2,1)S(1)}, u32[]{:S(2)}) copy-start(bf16[4,128,640]{2,1,0:T(8,128)(2,1)S(1)} %collective-permute-done.3.kother) | copy-start | bytes 1966084
  44.6 20.8 %all-to-all-start.1 = ((bf16[4,1280,128]{2,1,0:T(8,128)(2,1)}), bf16[4,1280,128]{2,1,0:T(8,128)(2,1)S(1)}, u32[]{:S(2)}, u32[]{:S(2)}) async-start(bf16[4,1280,128]{2,1,0:T(8,128)(2,1)} %get-tuple-element.22), calls=%async_computation.1 | async-start | bytes 2621440 | tf_op jit(solution)/shard_map/all_to_all | solution.py:306
  48.2 29.2 %copy-start = (f32[4,576,128]{2,1,0:T(8,128)S(1)}, f32[4,576,128]{2,1,0:T(8,128)}, u32[]{:S(2)}) copy-start(f32[4,576,128]{2,1,0:T(8,128)} %get-tuple-element.25.mine) | copy-start | bytes 3538948
  48.2 29.2 %collective-permute-start.4 = (f32[4,576,128]{2,1,0:T(8,128)}, f32[4,576,128]{2,1,0:T(8,128)}, u32[]{:S(2)}, u32[]{:S(2)}) collective-permute-start(f32[4,576,128]{2,1,0:T(8,128)} %get-tuple-element.26), channel_id=1, source_target_pairs={{0,4},{4,0},{1,5},{5,1},{2,6},{6,2},{3,7},{7,3},{8,12},{12,8},{9,1... | collective-permute-start | bytes 3538952 | tf_op jit(solution)/shard_map/ppermute | solution.py:19
  66.4 27.3 %all-to-all-start.2 = ((f32[8,64,128]{2,1,0:T(8,128)}), f32[8,64,128]{2,1,0:T(8,128)S(1)}, u32[]{:S(2)}, u32[]{:S(2)}) async-start(f32[8,64,128]{2,1,0:T(8,128)} %get-tuple-element.31), calls=%async_computation.2 | async-start | bytes 524288 | tf_op jit(solution)/shard_map/all_to_all | solution.py:306
  78.8 11.3 %collective-permute-start.5 = (bf16[576,128]{1,0:T(8,128)(2,1)S(1)}, bf16[576,128]{1,0:T(8,128)(2,1)S(1)}, u32[]{:S(2)}, u32[]{:S(2)}) collective-permute-start(bf16[576,128]{1,0:T(8,128)(2,1)S(1)} %get-tuple-element.28), channel_id=1, source_target_pairs={{32,0},{64,32},{128,96},{160,128},{192,160},{256,224},{288,256},{3... | collective-permute-start | bytes 442376 | tf_op jit(solution)/shard_map/ppermute | solution.py:26
  81.3 8.8 %collective-permute-start.6 = (bf16[576,128]{1,0:T(8,128)(2,1)S(1)}, bf16[576,128]{1,0:T(8,128)(2,1)S(1)}, u32[]{:S(2)}, u32[]{:S(2)}) collective-permute-start(bf16[576,128]{1,0:T(8,128)(2,1)S(1)} %get-tuple-element.29), channel_id=1, source_target_pairs={{64,0},{160,96},{192,128},{288,224},{320,256},{416,352},{448,384},... | collective-permute-start | bytes 442376 | tf_op jit(solution)/shard_map/ppermute | solution.py:26
  82.0 8.1 %collective-permute-start.7 = (bf16[576,128]{1,0:T(8,128)(2,1)S(1)}, bf16[576,128]{1,0:T(8,128)(2,1)S(1)}, u32[]{:S(2)}, u32[]{:S(2)}) collective-permute-start(bf16[576,128]{1,0:T(8,128)(2,1)S(1)} %get-tuple-element.30), channel_id=1, source_target_pairs={{192,96},{320,224},{448,352},{193,97},{321,225},{449,353},{194,98}... | collective-permute-start | bytes 442376 | tf_op jit(solution)/shard_map/ppermute | solution.py:26
  90.2 32.5 %collective-permute-start.8 = (bf16[576,128]{1,0:T(8,128)(2,1)S(1)}, bf16[576,128]{1,0:T(8,128)(2,1)S(1)}, u32[]{:S(2)}, u32[]{:S(2)}) collective-permute-start(bf16[576,128]{1,0:T(8,128)(2,1)S(1)} %shard_map.131.mine), channel_id=1, source_target_pairs={{0,1},{1,0},{2,3},{3,2},{4,5},{5,4},{6,7},{7,6},{8,9},{9,8},{10,11... | collective-permute-start | bytes 442376 | tf_op jit(solution)/shard_map/ppermute | solution.py:302
  94.3 41.4 %all-to-all-start.3 = ((f32[4,32,128]{2,1,0:T(8,128)}), f32[4,32,128]{2,1,0:T(8,128)S(1)}, u32[]{:S(2)}, u32[]{:S(2)}) async-start(f32[4,32,128]{2,1,0:T(8,128)} %shard_map.133), calls=%async_computation.3 | async-start | bytes 131072 | tf_op jit(solution)/shard_map/all_to_all | solution.py:306
  122.8 8.5 %collective-permute-start.9 = (bf16[576,128]{1,0:T(8,128)(2,1)S(1)}, bf16[576,128]{1,0:T(8,128)(2,1)S(1)}, u32[]{:S(2)}, u32[]{:S(2)}) collective-permute-start(bf16[576,128]{1,0:T(8,128)(2,1)S(1)} %shard_map.132.keys), channel_id=1, source_target_pairs={{0,2},{1,3},{2,0},{3,1},{4,6},{5,7},{6,4},{7,5},{8,10},{9,11},{10,... | collective-permute-start | bytes 442376 | tf_op jit(solution)/shard_map/ppermute | solution.py:302
